TPU v7x, 512 devices: a whole 4x4x16 slice. The times are simulated.
512 devices in a mesh: sp: 32 (over z, core), tp: 16 (over y, x).
Axes of the slice: x: 4, y: 4, z: 16, core: 2. Of those that a mesh axis runs over, the one named last changes fastest.
Arguments:
- target: bfloat16 [4096, 2048], P(('sp', 'tp')), may hold values from -3 to 3
- source: bfloat16 [24576, 2048], P(('sp', 'tp')), may hold values from -6 to 6
- target_gain: float32 [2048], replicated, may hold values from 0.1 to 1.9
- source_gain: float32 [2048], replicated, may hold values from 0.1 to 1.9
- query_weight: bfloat16 [2048, 2048], P(None, 'tp'), may hold values from -0.125 to 0.125
- key_matrix: bfloat16 [2048, 256], replicated, may hold values from -0.125 to 0.125
- value_matrix: bfloat16 [2048, 256], replicated, may hold values from -0.125 to 0.125
- query_gain: float32 [16, 128], P('tp'), may hold values from 0.24 to 20
- key_gain: float32 [2, 128], replicated, may hold values from 1.2 to 4
- out_weight: bfloat16 [2048, 2048], P('tp'), may hold values from -0.125 to 0.125
Outputs:
- updated_target: bfloat16 [4096, 2048], P(('sp', 'tp'))
All inputs are finite; a program needn't handle non-finite values.
Results may differ from a plain program's by a relative error of at most 0.018.
The roundings to bfloat16 on the way count: a program that leaves them out, or rounds other values in their place, can miss the bound.
Values may be sent and summed in bfloat16 or wider, within the bound.
No kernel may reach another device: no remote copies, remote signals or barrier semaphores. Data moves between devices by JAX's collectives and lax.ppermute only.
A program may use at most 64 MiB of HBM per device.

v0:
```python
import math

import jax
import jax.numpy as jnp
from jax import lax
from jax.sharding import PartitionSpec as P

QUERY_HEAD_COUNT = 16
KEY_VALUE_HEADS = 2
HEAD_SIZE = 128


EPSILON = 1e-06


def laid_out(blocks, dim):
    lengths = list(blocks.shape[1:])
    lengths[dim] *= blocks.shape[0]
    return jnp.moveaxis(blocks, 0, dim).reshape(lengths)


def copy_for_each(shard, axis):
    copies = jnp.broadcast_to(shard, (lax.axis_size(axis), *shard.shape))
    return lax.all_to_all(copies, axis, split_axis=0, concat_axis=0, tiled=True)


def collect(shard, axis, dim):
    return laid_out(copy_for_each(shard, axis), dim)


def side_by_side(arrays, axis, dim, along):
    both = jnp.concatenate(arrays, axis=along)
    filled, at, done = (lax.all_gather(both, axis, axis=dim, tiled=True), 0, [])
    for a in arrays:
        done.append(lax.slice_in_dim(filled, at, at + a.shape[along], axis=along))
        at += a.shape[along]
    return tuple(done)


def over_copies(shard, axis):
    everything = copy_for_each(shard, axis)
    return jnp.max(everything, axis=0)


def in_blocks_2(shard, dim, devices):
    before, after = (shard.shape[:dim], shard.shape[dim + 1 :])
    return jnp.moveaxis(shard.reshape(*before, devices, -1, *after), dim, 0)


def summed_on_arrival(shard, axis, dim):
    devices = lax.axis_size(axis)
    blocks = lax.all_to_all(in_blocks_2(shard, dim, devices), axis, 0, 0, tiled=True)
    return jnp.sum(blocks.astype(jnp.float32), axis=0)


def side_by_side_2(arrays, axis, dim, along):
    columns = [a.reshape(*a.shape[:along], -1) for a in arrays]
    both = jnp.concatenate(columns, axis=along)
    filled, at, done = (summed_on_arrival(both, axis, dim), 0, [])
    for a, column in zip(arrays, columns):
        section = filled[..., at : at + column.shape[along]]
        done.append(section.reshape(*section.shape[:along], *a.shape[along:]))
        at += column.shape[along]
    return tuple(done)


def normed(values_in, gain):
    return (
        values_in
        * lax.rsqrt(jnp.mean(values_in * values_in, axis=-1, keepdims=True) + EPSILON)
        * gain
    )


def softmax_step(running, scores, seg_values, form):
    maxima, totals, weighted = running
    new_maxima = jnp.maximum(maxima, jnp.max(scores, axis=-1))
    fading = jnp.exp(maxima - new_maxima)
    weights = jnp.exp(scores - new_maxima[..., None])
    totals = totals * fading + jnp.sum(weights, axis=-1)
    weighted = weighted * fading[..., None] + jnp.einsum(
        form, weights.astype(jnp.bfloat16), seg_values, preferred_element_type=jnp.float32
    )
    return (new_maxima, totals, weighted)


def in_blocks(advance, running, segment, own_rows, limit):
    length = segment[0].shape[0]
    shards = length // own_rows
    widest = max(own_rows, limit)
    per_block = max(
        [
            number
            for number in range(1, shards + 1)
            if shards % number == 0 and own_rows * number <= widest
        ]
    )
    blocks = shards // per_block
    shaped = tuple(
        (member.reshape((blocks, own_rows * per_block) + member.shape[1:]) for member in segment)
    )

    def one_turn(carried, portion):
        return (advance(carried, portion), None)

    return lax.scan(one_turn, running, shaped)[0]


def body(
    target,
    source,
    target_gain,
    source_gain,
    query_weight,
    key_matrix,
    value_matrix,
    query_gain,
    key_gain,
    out_weight,
):
    local_heads = query_weight.shape[1] // HEAD_SIZE
    heads_per_group = QUERY_HEAD_COUNT // KEY_VALUE_HEADS
    score_scale = 1.0 / math.sqrt(HEAD_SIZE)
    target_normed = normed(target.astype(jnp.float32), target_gain).astype(jnp.bfloat16)
    segment = collect(target_normed, "tp", 0)
    raw_queries = jnp.dot(segment, query_weight, preferred_element_type=jnp.float32)
    shaped = raw_queries.reshape(segment.shape[0], local_heads, HEAD_SIZE)
    query_vectors = normed(shaped, query_gain).astype(jnp.bfloat16)
    block_rows = query_vectors.shape[0]
    normed_source_rows = normed(source.astype(jnp.float32), source_gain).astype(jnp.bfloat16)
    unnormed_keys = jnp.dot(
        normed_source_rows, key_matrix, preferred_element_type=jnp.float32
    ).reshape(source.shape[0], KEY_VALUE_HEADS, HEAD_SIZE)
    key_rows = normed(unnormed_keys, key_gain).astype(jnp.bfloat16)
    value_vectors = (
        jnp.dot(normed_source_rows, value_matrix, preferred_element_type=jnp.float32)
        .astype(jnp.bfloat16)
        .reshape(source.shape[0], KEY_VALUE_HEADS, HEAD_SIZE)
    )
    all_heads = collect(query_vectors, "tp", 1).reshape(
        block_rows, KEY_VALUE_HEADS, heads_per_group, HEAD_SIZE
    )
    own_rows = key_rows.shape[0]
    group_keys, group_values = side_by_side((key_rows, value_vectors), "sp", 0, 1)

    def advance(carried, portion):
        scores = (
            jnp.einsum("rgqd,ngd->rgqn", all_heads, portion[0], preferred_element_type=jnp.float32)
            * score_scale
        )
        return softmax_step(carried, scores, portion[1], "rgqn,ngd->rgqd")

    small_shape = (block_rows, KEY_VALUE_HEADS, heads_per_group)
    initial = (
        jnp.full(small_shape, -1e30, jnp.float32),
        jnp.zeros(small_shape, jnp.float32),
        jnp.zeros(small_shape + (HEAD_SIZE,), jnp.float32),
    )
    maxima, totals, weighted = in_blocks(
        advance, initial, (group_keys, group_values), own_rows, 512
    )
    peaks = over_copies(maxima, "tp")
    fading = jnp.exp(maxima - peaks)
    summed, counted = side_by_side_2(
        (
            (weighted * fading[..., None])
            .reshape(block_rows, QUERY_HEAD_COUNT, HEAD_SIZE)
            .astype(jnp.bfloat16),
            (totals * fading).reshape(block_rows, QUERY_HEAD_COUNT).astype(jnp.bfloat16),
        ),
        "tp",
        1,
        2,
    )
    attended = (
        (summed / counted[..., None])
        .astype(jnp.bfloat16)
        .reshape(block_rows, local_heads * HEAD_SIZE)
    )
    portion = attended
    update = summed_on_arrival(
        jnp.dot(portion, out_weight, preferred_element_type=jnp.float32).astype(jnp.bfloat16),
        "tp",
        0,
    )
    return (target.astype(jnp.float32) + update).astype(jnp.bfloat16)


def solution(mesh):
    return jax.shard_map(
        body,
        mesh=mesh,
        in_specs=(
            P(("sp", "tp"), None),
            P(("sp", "tp"), None),
            P(),
            P(),
            P(None, "tp"),
            P(),
            P(),
            P("tp", None),
            P(),
            P("tp", None),
        ),
        out_specs=P(("sp", "tp"), None),
        check_vma=False,
    )
```

profile of v0, /device:TPU:32, one launch (start us, length us, event | category | flops | bytes accessed | tf_op | source)
XLA Modules:
  0.0 168.9 jit_solution(11723891742025835742)
XLA Ops:
  6.6 1.2 fusion.26
  7.9 1.3 fusion.35
  9.4 1.7 %fusion.23 = bf16[6,2,8,128]{3,2,1,0:T(8,128)(2,1)S(1)} fusion(bf16[2048,256]{1,0:T(8,128)(2,1)} %param.18, bf16[48,2048]{1,0:T(8,128)(2,1)} %param.13, f32[2048]{0:T(1024)} %param.15, f32[48]{0:T(128)S(1)} %add_rsqrt_fusion.3), kind=kOutput, calls=%fused_computation.27 | convolution fusion | flops 50737152 | bytes 1278144 | tf_op jit(solution)/shard_map/dot_general | solution.py:136
  13.6 7.0 %all-to-all-start = ((bf16[16,8,2048]{2,1,0:T(8,128)(2,1)}), bf16[16,8,2048]{2,1,0:T(8,128)(2,1)S(1)}, u32[]{:S(2)}, u32[]{:S(2)}) async-start(bf16[16,8,2048]{2,1,0:T(8,128)(2,1)} %broadcast_in_dim.17), calls=%async_computation | async-start | bytes 1048576 | tf_op jit(solution)/shard_map/all_to_all | solution.py:24
  20.7 11.5 %all-to-all-done = bf16[16,8,2048]{2,1,0:T(8,128)(2,1)S(1)} async-done(((bf16[16,8,2048]{2,1,0:T(8,128)(2,1)}), bf16[16,8,2048]{2,1,0:T(8,128)(2,1)S(1)}, u32[]{:S(2)}, u32[]{:S(2)}) %all-to-all-start) | async-done | bytes 524320 | tf_op jit(solution)/shard_map/all_to_all | solution.py:24
  33.7 3.6 %all-to-all-start.1 = ((bf16[16,128,1,128]{3,1,2,0:T(8,128)(2,1)}), bf16[16,128,1,128]{3,1,2,0:T(8,128)(2,1)S(1)}, u32[]{:S(2)}, u32[]{:S(2)}) async-start(bf16[16,128,1,128]{3,1,2,0:T(8,128)(2,1)} %broadcast_in_dim.18), calls=%async_computation.1 | async-start | bytes 1048576 | tf_op jit(solution)/shard_map/all_to_all | solution.py:24
  37.3 50.4 %all-gather.2.cloned.1.call-done = bf16[1536,4,128]{2,0,1:T(8,128)(2,1)} async-done(((bf16[48,4,128]{2,0,1:T(8,128)(2,1)}), bf16[1536,4,128]{2,0,1:T(8,128)(2,1)}) %all-gather.2.cloned.1.call-update) | async-done | bytes 1572880 | tf_op jit(solution)/shard_map/all_gather | solution.py:33
  87.7 2.4 %fusion.42 = (bf16[1536,2,128]{2,0,1:T(8,128)(2,1)S(1)}, bf16[1536,2,128]{2,0,1:T(8,128)(2,1)}) fusion(bf16[1536,4,128]{2,0,1:T(8,128)(2,1)} %all-gather.2.cloned.1.call-done), kind=kLoop, calls=%fused_computation.65 | loop fusion | bytes 3145728 | tf_op jit(solution)/shard_map/slice | solution.py:35
  90.0 28.3 %while.15 = (s32[]{:T(128)}, f32[128,2,8]{0,2,1:T(8,128)S(1)}, f32[128,2,8]{0,2,1:T(8,128)S(1)}, f32[128,2,8,128]{0,3,2,1:T(8,128)S(1)}, bf16[4,384,2,128]{3,1,0...) while((s32[]{:T(128)}, f32[128,2,8]{0,2,1:T(8,128)S(1)}, ...), condition=%wide.region_7.8_spmd.clone, body=%wide.region_4.7_spmd.clone.sunk | while | flops 409741312 | bytes 25166472 | solution.py:106
  90.0 3.2 %bitcast_reduce_fusion.2 = (f32[128,2,8]{0,2,1:T(8,128)S(1)}, f32[2,384,128,8]{2,1,3,0:T(8,128)}) fusion(bf16[128,2,8,128]{3,0,2,1:T(8,128)(2,1)S(1)} %get-tuple-element.197, bf16[4,384,2,128]{3,1,0,2:T(8,128)(2,1)} %get-tuple-element.196, s32[]{:T(128)} %get-tuple-element.183), kind=kOutput, calls=%fused_computation.1.clone.1 | convolution fusion | flops 202897408 | bytes 3875328 | tf_op jit(solution)/shard_map/while/body/eval_jaxpr/rgqd,ngd->rgqn/dot_general | solution.py:148
  93.2 2.6 %fusion.58 = f32[128,2,8]{0,2,1:T(8,128)S(1)} fusion(f32[2,384,128,8]{2,1,3,0:T(8,128)} %get-tuple-element.171, f32[128,2,8]{0,2,1:T(8,128)S(1)} %select_maximum_fusion.2), kind=kLoop, calls=%fused_computation.4.clone.1 | loop fusion | flops 2357248 | bytes 3162112 | tf_op jit(solution)/shard_map/while/body/eval_jaxpr/reduce_sum | solution.py:80
  96.1 1.0 fusion.60
  97.1 3.2 %bitcast_reduce_fusion.2 = (f32[128,2,8]{0,2,1:T(8,128)S(1)}, f32[2,384,128,8]{2,1,3,0:T(8,128)}) fusion(bf16[128,2,8,128]{3,0,2,1:T(8,128)(2,1)S(1)} %get-tuple-element.197, bf16[4,384,2,128]{3,1,0,2:T(8,128)(2,1)} %get-tuple-element.196, s32[]{:T(128)} %get-tuple-element.183), kind=kOutput, calls=%fused_computation.1.clone.1 | convolution fusion | flops 202897408 | bytes 3875328 | tf_op jit(solution)/shard_map/while/body/eval_jaxpr/rgqd,ngd->rgqn/dot_general | solution.py:148
  100.3 2.6 %fusion.58 = f32[128,2,8]{0,2,1:T(8,128)S(1)} fusion(f32[2,384,128,8]{2,1,3,0:T(8,128)} %get-tuple-element.171, f32[128,2,8]{0,2,1:T(8,128)S(1)} %select_maximum_fusion.2), kind=kLoop, calls=%fused_computation.4.clone.1 | loop fusion | flops 2357248 | bytes 3162112 | tf_op jit(solution)/shard_map/while/body/eval_jaxpr/reduce_sum | solution.py:80
  103.1 1.0 fusion.60
  104.2 3.2 %bitcast_reduce_fusion.2 = (f32[128,2,8]{0,2,1:T(8,128)S(1)}, f32[2,384,128,8]{2,1,3,0:T(8,128)}) fusion(bf16[128,2,8,128]{3,0,2,1:T(8,128)(2,1)S(1)} %get-tuple-element.197, bf16[4,384,2,128]{3,1,0,2:T(8,128)(2,1)} %get-tuple-element.196, s32[]{:T(128)} %get-tuple-element.183), kind=kOutput, calls=%fused_computation.1.clone.1 | convolution fusion | flops 202897408 | bytes 3875328 | tf_op jit(solution)/shard_map/while/body/eval_jaxpr/rgqd,ngd->rgqn/dot_general | solution.py:148
  107.4 2.6 %fusion.58 = f32[128,2,8]{0,2,1:T(8,128)S(1)} fusion(f32[2,384,128,8]{2,1,3,0:T(8,128)} %get-tuple-element.171, f32[128,2,8]{0,2,1:T(8,128)S(1)} %select_maximum_fusion.2), kind=kLoop, calls=%fused_computation.4.clone.1 | loop fusion | flops 2357248 | bytes 3162112 | tf_op jit(solution)/shard_map/while/body/eval_jaxpr/reduce_sum | solution.py:80
  110.2 1.0 fusion.60
  111.3 3.2 %bitcast_reduce_fusion.2 = (f32[128,2,8]{0,2,1:T(8,128)S(1)}, f32[2,384,128,8]{2,1,3,0:T(8,128)}) fusion(bf16[128,2,8,128]{3,0,2,1:T(8,128)(2,1)S(1)} %get-tuple-element.197, bf16[4,384,2,128]{3,1,0,2:T(8,128)(2,1)} %get-tuple-element.196, s32[]{:T(128)} %get-tuple-element.183), kind=kOutput, calls=%fused_computation.1.clone.1 | convolution fusion | flops 202897408 | bytes 3875328 | tf_op jit(solution)/shard_map/while/body/eval_jaxpr/rgqd,ngd->rgqn/dot_general | solution.py:148
  114.5 2.6 %fusion.58 = f32[128,2,8]{0,2,1:T(8,128)S(1)} fusion(f32[2,384,128,8]{2,1,3,0:T(8,128)} %get-tuple-element.171, f32[128,2,8]{0,2,1:T(8,128)S(1)} %select_maximum_fusion.2), kind=kLoop, calls=%fused_computation.4.clone.1 | loop fusion | flops 2357248 | bytes 3162112 | tf_op jit(solution)/shard_map/while/body/eval_jaxpr/reduce_sum | solution.py:80
  117.3 1.0 fusion.60
  118.4 14.7 %all_to_all.25 = f32[16,128,2,8]{1,3,2,0:T(8,128)S(1)} all-to-all(f32[16,128,2,8]{1,3,2,0:T(8,128)S(1)} %broadcast_in_dim.34), channel_id=1, replica_groups=mesh['sp'=32,'tp'=16] {'tp'}, dimensions={0} | all-to-all | bytes 262144 | tf_op jit(solution)/shard_map/all_to_all | solution.py:24
  133.4 14.3 %all_to_all.26 = bf16[16,128,1,129]{1,3,2,0:T(8,128)(2,1)S(1)} all-to-all(bf16[16,128,1,129]{1,3,2,0:T(8,128)(2,1)S(1)} %maximum_bitcast_fusion), channel_id=1, replica_groups=mesh['sp'=32,'tp'=16] {'tp'}, dimensions={0} | all-to-all | bytes 1056768 | tf_op jit(solution)/shard_map/all_to_all | solution.py:52
  148.1 13.2 %all_to_all.27 = bf16[16,8,2048]{2,1,0:T(8,128)(2,1)S(1)} all-to-all(bf16[16,8,2048]{2,1,0:T(8,128)(2,1)S(1)} %fusion.22), channel_id=1, replica_groups=mesh['sp'=32,'tp'=16] {'tp'}, dimensions={0} | all-to-all | bytes 1048576 | tf_op jit(solution)/shard_map/all_to_all | solution.py:52
  (66 shorter events, 6.7 us)
Async XLA Ops:
  6.5 1.3 copy-start
  6.5 6.0 %copy-start.4 = (bf16[8,2048]{1,0:T(8,128)(2,1)S(1)}, bf16[8,2048]{1,0:T(8,128)(2,1)}, u32[]{:S(2)}) copy-start(bf16[8,2048]{1,0:T(8,128)(2,1)} %param.12) | copy-start | bytes 98308
  6.5 6.1 %copy-start.5 = (f32[2048]{0:T(1024)S(1)}, f32[2048]{0:T(1024)}, u32[]{:S(2)}) copy-start(f32[2048]{0:T(1024)} %param.14) | copy-start | bytes 24580
  6.5 25.6 %copy-start.2 = (bf16[2048,128]{1,0:T(8,128)(2,1)S(1)}, bf16[2048,128]{1,0:T(8,128)(2,1)}, u32[]{:S(2)}) copy-start(bf16[2048,128]{1,0:T(8,128)(2,1)} %param.16) | copy-start | bytes 1572868
  6.5 26.0 %copy-start.6 = (f32[1,128]{1,0:T(1,128)S(1)}, f32[1,128]{1,0:T(1,128)}, u32[]{:S(2)}) copy-start(f32[1,128]{1,0:T(1,128)} %param.19) | copy-start | bytes 1540
  6.5 81.1 %all-gather.2.cloned.1.call-start = ((), (), s32[]{:S(2)}) async-start(), calls=%async_computation.5 | async-start | bytes 1622016 | tf_op jit(solution)/shard_map/all_gather | solution.py:33
  13.6 18.6 %all-to-all-start = ((bf16[16,8,2048]{2,1,0:T(8,128)(2,1)}), bf16[16,8,2048]{2,1,0:T(8,128)(2,1)S(1)}, u32[]{:S(2)}, u32[]{:S(2)}) async-start(bf16[16,8,2048]{2,1,0:T(8,128)(2,1)} %broadcast_in_dim.17), calls=%async_computation | async-start | bytes 1048576 | tf_op jit(solution)/shard_map/all_to_all | solution.py:24
  33.7 56.4 %all-to-all-start.1 = ((bf16[16,128,1,128]{3,1,2,0:T(8,128)(2,1)}), bf16[16,128,1,128]{3,1,2,0:T(8,128)(2,1)S(1)}, u32[]{:S(2)}, u32[]{:S(2)}) async-start(bf16[16,128,1,128]{3,1,2,0:T(8,128)(2,1)} %broadcast_in_dim.18), calls=%async_computation.1 | async-start | bytes 1048576 | tf_op jit(solution)/shard_map/all_to_all | solution.py:24
  93.2 2.8 %copy-start.1 = (f32[2,384,128,8]{2,1,3,0:T(8,128)S(1)}, f32[2,384,128,8]{2,1,3,0:T(8,128)}, u32[]{:S(2)}) copy-start(f32[2,384,128,8]{2,1,3,0:T(8,128)} %get-tuple-element.171) | copy-start | bytes 9437188 | tf_op jit(solution)/shard_map/while
  100.3 2.8 %copy-start.1 = (f32[2,384,128,8]{2,1,3,0:T(8,128)S(1)}, f32[2,384,128,8]{2,1,3,0:T(8,128)}, u32[]{:S(2)}) copy-start(f32[2,384,128,8]{2,1,3,0:T(8,128)} %get-tuple-element.171) | copy-start | bytes 9437188 | tf_op jit(solution)/shard_map/while
  107.4 2.8 %copy-start.1 = (f32[2,384,128,8]{2,1,3,0:T(8,128)S(1)}, f32[2,384,128,8]{2,1,3,0:T(8,128)}, u32[]{:S(2)}) copy-start(f32[2,384,128,8]{2,1,3,0:T(8,128)} %get-tuple-element.171) | copy-start | bytes 9437188 | tf_op jit(solution)/shard_map/while
  114.5 2.8 %copy-start.1 = (f32[2,384,128,8]{2,1,3,0:T(8,128)S(1)}, f32[2,384,128,8]{2,1,3,0:T(8,128)}, u32[]{:S(2)}) copy-start(f32[2,384,128,8]{2,1,3,0:T(8,128)} %get-tuple-element.171) | copy-start | bytes 9437188 | tf_op jit(solution)/shard_map/while
  118.4 29.4 %copy-start.3 = (bf16[128,2048]{1,0:T(8,128)(2,1)S(1)}, bf16[128,2048]{1,0:T(8,128)(2,1)}, u32[]{:S(2)}) copy-start(bf16[128,2048]{1,0:T(8,128)(2,1)} %param.21) | copy-start | bytes 1572868
Sparse Core Ops, SparseCore 0:
  12.6 75.0 all-gather.1
where the time goes:
time: 169 us
  waiting for transfers between devices  61.9 us (37%)
  blocking collectives  42.2 us (25%)
  matrix products  20.5 us (12%)
  other arithmetic  14.4 us (9%)
  between operations  13.6 us (8%)
  starting transfers between devices  10.6 us (6%)
  local copies, waits for them, and re-layouts  5.41 us (3%)
    all_gather x1, waiting for transfers between devices, side_by_side(): filled, at, done = (lax.all_gather(both, axis, axis=dim, tiled=True), 0, [])  50.4 us
    all_to_all x2, blocking collectives, summed_on_arrival(): lax.all_to_all(in_blocks_2(shard, dim, devices), axis, 0, 0, tiled=True)  27.5 us
    all_to_all x1, blocking collectives, copy_for_each(): return lax.all_to_all(copies, axis, split_axis=0, concat_axis=0, tiled=True)  14.7 us
    dot_general x4, matrix products, advance(): jnp.einsum('rgqd,ngd->rgqn', all_heads, portion[0], preferred_element_typ...  12.7 us
    all_to_all x2, waiting for transfers between devices, copy_for_each(): return lax.all_to_all(copies, axis, split_axis=0, concat_axis=0, tiled=True)  11.5 us
    all_to_all x2, starting transfers between devices, copy_for_each(): return lax.all_to_all(copies, axis, split_axis=0, concat_axis=0, tiled=True)  10.6 us
    reduce_sum x4, other arithmetic, softmax_step(): totals = totals * fading + jnp.sum(weights, axis=-1)  10.3 us
    dot_general x4, matrix products, softmax_step(): jnp.einsum(form, weights.astype(jnp.bfloat16), seg_values, preferred_elem...  4.18 us
  transfers between devices with their start and end apart: 3, of which 2 were waited for; matrix products, arithmetic and copies ran while one was open for 3% of the time, Pallas kernels for 0%

commit v1 on v0

v1 whole, which is shorter than its diff:
```python
import math

import jax
import jax.numpy as jnp
from jax import lax
from jax.experimental import pallas as pl
from jax.experimental.pallas import tpu as pltpu
from jax.sharding import PartitionSpec as P


QUERY_HEAD_COUNT = 16
KEY_VALUE_HEADS = 2
HEAD_SIZE = 128
GROUP = QUERY_HEAD_COUNT // KEY_VALUE_HEADS
EPSILON = 1e-06
EXP2_SCALE = math.log2(math.e) / math.sqrt(HEAD_SIZE)
STAT_ROWS = 16

VMEM = pl.BlockSpec(memory_space=pltpu.VMEM)


def cost(flops, nbytes, transcendentals=0):
    return pl.CostEstimate(
        flops=flops, bytes_accessed=nbytes, transcendentals=transcendentals
    )


def normed(values_in, gain):
    return (
        values_in
        * lax.rsqrt(jnp.mean(values_in * values_in, axis=-1, keepdims=True) + EPSILON)
        * gain
    )


def key_value_kernel(source, gain, key_matrix, value_matrix, key_gain, own, other):
    second = lax.axis_index("tp") >= GROUP
    rows = normed(source[...].astype(jnp.float32), gain[...]).astype(jnp.bfloat16)
    raw = jnp.dot(rows, key_matrix[...], preferred_element_type=jnp.float32)
    values = jnp.dot(rows, value_matrix[...], preferred_element_type=jnp.float32)
    values = values.astype(jnp.bfloat16)
    heads = []
    for h in range(KEY_VALUE_HEADS):
        at = slice(h * HEAD_SIZE, (h + 1) * HEAD_SIZE)
        keys = normed(raw[:, at], key_gain[h : h + 1, :]).astype(jnp.bfloat16)
        heads.append(jnp.concatenate([keys, values[:, at]], axis=1))
    own[...] = jnp.where(second, heads[1], heads[0])
    other[...] = jnp.where(second, heads[0], heads[1])


def query_kernel(target, gain, weight, head_gain, copies):
    rows = normed(target[...].astype(jnp.float32), gain[...]).astype(jnp.bfloat16)
    raw = jnp.dot(rows, weight[...], preferred_element_type=jnp.float32)
    queries = normed(raw, head_gain[...]).astype(jnp.bfloat16)
    for i in range(GROUP):
        copies[i] = queries


def in_three(x):
    first = x.astype(jnp.bfloat16)
    rest = x - first.astype(jnp.float32)
    second = rest.astype(jnp.bfloat16)
    third = (rest - second.astype(jnp.float32)).astype(jnp.bfloat16)
    return [first, second, third]


def attention_kernel(queries, near, far, out):
    per_tile = 2
    rows = per_tile * HEAD_SIZE
    at_row = lax.broadcasted_iota(jnp.int32, (HEAD_SIZE, HEAD_SIZE), 0)
    at_lane = lax.broadcasted_iota(jnp.int32, (HEAD_SIZE, HEAD_SIZE), 1)
    eye = (at_row == at_lane).astype(jnp.float32)

    def as_row(column):
        return jnp.sum(eye * column, axis=0, keepdims=True)

    for tile in range(GROUP // per_tile):
        q = queries[tile * per_tile : (tile + 1) * per_tile].reshape(rows, HEAD_SIZE)
        scores = [
            lax.dot_general(
                q,
                kv[:, :HEAD_SIZE],
                (((1,), (1,)), ((), ())),
                preferred_element_type=jnp.float32,
            )
            for kv in (near, far)
        ]
        peak = jnp.maximum(
            jnp.max(scores[0], axis=-1, keepdims=True),
            jnp.max(scores[1], axis=-1, keepdims=True),
        )
        total, weighted = 0.0, 0.0
        for kv, s in zip((near, far), scores):
            weights = jnp.exp2((s - peak) * EXP2_SCALE)
            total += jnp.sum(weights, axis=-1, keepdims=True)
            weighted += jnp.dot(
                weights.astype(jnp.bfloat16),
                kv[:, HEAD_SIZE:],
                preferred_element_type=jnp.float32,
            )
        for i in range(per_tile):
            at = slice(i * HEAD_SIZE, (i + 1) * HEAD_SIZE)
            head = tile * per_tile + i
            out[head, :HEAD_SIZE, :] = weighted[at].astype(jnp.bfloat16)
            stats = in_three(as_row(peak[at])) + in_three(as_row(total[at]))
            empty = jnp.zeros((STAT_ROWS - len(stats), HEAD_SIZE), jnp.bfloat16)
            out[head, HEAD_SIZE:, :] = jnp.concatenate(stats + [empty], axis=0)


def output_kernel(partials, weight, out):
    at_row = lax.broadcasted_iota(jnp.int32, (HEAD_SIZE, HEAD_SIZE), 0)
    at_lane = lax.broadcasted_iota(jnp.int32, (HEAD_SIZE, HEAD_SIZE), 1)
    eye = (at_row == at_lane).astype(jnp.float32)
    peaks, totals = [], []
    for j in range(GROUP):
        stats = partials[j, HEAD_SIZE:, :].astype(jnp.float32)
        peaks.append(stats[0:1] + stats[1:2] + stats[2:3])
        totals.append(stats[3:4] + stats[4:5] + stats[5:6])
    peak = peaks[0]
    for p in peaks[1:]:
        peak = jnp.maximum(peak, p)
    fades = [jnp.exp2((p - peak) * EXP2_SCALE) for p in peaks]
    total = fades[0] * totals[0]
    for f, t in zip(fades[1:], totals[1:]):
        total += f * t
    attended = 0.0
    for j in range(GROUP):
        column = jnp.sum(eye * (fades[j] / total), axis=1, keepdims=True)
        attended += column * partials[j, :HEAD_SIZE, :].astype(jnp.float32)
    update = jnp.dot(
        attended.astype(jnp.bfloat16), weight[...], preferred_element_type=jnp.float32
    )
    out[...] = update.astype(jnp.bfloat16).reshape(out.shape)


def final_kernel(target, parts, out):
    update = parts[0].astype(jnp.float32)
    for i in range(1, parts.shape[0]):
        update += parts[i].astype(jnp.float32)
    out[...] = (target[...].astype(jnp.float32) + update).astype(jnp.bfloat16)


def call(kernel, outs, estimate, count):
    return pl.pallas_call(
        kernel,
        out_shape=outs,
        in_specs=[VMEM] * count,
        out_specs=jax.tree.map(lambda _: VMEM, outs),
        cost_estimate=estimate,
        compiler_params=pltpu.CompilerParams(vmem_limit_bytes=48 * 1024 * 1024),
    )


def bf16(*shape):
    return jax.ShapeDtypeStruct(shape, jnp.bfloat16)


def body(
    target,
    source,
    target_gain,
    source_gain,
    query_weight,
    key_matrix,
    value_matrix,
    query_gain,
    key_gain,
    out_weight,
):
    width = target.shape[1]
    tp = lax.axis_size("tp")
    sp = lax.axis_size("sp")
    own_rows = target.shape[0]
    block = own_rows * tp
    source_rows = source.shape[0]
    halves = [[i + h * GROUP for i in range(GROUP)] for h in range(KEY_VALUE_HEADS)]
    along_z = [[core + 2 * z for z in range(sp // 2)] for core in range(2)]

    everyone = lax.all_to_all(
        jnp.broadcast_to(target, (tp, own_rows, width)), "tp", 0, 0, tiled=True
    ).reshape(block, width)
    own, other = call(
        key_value_kernel,
        (bf16(source_rows, 2 * HEAD_SIZE), bf16(source_rows, 2 * HEAD_SIZE)),
        cost(2 * source_rows * width * 512, 2400000),
        5,
    )(source, source_gain.reshape(1, width), key_matrix, value_matrix, key_gain)
    received = lax.ppermute(other, "tp", [(i, i ^ GROUP) for i in range(tp)])
    copies = call(
        query_kernel,
        bf16(GROUP, block, HEAD_SIZE),
        cost(2 * block * width * HEAD_SIZE, 1400000),
        4,
    )(everyone, target_gain.reshape(1, width), query_weight, query_gain)
    all_queries = lax.all_to_all(
        copies, "tp", 0, 0, tiled=True, axis_index_groups=halves
    )
    near = lax.all_gather(
        jnp.concatenate([own, received], axis=0),
        "sp",
        axis=0,
        tiled=True,
        axis_index_groups=along_z,
    )
    far = lax.ppermute(near, "sp", [(i, i ^ 1) for i in range(sp)])
    keys = 2 * near.shape[0]
    partials = call(
        attention_kernel,
        bf16(GROUP, block + STAT_ROWS, HEAD_SIZE),
        cost(4 * GROUP * block * keys * HEAD_SIZE, 2500000, GROUP * block * keys),
        3,
    )(all_queries, near, far)
    mine = lax.all_to_all(partials, "tp", 0, 0, tiled=True, axis_index_groups=halves)
    update = call(
        output_kernel,
        bf16(tp, own_rows, width),
        cost(2 * block * width * HEAD_SIZE, 1400000),
        2,
    )(mine, out_weight)
    parts = lax.all_to_all(update, "tp", 0, 0, tiled=True)
    return call(
        final_kernel, bf16(own_rows, width), cost(tp * own_rows * width, 600000), 2
    )(target, parts)


def solution(mesh):
    return jax.shard_map(
        body,
        mesh=mesh,
        in_specs=(
            P(("sp", "tp"), None),
            P(("sp", "tp"), None),
            P(),
            P(),
            P(None, "tp"),
            P(),
            P(),
            P("tp", None),
            P(),
            P("tp", None),
        ),
        out_specs=P(("sp", "tp"), None),
        check_vma=False,
    )
```

time: 169 us -> 114 us (0.67)
  the two profiles are of different devices: /device:TPU:32 before, /device:TPU:2 now
where the time goes in v1:
time: 114 us
  blocking collectives  92 us (81%)
  Pallas kernels  7.05 us (6%)
  starting transfers between devices  7.01 us (6%)
  local copies, waits for them, and re-layouts  5.47 us (5%)
  waiting for transfers between devices  2.12 us (2%)
    all_gather x1, blocking collectives, body(): lax.all_gather(jnp.concatenate([own, received], axis=0), 'sp', axis=0, ti...  40.4 us
    all_to_all x1, blocking collectives, body(): lax.all_to_all(jnp.broadcast_to(target, (tp, own_rows, width)), 'tp', 0,...  18.2 us
    all_to_all x1, blocking collectives, body(): parts = lax.all_to_all(update, 'tp', 0, 0, tiled=True)  13.2 us
    all_to_all x1, blocking collectives, body(): lax.all_to_all(partials, 'tp', 0, 0, tiled=True, axis_index_groups=halves)  10.1 us
    all_to_all x1, blocking collectives, body(): lax.all_to_all(copies, 'tp', 0, 0, tiled=True, axis_index_groups=halves)  9.99 us
    unnamed x20, local copies, waits for them, and re-layouts  5.42 us
    ppermute x1, starting transfers between devices, body(): received = lax.ppermute(other, 'tp', [(i, i ^ GROUP) for i in range(tp)])  5.1 us
    pallas_call x1, Pallas kernels, body(): call(attention_kernel, bf16(GROUP, block + STAT_ROWS, HEAD_SIZE), cost(4...  4.7 us
  transfers between devices with their start and end apart: 2, of which 1 were waited for; matrix products, arithmetic and copies ran while one was open for 0% of the time, Pallas kernels for 0%

profile of v1, /device:TPU:2, one launch (start us, length us, event | category | flops | bytes accessed | tf_op | source)
XLA Modules:
  0.0 113.7 jit_solution(15666150861732202585)
XLA Ops:
  0.0 0.7 copy-done.8
  0.7 1.2 %copy-done = bf16[2048,256]{1,0:T(8,128)(2,1)S(1)} copy-done((bf16[2048,256]{1,0:T(8,128)(2,1)S(1)}, bf16[2048,256]{1,0:T(8,128)(2,1)}, u32[]{:S(2)}) %copy-start) | copy-done | bytes 1048600
  1.9 1.2 %copy-done.1 = bf16[2048,256]{1,0:T(8,128)(2,1)S(1)} copy-done((bf16[2048,256]{1,0:T(8,128)(2,1)S(1)}, bf16[2048,256]{1,0:T(8,128)(2,1)}, u32[]{:S(2)}) %copy-start.1) | copy-done | bytes 1048600
  3.1 0.9 copy-done.4
  4.1 0.7 copy-done.6
  4.8 0.6 shard_map.101
  5.4 5.1 %collective-permute-start = (bf16[48,256]{1,0:T(8,128)(2,1)S(1)}, bf16[48,256]{1,0:T(8,128)(2,1)S(1)}, u32[]{:S(2)}, u32[]{:S(2)}) collective-permute-start(bf16[48,256]{1,0:T(8,128)(2,1)S(1)} %get-tuple-element.8), channel_id=1, source_target_pairs={{0,8},{1,9},{2,10},{3,11},{4,12},{5,13},{6,14},{7,15},{8,0},{9,1},... | collective-permute-start | bytes 73736 | tf_op jit(solution)/shard_map/ppermute | solution.py:188
  10.5 2.1 %collective-permute-done = bf16[48,256]{1,0:T(8,128)(2,1)S(1)} collective-permute-done((bf16[48,256]{1,0:T(8,128)(2,1)S(1)}, bf16[48,256]{1,0:T(8,128)(2,1)S(1)}, u32[]{:S(2)}, u32[]{:S(2)}) %collective-permute-start) | collective-permute-done | bytes 24608 | tf_op jit(solution)/shard_map/ppermute | solution.py:188
  12.6 40.4 %all_gather.3.near = bf16[1536,256]{1,0:T(8,128)(2,1)S(1)} all-gather(bf16[96,256]{1,0:T(8,128)(2,1)S(1)} %pad_maximum_fusion), channel_id=1, replica_groups={{0,32,64,96,128,160,192,224,256,288,320,352,384,416,448,480},{16,48,80,..., dimensions={0}, use_global_device_ids=true | all-gather | bytes 835584 | tf_op jit(solution)/shard_map/all_gather | solution.py:198
  53.0 1.9 %collective-permute-start.1 = (bf16[1536,256]{1,0:T(8,128)(2,1)S(1)}, bf16[1536,256]{1,0:T(8,128)(2,1)S(1)}, u32[]{:S(2)}, u32[]{:S(2)}) collective-permute-start(bf16[1536,256]{1,0:T(8,128)(2,1)S(1)} %all_gather.3.near), channel_id=1, source_target_pairs={{0,16},{16,0},{32,48},{48,32},{64,80},{80,64},{96,112},{112,96},{1... | collective-permute-start | bytes 2359304 | tf_op jit(solution)/shard_map/ppermute | solution.py:205
  54.9 0.0 copy-done.5
  55.0 0.0 copy-start.2
  55.0 0.0 copy-start.7
  55.0 18.2 %all_to_all.20 = bf16[16,8,2048]{2,1,0:T(8,128)(2,1)S(1)} all-to-all(bf16[16,8,2048]{2,1,0:T(8,128)(2,1)S(1)} %broadcast_in_dim.3), channel_id=1, replica_groups=mesh['sp'=32,'tp'=16] {'tp'}, dimensions={0} | all-to-all | bytes 1048576 | tf_op jit(solution)/shard_map/all_to_all | solution.py:179
  73.3 0.6 copy-done.9
  73.9 0.5 shard_map.100
  74.5 10.0 %all_to_all.21.queries = bf16[8,128,128]{2,1,0:T(8,128)(2,1)S(1)} all-to-all(bf16[8,128,128]{2,1,0:T(8,128)(2,1)S(1)} %shard_map.100), channel_id=1, replica_groups={{0,1,2,3,4,5,6,7},{8,9,10,11,12,13,14,15},{16,17,18,19,20,21,22,23},{24..., dimensions={0} | all-to-all | bytes 524288 | tf_op jit(solution)/shard_map/all_to_all | solution.py:195
  84.5 0.0 collective-permute-done.1.far
  84.5 4.7 %shard_map.102 = bf16[8,144,128]{2,1,0:T(8,128)(2,1)S(1)} custom-call(bf16[8,128,128]{2,1,0:T(8,128)(2,1)S(1)} %all_to_all.21.queries, bf16[1536,256]{1,0:T(8,128)(2,1)S(1)} %all_gather.3.near, bf16[1536,256]{1,0:T(8,128)(2,1)S(1)} %collective-permute-done.1.far), custom_call_target="tpu_custom_call" | custom-call | flops 1610612736 | bytes 2500000 | tf_op jit(solution)/shard_map/pallas_call | solution.py:207
  89.2 0.0 copy-start.3
  89.2 10.1 %all_to_all.22.partials = bf16[8,144,128]{2,1,0:T(8,128)(2,1)S(1)} all-to-all(bf16[8,144,128]{2,1,0:T(8,128)(2,1)S(1)} %shard_map.102), channel_id=1, replica_groups={{0,1,2,3,4,5,6,7},{8,9,10,11,12,13,14,15},{16,17,18,19,20,21,22,23},{24..., dimensions={0} | all-to-all | bytes 589824 | tf_op jit(solution)/shard_map/all_to_all | solution.py:213
  99.3 0.5 shard_map.103
  99.8 13.2 %all_to_all.23.parts = bf16[16,8,2048]{2,1,0:T(8,128)(2,1)S(1)} all-to-all(bf16[16,8,2048]{2,1,0:T(8,128)(2,1)S(1)} %shard_map.103), channel_id=1, replica_groups=mesh['sp'=32,'tp'=16] {'tp'}, dimensions={0} | all-to-all | bytes 1048576 | tf_op jit(solution)/shard_map/all_to_all | solution.py:220
  113.0 0.7 shard_map.104
  (12 shorter events, 0.1 us)
Async XLA Ops:
  0.0 0.7 copy-start.8
  0.7 1.2 %copy-start = (bf16[2048,256]{1,0:T(8,128)(2,1)S(1)}, bf16[2048,256]{1,0:T(8,128)(2,1)}, u32[]{:S(2)}) copy-start(bf16[2048,256]{1,0:T(8,128)(2,1)} %key_matrix.1) | copy-start | bytes 3145732
  1.9 1.2 %copy-start.1 = (bf16[2048,256]{1,0:T(8,128)(2,1)S(1)}, bf16[2048,256]{1,0:T(8,128)(2,1)}, u32[]{:S(2)}) copy-start(bf16[2048,256]{1,0:T(8,128)(2,1)} %value_matrix.1) | copy-start | bytes 3145732
  3.1 0.9 copy-start.4
  4.1 0.7 copy-start.6
  5.4 7.2 %collective-permute-start = (bf16[48,256]{1,0:T(8,128)(2,1)S(1)}, bf16[48,256]{1,0:T(8,128)(2,1)S(1)}, u32[]{:S(2)}, u32[]{:S(2)}) collective-permute-start(bf16[48,256]{1,0:T(8,128)(2,1)S(1)} %get-tuple-element.8), channel_id=1, source_target_pairs={{0,8},{1,9},{2,10},{3,11},{4,12},{5,13},{6,14},{7,15},{8,0},{9,1},... | collective-permute-start | bytes 73736 | tf_op jit(solution)/shard_map/ppermute | solution.py:188
  12.6 42.3 %copy-start.5 = (bf16[8,2048]{1,0:T(8,128)(2,1)S(1)}, bf16[8,2048]{1,0:T(8,128)(2,1)}, u32[]{:S(2)}) copy-start(bf16[8,2048]{1,0:T(8,128)(2,1)} %target.1) | copy-start | bytes 98308
  53.0 31.4 %collective-permute-start.1 = (bf16[1536,256]{1,0:T(8,128)(2,1)S(1)}, bf16[1536,256]{1,0:T(8,128)(2,1)S(1)}, u32[]{:S(2)}, u32[]{:S(2)}) collective-permute-start(bf16[1536,256]{1,0:T(8,128)(2,1)S(1)} %all_gather.3.near), channel_id=1, source_target_pairs={{0,16},{16,0},{32,48},{48,32},{64,80},{80,64},{96,112},{112,96},{1... | collective-permute-start | bytes 2359304 | tf_op jit(solution)/shard_map/ppermute | solution.py:205
  55.0 18.3 %copy-start.2 = (bf16[2048,128]{1,0:T(8,128)(2,1)S(1)}, bf16[2048,128]{1,0:T(8,128)(2,1)}, u32[]{:S(2)}) copy-start(bf16[2048,128]{1,0:T(8,128)(2,1)} %weight.2) | copy-start | bytes 1572868
  55.0 18.3 %copy-start.7 = (f32[2048]{0:T(1024)S(1)}, f32[2048]{0:T(1024)}, u32[]{:S(2)}) copy-start(f32[2048]{0:T(1024)} %param.12) | copy-start | bytes 24580
  73.3 0.7 copy-start.9
  89.2 10.1 %copy-start.3 = (bf16[128,2048]{1,0:T(8,128)(2,1)S(1)}, bf16[128,2048]{1,0:T(8,128)(2,1)}, u32[]{:S(2)}) copy-start(bf16[128,2048]{1,0:T(8,128)(2,1)} %weight.3) | copy-start | bytes 1572868

commit v2 on v1

--- a/solution.py
+++ b/solution.py
@@ -17,6 +17,7 @@
 STAT_ROWS = 16
 
 VMEM = pl.BlockSpec(memory_space=pltpu.VMEM)
+HBM = pl.BlockSpec(memory_space=pltpu.HBM)
 
 
 def cost(flops, nbytes, transcendentals=0):
@@ -33,11 +34,31 @@
     )
 
 
-def key_value_kernel(source, gain, key_matrix, value_matrix, key_gain, own, other):
+def key_value_kernel(
+    source, gain, key_matrix, value_matrix, key_gain, own, other, key_part, value_part, arrived
+):
+    depth = key_part.shape[1]
+    parts = key_part.shape[0]
+    copies = [
+        pltpu.make_async_copy(
+            matrix.at[pl.ds(i * depth, depth), :], buffer.at[i], arrived.at[i, j]
+        )
+        for i in range(parts)
+        for j, (matrix, buffer) in enumerate(
+            ((key_matrix, key_part), (value_matrix, value_part))
+        )
+    ]
+    for c in copies:
+        c.start()
     second = lax.axis_index("tp") >= GROUP
     rows = normed(source[...].astype(jnp.float32), gain[...]).astype(jnp.bfloat16)
-    raw = jnp.dot(rows, key_matrix[...], preferred_element_type=jnp.float32)
-    values = jnp.dot(rows, value_matrix[...], preferred_element_type=jnp.float32)
+    raw, values = 0.0, 0.0
+    for i in range(parts):
+        copies[2 * i].wait()
+        copies[2 * i + 1].wait()
+        part = rows[:, i * depth : (i + 1) * depth]
+        raw += jnp.dot(part, key_part[i], preferred_element_type=jnp.float32)
+        values += jnp.dot(part, value_part[i], preferred_element_type=jnp.float32)
     values = values.astype(jnp.bfloat16)
     heads = []
     for h in range(KEY_VALUE_HEADS):
@@ -98,16 +119,20 @@
                 kv[:, HEAD_SIZE:],
                 preferred_element_type=jnp.float32,
             )
-        for i in range(per_tile):
-            at = slice(i * HEAD_SIZE, (i + 1) * HEAD_SIZE)
-            head = tile * per_tile + i
-            out[head, :HEAD_SIZE, :] = weighted[at].astype(jnp.bfloat16)
-            stats = in_three(as_row(peak[at])) + in_three(as_row(total[at]))
+        for odd in range(2):
+            def picked(column):
+                return jnp.concatenate(
+                    [column[i : i + 8] for i in range(8 * odd, rows, 16)], axis=0
+                )
+
+            to = tile * 2 + odd
+            out[to, :HEAD_SIZE, :] = picked(weighted).astype(jnp.bfloat16)
+            stats = in_three(as_row(picked(peak))) + in_three(as_row(picked(total)))
             empty = jnp.zeros((STAT_ROWS - len(stats), HEAD_SIZE), jnp.bfloat16)
-            out[head, HEAD_SIZE:, :] = jnp.concatenate(stats + [empty], axis=0)
-
-
-def output_kernel(partials, weight, out):
+            out[to, HEAD_SIZE:, :] = jnp.concatenate(stats + [empty], axis=0)
+
+
+def output_kernel(partials, own_weight, pair_weight, out):
     at_row = lax.broadcasted_iota(jnp.int32, (HEAD_SIZE, HEAD_SIZE), 0)
     at_lane = lax.broadcasted_iota(jnp.int32, (HEAD_SIZE, HEAD_SIZE), 1)
     eye = (at_row == at_lane).astype(jnp.float32)
@@ -127,8 +152,13 @@
     for j in range(GROUP):
         column = jnp.sum(eye * (fades[j] / total), axis=1, keepdims=True)
         attended += column * partials[j, :HEAD_SIZE, :].astype(jnp.float32)
+    attended = attended.astype(jnp.bfloat16)
+    even, odd = attended[: HEAD_SIZE // 2], attended[HEAD_SIZE // 2 :]
+    is_odd = lax.rem(lax.axis_index("tp"), 2) == 1
     update = jnp.dot(
-        attended.astype(jnp.bfloat16), weight[...], preferred_element_type=jnp.float32
+        jnp.where(is_odd, odd, even), own_weight[...], preferred_element_type=jnp.float32
+    ) + jnp.dot(
+        jnp.where(is_odd, even, odd), pair_weight[...], preferred_element_type=jnp.float32
     )
     out[...] = update.astype(jnp.bfloat16).reshape(out.shape)
 
@@ -140,14 +170,15 @@
     out[...] = (target[...].astype(jnp.float32) + update).astype(jnp.bfloat16)
 
 
-def call(kernel, outs, estimate, count):
+def call(kernel, outs, estimate, specs, scratch=(), vmem=48 * 1024 * 1024):
     return pl.pallas_call(
         kernel,
         out_shape=outs,
-        in_specs=[VMEM] * count,
+        in_specs=specs,
+        scratch_shapes=list(scratch),
         out_specs=jax.tree.map(lambda _: VMEM, outs),
         cost_estimate=estimate,
-        compiler_params=pltpu.CompilerParams(vmem_limit_bytes=48 * 1024 * 1024),
+        compiler_params=pltpu.CompilerParams(vmem_limit_bytes=vmem),
     )
 
 
@@ -174,27 +205,28 @@
     block = own_rows * tp
     source_rows = source.shape[0]
     halves = [[i + h * GROUP for i in range(GROUP)] for h in range(KEY_VALUE_HEADS)]
-    along_z = [[core + 2 * z for z in range(sp // 2)] for core in range(2)]
-
-    everyone = lax.all_to_all(
-        jnp.broadcast_to(target, (tp, own_rows, width)), "tp", 0, 0, tiled=True
-    ).reshape(block, width)
+    parities = [[e + 2 * i for i in range(tp // 2)] for e in range(2)]
+    along_z = [[2 * z + (z + core) % 2 for z in range(sp // 2)] for core in range(2)]
+    side = math.isqrt(tp)
+    opposite = [(i, (side - 1 - i // side) * side + i % side) for i in range(tp)]
+    depth = width // 4
+
     own, other = call(
         key_value_kernel,
         (bf16(source_rows, 2 * HEAD_SIZE), bf16(source_rows, 2 * HEAD_SIZE)),
         cost(2 * source_rows * width * 512, 2400000),
-        5,
+        [VMEM, VMEM, HBM, HBM, VMEM],
+        (
+            pltpu.VMEM((4, depth, 2 * HEAD_SIZE), jnp.bfloat16),
+            pltpu.VMEM((4, depth, 2 * HEAD_SIZE), jnp.bfloat16),
+            pltpu.SemaphoreType.DMA((4, 2)),
+        ),
+        vmem=67043328,
     )(source, source_gain.reshape(1, width), key_matrix, value_matrix, key_gain)
-    received = lax.ppermute(other, "tp", [(i, i ^ GROUP) for i in range(tp)])
-    copies = call(
-        query_kernel,
-        bf16(GROUP, block, HEAD_SIZE),
-        cost(2 * block * width * HEAD_SIZE, 1400000),
-        4,
-    )(everyone, target_gain.reshape(1, width), query_weight, query_gain)
-    all_queries = lax.all_to_all(
-        copies, "tp", 0, 0, tiled=True, axis_index_groups=halves
-    )
+    received = lax.ppermute(other, "tp", opposite)
+    everyone = lax.all_to_all(
+        jnp.broadcast_to(target, (tp, own_rows, width)), "tp", 0, 0, tiled=True
+    ).reshape(block, width)
     near = lax.all_gather(
         jnp.concatenate([own, received], axis=0),
         "sp",
@@ -202,24 +234,37 @@
         tiled=True,
         axis_index_groups=along_z,
     )
+    copies = call(
+        query_kernel,
+        bf16(GROUP, block, HEAD_SIZE),
+        cost(2 * block * width * HEAD_SIZE, 1400000),
+        [VMEM] * 4,
+    )(everyone, target_gain.reshape(1, width), query_weight, query_gain)
+    all_queries = lax.all_to_all(
+        copies, "tp", 0, 0, tiled=True, axis_index_groups=halves
+    )
     far = lax.ppermute(near, "sp", [(i, i ^ 1) for i in range(sp)])
+    pair_weight = lax.ppermute(out_weight, "tp", [(i, i ^ 1) for i in range(tp)])
     keys = 2 * near.shape[0]
     partials = call(
         attention_kernel,
         bf16(GROUP, block + STAT_ROWS, HEAD_SIZE),
         cost(4 * GROUP * block * keys * HEAD_SIZE, 2500000, GROUP * block * keys),
-        3,
+        [VMEM] * 3,
     )(all_queries, near, far)
     mine = lax.all_to_all(partials, "tp", 0, 0, tiled=True, axis_index_groups=halves)
     update = call(
         output_kernel,
-        bf16(tp, own_rows, width),
-        cost(2 * block * width * HEAD_SIZE, 1400000),
-        2,
-    )(mine, out_weight)
-    parts = lax.all_to_all(update, "tp", 0, 0, tiled=True)
+        bf16(tp // 2, own_rows, width),
+        cost(2 * block * width * HEAD_SIZE, 1900000),
+        [VMEM] * 3,
+    )(mine, out_weight, pair_weight)
+    parts = lax.all_to_all(update, "tp", 0, 0, tiled=True, axis_index_groups=parities)
     return call(
-        final_kernel, bf16(own_rows, width), cost(tp * own_rows * width, 600000), 2
+        final_kernel,
+        bf16(own_rows, width),
+        cost(tp // 2 * own_rows * width, 300000),
+        [VMEM] * 2,
     )(target, parts)
 
 

time: 114 us -> 111 us (0.974)
  blocking collectives: 92 us -> 64 us
  starting transfers between devices: 7.01 us -> 18.9 us
  waiting for transfers between devices: 2.12 us -> 14 us
  local copies, waits for them, and re-layouts: 5.47 us -> 0.71 us
  Pallas kernels: 7.05 us -> 11.5 us
    all_to_all x3 -> x1, blocking collectives: 33.3 us -> 11.3 us  [body(): lax.all_to_all(update, 'tp', 0, 0, tiled=True, axis_index_groups=parities)]
    all_to_all x0 -> x2, waiting for transfers between devices: none -> 11.8 us  [the longest x1 6.29 us: body(): lax.all_to_all(partials, 'tp', 0, 0, tiled=True, axis_index_groups=halves)]
    all_to_all x0 -> x2, starting transfers between devices: none -> 8.8 us  [the longest x1 4.91 us: body(): lax.all_to_all(copies, 'tp', 0, 0, tiled=True, axis_index_groups=halves)]
    all_gather x1, blocking collectives: 40.4 us -> 35.1 us  [body(): lax.all_gather(jnp.concatenate([own, received], axis=0), 'sp', axis=0, ti...]
    unnamed x20 -> x10, local copies, waits for them, and re-layouts: 5.42 us -> 0.67 us
    pallas_call x1, Pallas kernels: 0.64 us -> 3.42 us  [body(): call(key_value_kernel, (bf16(source_rows, 2 * HEAD_SIZE), bf16(source_row...]
    ppermute x1 -> x2, starting transfers between devices: 5.1 us -> 6.94 us  [the longest x1 4.92 us: body(): received = lax.ppermute(other, 'tp', opposite)]
    ppermute x1, starting transfers between devices: 1.91 us -> 3.16 us  [body(): far = lax.ppermute(near, 'sp', [(i, i ^ 1) for i in range(sp)])]
  transfers between devices with their start and end apart: 2 -> 5, of which waited for: 1 -> 3; matrix products, arithmetic and copies ran while one was open for 0% -> 0% of each run, Pallas kernels for 0% -> 6%
where the time goes in v2:
time: 111 us; the launch traced here: 110 us
  blocking collectives  64 us (58%)
  starting transfers between devices  18.9 us (17%)
  waiting for transfers between devices  14 us (13%)
  Pallas kernels  11.5 us (10%)
    all_gather x1, blocking collectives, body(): lax.all_gather(jnp.concatenate([own, received], axis=0), 'sp', axis=0, ti...  35.1 us
    all_to_all x1, blocking collectives, body(): lax.all_to_all(jnp.broadcast_to(target, (tp, own_rows, width)), 'tp', 0,...  17.6 us
    all_to_all x1, blocking collectives, body(): lax.all_to_all(update, 'tp', 0, 0, tiled=True, axis_index_groups=parities)  11.3 us
    all_to_all x1, waiting for transfers between devices, body(): lax.all_to_all(partials, 'tp', 0, 0, tiled=True, axis_index_groups=halves)  6.29 us
    pallas_call x1, Pallas kernels, body(): call(attention_kernel, bf16(GROUP, block + STAT_ROWS, HEAD_SIZE), cost(4...  5.63 us
    all_to_all x1, waiting for transfers between devices, body(): lax.all_to_all(copies, 'tp', 0, 0, tiled=True, axis_index_groups=halves)  5.52 us
    ppermute x1, starting transfers between devices, body(): received = lax.ppermute(other, 'tp', opposite)  4.92 us
    all_to_all x1, starting transfers between devices, body(): lax.all_to_all(copies, 'tp', 0, 0, tiled=True, axis_index_groups=halves)  4.91 us
  transfers between devices with their start and end apart: 5, of which 3 were waited for; matrix products, arithmetic and copies ran while one was open for 0% of the time, Pallas kernels for 6%

profile of v2, /device:TPU:2, one launch (start us, length us, event | category | flops | bytes accessed | tf_op | source)
XLA Modules:
  0.0 109.9 jit_solution(8116587699822216967)
XLA Ops:
  0.0 3.4 %shard_map.101 = (bf16[48,256]{1,0:T(8,128)(2,1)}, bf16[48,256]{1,0:T(8,128)(2,1)}) custom-call(bf16[48,2048]{1,0:T(8,128)(2,1)} %source.1, f32[1,2048]{1,0:T(1,128)} %bitcast.5, bf16[2048,256]{1,0:T(8,128)(2,1)} %key_matrix.1, bf16[2048,256]{1,0:T(8,128)(2,1)} %value_matrix.1, f32[2,128]{1,0:T(2,128)} %key_gain.1), custom_call_target="tpu_custom_call" | custom-call | flops 100663296 | bytes 2400000 | tf_op jit(solution)/shard_map/pallas_call | solution.py:214
  3.4 4.9 %collective-permute-start = (bf16[48,256]{1,0:T(8,128)(2,1)}, bf16[48,256]{1,0:T(8,128)(2,1)S(1)}, u32[]{:S(2)}, u32[]{:S(2)}) collective-permute-start(bf16[48,256]{1,0:T(8,128)(2,1)} %get-tuple-element.8), channel_id=1, source_target_pairs={{0,12},{1,13},{2,14},{3,15},{4,8},{5,9},{6,10},{7,11},{8,4},{9,5},... | collective-permute-start | bytes 73736 | tf_op jit(solution)/shard_map/ppermute | solution.py:226
  8.4 2.2 %collective-permute-done = bf16[48,256]{1,0:T(8,128)(2,1)S(1)} collective-permute-done((bf16[48,256]{1,0:T(8,128)(2,1)}, bf16[48,256]{1,0:T(8,128)(2,1)S(1)}, u32[]{:S(2)}, u32[]{:S(2)}) %collective-permute-start) | collective-permute-done | bytes 24608 | tf_op jit(solution)/shard_map/ppermute | solution.py:226
  10.6 0.7 pad_maximum_fusion
  11.3 35.1 %all_gather.3.near = bf16[1536,256]{1,0:T(8,128)(2,1)S(1)} all-gather(bf16[96,256]{1,0:T(8,128)(2,1)S(1)} %pad_maximum_fusion), channel_id=1, replica_groups={{0,48,64,112,128,176,192,240,256,304,320,368,384,432,448,496},{16,32,80..., dimensions={0}, use_global_device_ids=true | all-gather | bytes 835584 | tf_op jit(solution)/shard_map/all_gather | solution.py:230
  46.4 3.2 %collective-permute-start.1 = (bf16[1536,256]{1,0:T(8,128)(2,1)S(1)}, bf16[1536,256]{1,0:T(8,128)(2,1)S(1)}, u32[]{:S(2)}, u32[]{:S(2)}) collective-permute-start(bf16[1536,256]{1,0:T(8,128)(2,1)S(1)} %all_gather.3.near), channel_id=1, source_target_pairs={{0,16},{16,0},{32,48},{48,32},{64,80},{80,64},{96,112},{112,96},{1... | collective-permute-start | bytes 2359304 | tf_op jit(solution)/shard_map/ppermute | solution.py:246
  49.6 0.0 copy-done.2
  49.6 0.0 copy-start
  49.6 0.0 copy-start.3
  49.7 17.6 %all_to_all.20 = bf16[16,8,2048]{2,1,0:T(8,128)(2,1)S(1)} all-to-all(bf16[16,8,2048]{2,1,0:T(8,128)(2,1)S(1)} %broadcast_in_dim.3), channel_id=1, replica_groups=mesh['sp'=32,'tp'=16] {'tp'}, dimensions={0} | all-to-all | bytes 1048576 | tf_op jit(solution)/shard_map/all_to_all | solution.py:227
  67.2 0.0 copy-done
  67.2 0.6 copy-done.4
  67.9 1.2 %shard_map.100 = bf16[8,128,128]{2,1,0:T(8,128)(2,1)} custom-call(bf16[128,2048]{1,0:T(8,128)(2,1)S(1)} %bitcast.3, f32[1,2048]{1,0:T(1,128)S(1)} %bitcast.4, bf16[2048,128]{1,0:T(8,128)(2,1)S(1)} %copy-done, f32[1,128]{1,0:T(1,128)S(1)} %copy-done.4), custom_call_target="tpu_custom_call" | custom-call | flops 67108864 | bytes 1400000 | tf_op jit(solution)/shard_map/pallas_call | solution.py:237
  69.1 4.9 %all-to-all-start.1 = ((bf16[8,128,128]{2,1,0:T(8,128)(2,1)}), bf16[8,128,128]{2,1,0:T(8,128)(2,1)S(1)}, u32[]{:S(2)}, u32[]{:S(2)}) async-start(bf16[8,128,128]{2,1,0:T(8,128)(2,1)} %shard_map.100), calls=%async_computation.1 | async-start | bytes 524288 | tf_op jit(solution)/shard_map/all_to_all | solution.py:243
  74.0 2.0 %collective-permute-start.2 = (bf16[128,2048]{1,0:T(8,128)(2,1)S(1)}, bf16[128,2048]{1,0:T(8,128)(2,1)S(1)}, u32[]{:S(2)}, u32[]{:S(2)}) collective-permute-start(bf16[128,2048]{1,0:T(8,128)(2,1)S(1)} %copy-done.1), channel_id=1, source_target_pairs={{0,1},{1,0},{2,3},{3,2},{4,5},{5,4},{6,7},{7,6},{8,9},{9,8},{10,11... | collective-permute-start | bytes 1572872 | tf_op jit(solution)/shard_map/ppermute | solution.py:247
  76.1 5.5 %all-to-all-done.1.queries = bf16[8,128,128]{2,1,0:T(8,128)(2,1)S(1)} async-done(((bf16[8,128,128]{2,1,0:T(8,128)(2,1)}), bf16[8,128,128]{2,1,0:T(8,128)(2,1)S(1)}, u32[]{:S(2)}, u32[]{:S(2)}) %all-to-all-start.1) | async-done | bytes 262176 | tf_op jit(solution)/shard_map/all_to_all | solution.py:243
  81.6 0.0 collective-permute-done.1.far
  81.6 5.6 %shard_map.102 = bf16[8,144,128]{2,1,0:T(8,128)(2,1)} custom-call(bf16[8,128,128]{2,1,0:T(8,128)(2,1)S(1)} %all-to-all-done.1.queries, bf16[1536,256]{1,0:T(8,128)(2,1)S(1)} %all_gather.3.near, bf16[1536,256]{1,0:T(8,128)(2,1)S(1)} %collective-permute-done.1.far), custom_call_target="tpu_custom_call" | custom-call | flops 1610612736 | bytes 2500000 | tf_op jit(solution)/shard_map/pallas_call | solution.py:249
  87.2 3.9 %all-to-all-start.2 = ((bf16[8,144,128]{2,1,0:T(8,128)(2,1)}), bf16[8,144,128]{2,1,0:T(8,128)(2,1)S(1)}, u32[]{:S(2)}, u32[]{:S(2)}) async-start(bf16[8,144,128]{2,1,0:T(8,128)(2,1)} %shard_map.102), calls=%async_computation.2 | async-start | bytes 589824 | tf_op jit(solution)/shard_map/all_to_all | solution.py:255
  91.1 0.0 collective-permute-done.2.pair_weight
  91.1 6.3 %all-to-all-done.2.partials = bf16[8,144,128]{2,1,0:T(8,128)(2,1)S(1)} async-done(((bf16[8,144,128]{2,1,0:T(8,128)(2,1)}), bf16[8,144,128]{2,1,0:T(8,128)(2,1)S(1)}, u32[]{:S(2)}, u32[]{:S(2)}) %all-to-all-start.2) | async-done | bytes 294944 | tf_op jit(solution)/shard_map/all_to_all | solution.py:255
  97.4 0.5 shard_map.103
  97.9 11.3 %all_to_all.21.parts = bf16[8,8,2048]{2,1,0:T(8,128)(2,1)S(1)} all-to-all(bf16[8,8,2048]{2,1,0:T(8,128)(2,1)S(1)} %shard_map.103), channel_id=1, replica_groups={{0,2,4,6,8,10,12,14},{1,3,5,7,9,11,13,15},{16,18,20,22,24,26,28,30},{17..., dimensions={0} | all-to-all | bytes 524288 | tf_op jit(solution)/shard_map/all_to_all | solution.py:262
  109.3 0.7 shard_map.104
  (6 shorter events, 0.1 us)
Async XLA Ops:
  3.4 7.1 %collective-permute-start = (bf16[48,256]{1,0:T(8,128)(2,1)}, bf16[48,256]{1,0:T(8,128)(2,1)S(1)}, u32[]{:S(2)}, u32[]{:S(2)}) collective-permute-start(bf16[48,256]{1,0:T(8,128)(2,1)} %get-tuple-element.8), channel_id=1, source_target_pairs={{0,12},{1,13},{2,14},{3,15},{4,8},{5,9},{6,10},{7,11},{8,4},{9,5},... | collective-permute-start | bytes 73736 | tf_op jit(solution)/shard_map/ppermute | solution.py:226
  11.3 38.3 %copy-start.2 = (bf16[8,2048]{1,0:T(8,128)(2,1)S(1)}, bf16[8,2048]{1,0:T(8,128)(2,1)}, u32[]{:S(2)}) copy-start(bf16[8,2048]{1,0:T(8,128)(2,1)} %target.1) | copy-start | bytes 98308
  46.4 35.2 %collective-permute-start.1 = (bf16[1536,256]{1,0:T(8,128)(2,1)S(1)}, bf16[1536,256]{1,0:T(8,128)(2,1)S(1)}, u32[]{:S(2)}, u32[]{:S(2)}) collective-permute-start(bf16[1536,256]{1,0:T(8,128)(2,1)S(1)} %all_gather.3.near), channel_id=1, source_target_pairs={{0,16},{16,0},{32,48},{48,32},{64,80},{80,64},{96,112},{112,96},{1... | collective-permute-start | bytes 2359304 | tf_op jit(solution)/shard_map/ppermute | solution.py:246
  49.6 17.6 %copy-start = (bf16[2048,128]{1,0:T(8,128)(2,1)S(1)}, bf16[2048,128]{1,0:T(8,128)(2,1)}, u32[]{:S(2)}) copy-start(bf16[2048,128]{1,0:T(8,128)(2,1)} %weight.1) | copy-start | bytes 1572868
  49.6 17.6 %copy-start.3 = (f32[2048]{0:T(1024)S(1)}, f32[2048]{0:T(1024)}, u32[]{:S(2)}) copy-start(f32[2048]{0:T(1024)} %param.12) | copy-start | bytes 24580
  67.2 0.7 copy-start.4
  69.1 4.9 %copy-start.1 = (bf16[128,2048]{1,0:T(8,128)(2,1)S(1)}, bf16[128,2048]{1,0:T(8,128)(2,1)}, u32[]{:S(2)}) copy-start(bf16[128,2048]{1,0:T(8,128)(2,1)} %own_weight.1) | copy-start | bytes 1572868
  69.1 12.5 %all-to-all-start.1 = ((bf16[8,128,128]{2,1,0:T(8,128)(2,1)}), bf16[8,128,128]{2,1,0:T(8,128)(2,1)S(1)}, u32[]{:S(2)}, u32[]{:S(2)}) async-start(bf16[8,128,128]{2,1,0:T(8,128)(2,1)} %shard_map.100), calls=%async_computation.1 | async-start | bytes 524288 | tf_op jit(solution)/shard_map/all_to_all | solution.py:243
  74.0 17.1 %collective-permute-start.2 = (bf16[128,2048]{1,0:T(8,128)(2,1)S(1)}, bf16[128,2048]{1,0:T(8,128)(2,1)S(1)}, u32[]{:S(2)}, u32[]{:S(2)}) collective-permute-start(bf16[128,2048]{1,0:T(8,128)(2,1)S(1)} %copy-done.1), channel_id=1, source_target_pairs={{0,1},{1,0},{2,3},{3,2},{4,5},{5,4},{6,7},{7,6},{8,9},{9,8},{10,11... | collective-permute-start | bytes 1572872 | tf_op jit(solution)/shard_map/ppermute | solution.py:247
  87.2 10.2 %all-to-all-start.2 = ((bf16[8,144,128]{2,1,0:T(8,128)(2,1)}), bf16[8,144,128]{2,1,0:T(8,128)(2,1)S(1)}, u32[]{:S(2)}, u32[]{:S(2)}) async-start(bf16[8,144,128]{2,1,0:T(8,128)(2,1)} %shard_map.102), calls=%async_computation.2 | async-start | bytes 589824 | tf_op jit(solution)/shard_map/all_to_all | solution.py:255

commit v3 on v2

--- a/solution.py
+++ b/solution.py
@@ -35,27 +35,65 @@
 
 
 def key_value_kernel(
-    source, gain, key_matrix, value_matrix, key_gain, own, other, key_part, value_part, arrived
+    target,
+    source,
+    gain,
+    key_matrix,
+    value_matrix,
+    key_gain,
+    own,
+    other,
+    target_copies,
+    target_here,
+    source_here,
+    gain_here,
+    key_gain_here,
+    key_part,
+    value_part,
+    arrived,
+    matrix_arrived,
+    left,
 ):
     depth = key_part.shape[1]
     parts = key_part.shape[0]
-    copies = [
+    inputs = [
+        pltpu.make_async_copy(a, b, arrived.at[i])
+        for i, (a, b) in enumerate(
+            (
+                (target, target_here),
+                (source, source_here),
+                (gain, gain_here),
+                (key_gain, key_gain_here),
+            )
+        )
+    ]
+    matrices = [
         pltpu.make_async_copy(
-            matrix.at[pl.ds(i * depth, depth), :], buffer.at[i], arrived.at[i, j]
+            matrix.at[pl.ds(i * depth, depth), :], buffer.at[i], matrix_arrived.at[i, j]
         )
         for i in range(parts)
         for j, (matrix, buffer) in enumerate(
             ((key_matrix, key_part), (value_matrix, value_part))
         )
     ]
-    for c in copies:
+    outputs = [
+        pltpu.make_async_copy(target_here, target_copies.at[i], left.at[i])
+        for i in range(target_copies.shape[0])
+    ]
+    for c in inputs + matrices:
+        c.start()
+    inputs[0].wait()
+    for c in outputs:
         c.start()
     second = lax.axis_index("tp") >= GROUP
-    rows = normed(source[...].astype(jnp.float32), gain[...]).astype(jnp.bfloat16)
+    for c in inputs[1:]:
+        c.wait()
+    rows = normed(source_here[...].astype(jnp.float32), gain_here[...])
+    rows = rows.astype(jnp.bfloat16)
     raw, values = 0.0, 0.0
     for i in range(parts):
-        copies[2 * i].wait()
-        copies[2 * i + 1].wait()
+        matrices[2 * i].wait()
+        matrices[2 * i + 1].wait()
         part = rows[:, i * depth : (i + 1) * depth]
         raw += jnp.dot(part, key_part[i], preferred_element_type=jnp.float32)
         values += jnp.dot(part, value_part[i], preferred_element_type=jnp.float32)
@@ -63,10 +101,12 @@
     heads = []
     for h in range(KEY_VALUE_HEADS):
         at = slice(h * HEAD_SIZE, (h + 1) * HEAD_SIZE)
-        keys = normed(raw[:, at], key_gain[h : h + 1, :]).astype(jnp.bfloat16)
+        keys = normed(raw[:, at], key_gain_here[h : h + 1, :]).astype(jnp.bfloat16)
         heads.append(jnp.concatenate([keys, values[:, at]], axis=1))
     own[...] = jnp.where(second, heads[1], heads[0])
     other[...] = jnp.where(second, heads[0], heads[1])
+    for c in outputs:
+        c.wait()
 
 
 def query_kernel(target, gain, weight, head_gain, copies):
@@ -85,44 +125,60 @@
     return [first, second, third]
 
 
-def attention_kernel(queries, near, far, out):
-    per_tile = 2
-    rows = per_tile * HEAD_SIZE
+TILE = 2 * HEAD_SIZE
+
+
+def scores_of(queries, kv, tile):
+    q = queries[tile * 2 : tile * 2 + 2].reshape(TILE, HEAD_SIZE)
+    return lax.dot_general(
+        q,
+        kv[:, :HEAD_SIZE],
+        (((1,), (1,)), ((), ())),
+        preferred_element_type=jnp.float32,
+    )
+
+
+def weighed(scores, peak, kv):
+    weights = jnp.exp2((scores - peak) * EXP2_SCALE)
+    return (
+        jnp.sum(weights, axis=-1, keepdims=True),
+        jnp.dot(
+            weights.astype(jnp.bfloat16),
+            kv[:, HEAD_SIZE:],
+            preferred_element_type=jnp.float32,
+        ),
+    )
+
+
+def near_kernel(queries, kv, peaks, totals, sums):
+    for tile in range(GROUP // 2):
+        scores = scores_of(queries, kv, tile)
+        peak = jnp.max(scores, axis=-1, keepdims=True)
+        total, weighted = weighed(scores, peak, kv)
+        peaks[tile] = jnp.broadcast_to(peak, (TILE, HEAD_SIZE))
+        totals[tile] = jnp.broadcast_to(total, (TILE, HEAD_SIZE))
+        sums[tile] = weighted
+
+
+def far_kernel(queries, kv, peaks, totals, sums, out):
     at_row = lax.broadcasted_iota(jnp.int32, (HEAD_SIZE, HEAD_SIZE), 0)
     at_lane = lax.broadcasted_iota(jnp.int32, (HEAD_SIZE, HEAD_SIZE), 1)
     eye = (at_row == at_lane).astype(jnp.float32)
 
-    def as_row(column):
-        return jnp.sum(eye * column, axis=0, keepdims=True)
-
-    for tile in range(GROUP // per_tile):
-        q = queries[tile * per_tile : (tile + 1) * per_tile].reshape(rows, HEAD_SIZE)
-        scores = [
-            lax.dot_general(
-                q,
-                kv[:, :HEAD_SIZE],
-                (((1,), (1,)), ((), ())),
-                preferred_element_type=jnp.float32,
-            )
-            for kv in (near, far)
-        ]
-        peak = jnp.maximum(
-            jnp.max(scores[0], axis=-1, keepdims=True),
-            jnp.max(scores[1], axis=-1, keepdims=True),
-        )
-        total, weighted = 0.0, 0.0
-        for kv, s in zip((near, far), scores):
-            weights = jnp.exp2((s - peak) * EXP2_SCALE)
-            total += jnp.sum(weights, axis=-1, keepdims=True)
-            weighted += jnp.dot(
-                weights.astype(jnp.bfloat16),
-                kv[:, HEAD_SIZE:],
-                preferred_element_type=jnp.float32,
-            )
+    def as_row(columns):
+        return jnp.sum(eye * columns, axis=0, keepdims=True)
+
+    for tile in range(GROUP // 2):
+        scores = scores_of(queries, kv, tile)
+        peak = jnp.maximum(peaks[tile], jnp.max(scores, axis=-1, keepdims=True))
+        fade = jnp.exp2((peaks[tile] - peak) * EXP2_SCALE)
+        total, weighted = weighed(scores, peak[:, :1], kv)
+        total = totals[tile] * fade + total
+        weighted = sums[tile] * fade + weighted
         for odd in range(2):
-            def picked(column):
+            def picked(columns):
                 return jnp.concatenate(
-                    [column[i : i + 8] for i in range(8 * odd, rows, 16)], axis=0
+                    [columns[i : i + 8] for i in range(8 * odd, TILE, 16)], axis=0
                 )
 
             to = tile * 2 + odd
@@ -170,13 +226,13 @@
     out[...] = (target[...].astype(jnp.float32) + update).astype(jnp.bfloat16)
 
 
-def call(kernel, outs, estimate, specs, scratch=(), vmem=48 * 1024 * 1024):
+def call(kernel, outs, estimate, specs, out_specs=None, scratch=(), vmem=48 * 1024 * 1024):
     return pl.pallas_call(
         kernel,
         out_shape=outs,
         in_specs=specs,
         scratch_shapes=list(scratch),
-        out_specs=jax.tree.map(lambda _: VMEM, outs),
+        out_specs=out_specs or jax.tree.map(lambda _: VMEM, outs),
         cost_estimate=estimate,
         compiler_params=pltpu.CompilerParams(vmem_limit_bytes=vmem),
     )
@@ -211,29 +267,33 @@
     opposite = [(i, (side - 1 - i // side) * side + i % side) for i in range(tp)]
     depth = width // 4
 
-    own, other = call(
+    own, other, target_copies = call(
         key_value_kernel,
-        (bf16(source_rows, 2 * HEAD_SIZE), bf16(source_rows, 2 * HEAD_SIZE)),
-        cost(2 * source_rows * width * 512, 2400000),
-        [VMEM, VMEM, HBM, HBM, VMEM],
         (
+            bf16(source_rows, 2 * HEAD_SIZE),
+            bf16(source_rows, 2 * HEAD_SIZE),
+            bf16(tp, own_rows, width),
+        ),
+        cost(2 * source_rows * width * 512, 3000000),
+        [HBM] * 6,
+        (VMEM, VMEM, HBM),
+        (
+            pltpu.VMEM((own_rows, width), jnp.bfloat16),
+            pltpu.VMEM((source_rows, width), jnp.bfloat16),
+            pltpu.VMEM((1, width), jnp.float32),
+            pltpu.VMEM((KEY_VALUE_HEADS, HEAD_SIZE), jnp.float32),
             pltpu.VMEM((4, depth, 2 * HEAD_SIZE), jnp.bfloat16),
             pltpu.VMEM((4, depth, 2 * HEAD_SIZE), jnp.bfloat16),
+            pltpu.SemaphoreType.DMA((4,)),
             pltpu.SemaphoreType.DMA((4, 2)),
+            pltpu.SemaphoreType.DMA((tp,)),
         ),
         vmem=67043328,
-    )(source, source_gain.reshape(1, width), key_matrix, value_matrix, key_gain)
+    )(target, source, source_gain.reshape(1, width), key_matrix, value_matrix, key_gain)
+    everyone = lax.all_to_all(target_copies, "tp", 0, 0, tiled=True)
+    everyone = everyone.reshape(block, width)
     received = lax.ppermute(other, "tp", opposite)
-    everyone = lax.all_to_all(
-        jnp.broadcast_to(target, (tp, own_rows, width)), "tp", 0, 0, tiled=True
-    ).reshape(block, width)
-    near = lax.all_gather(
-        jnp.concatenate([own, received], axis=0),
-        "sp",
-        axis=0,
-        tiled=True,
-        axis_index_groups=along_z,
-    )
+    pair_weight = lax.ppermute(out_weight, "tp", [(i, i ^ 1) for i in range(tp)])
     copies = call(
         query_kernel,
         bf16(GROUP, block, HEAD_SIZE),
@@ -243,15 +303,23 @@
     all_queries = lax.all_to_all(
         copies, "tp", 0, 0, tiled=True, axis_index_groups=halves
     )
+    near = lax.all_gather(
+        jnp.concatenate([own, received], axis=0),
+        "sp",
+        axis=0,
+        tiled=True,
+        axis_index_groups=along_z,
+    )
     far = lax.ppermute(near, "sp", [(i, i ^ 1) for i in range(sp)])
-    pair_weight = lax.ppermute(out_weight, "tp", [(i, i ^ 1) for i in range(tp)])
-    keys = 2 * near.shape[0]
+    keys = near.shape[0]
+    work = cost(
+        4 * GROUP * block * keys * HEAD_SIZE, 2500000, GROUP * block * keys
+    )
+    carried = jax.ShapeDtypeStruct((GROUP // 2, TILE, HEAD_SIZE), jnp.float32)
+    state = call(near_kernel, (carried,) * 3, work, [VMEM] * 2)(all_queries, near)
     partials = call(
-        attention_kernel,
-        bf16(GROUP, block + STAT_ROWS, HEAD_SIZE),
-        cost(4 * GROUP * block * keys * HEAD_SIZE, 2500000, GROUP * block * keys),
-        [VMEM] * 3,
-    )(all_queries, near, far)
+        far_kernel, bf16(GROUP, block + STAT_ROWS, HEAD_SIZE), work, [VMEM] * 5
+    )(all_queries, far, *state)
     mine = lax.all_to_all(partials, "tp", 0, 0, tiled=True, axis_index_groups=halves)
     update = call(
         output_kernel,

time: 111 us -> 97.8 us (0.88)
  blocking collectives: 64 us -> 45.7 us
  starting transfers between devices: 18.9 us -> 27.4 us
  waiting for transfers between devices: 14 us -> 11.2 us
    all_to_all x1 -> x0, blocking collectives: 17.6 us -> none  [body(): lax.all_to_all(jnp.broadcast_to(target, (tp, own_rows, width)), 'tp', 0,...]
    all_to_all x0 -> x1, starting transfers between devices: none -> 7.4 us  [body(): everyone = lax.all_to_all(target_copies, 'tp', 0, 0, tiled=True)]
    all_gather x1, blocking collectives: 35.1 us -> 32.7 us  [body(): lax.all_gather(jnp.concatenate([own, received], axis=0), 'sp', axis=0, ti...]
    ppermute x1, waiting for transfers between devices: 2.21 us -> 0.01 us  [body(): received = lax.ppermute(other, 'tp', opposite)]
    all_to_all x1, blocking collectives: 11.3 us -> 13 us  [body(): lax.all_to_all(update, 'tp', 0, 0, tiled=True, axis_index_groups=parities)]
    pallas_call x1 -> x2, Pallas kernels: 5.63 us -> 6.63 us  [the longest x1 3.96 us: body(): call(far_kernel, bf16(GROUP, block + STAT_ROWS, HEAD_SIZE), work, [VMEM]...]
  transfers between devices with their start and end apart: 5 -> 6, of which waited for: 3 -> 2; matrix products, arithmetic and copies ran while one was open for 0% -> 0% of each run, Pallas kernels for 6% -> 8%
where the time goes in v3:
time: 97.8 us; the launch traced here: 97.1 us
  blocking collectives  45.7 us (47%)
  starting transfers between devices  27.4 us (28%)
  Pallas kernels  12 us (12%)
  waiting for transfers between devices  11.2 us (11%)
    all_gather x1, blocking collectives, body(): lax.all_gather(jnp.concatenate([own, received], axis=0), 'sp', axis=0, ti...  32.7 us
    all_to_all x1, blocking collectives, body(): lax.all_to_all(update, 'tp', 0, 0, tiled=True, axis_index_groups=parities)  13 us
    all_to_all x1, starting transfers between devices, body(): everyone = lax.all_to_all(target_copies, 'tp', 0, 0, tiled=True)  7.4 us
    all_to_all x1, waiting for transfers between devices, body(): lax.all_to_all(partials, 'tp', 0, 0, tiled=True, axis_index_groups=halves)  6.29 us
    all_to_all x1, starting transfers between devices, body(): lax.all_to_all(copies, 'tp', 0, 0, tiled=True, axis_index_groups=halves)  5.83 us
    ppermute x1, starting transfers between devices, body(): received = lax.ppermute(other, 'tp', opposite)  4.92 us
    all_to_all x1, waiting for transfers between devices, body(): lax.all_to_all(copies, 'tp', 0, 0, tiled=True, axis_index_groups=halves)  4.91 us
    all_to_all x1, starting transfers between devices, body(): lax.all_to_all(partials, 'tp', 0, 0, tiled=True, axis_index_groups=halves)  4.19 us
  transfers between devices with their start and end apart: 6, of which 2 were waited for; matrix products, arithmetic and copies ran while one was open for 0% of the time, Pallas kernels for 8%

profile of v3, /device:TPU:2, one launch (start us, length us, event | category | flops | bytes accessed | tf_op | source)
XLA Modules:
  0.0 97.1 jit_solution(12999384247635613067)
XLA Ops:
  0.0 3.0 %shard_map.100 = (bf16[48,256]{1,0:T(8,128)(2,1)}, bf16[48,256]{1,0:T(8,128)(2,1)}, bf16[16,8,2048]{2,1,0:T(8,128)(2,1)}) custom-call(bf16[8,2048]{1,0:T(8,128)(2,1)} %target.3, bf16[48,2048]{1,0:T(8,128)(2,1)} %source.1, f32[1,2048]{1,0:T(1,128)} %bitcast.5, bf16[2048,256]{1,0:T(8,128)(2,1)} %key_matrix.1, bf16[2048,256]{1,0:T(8,128)(2,1)} %value_matrix.1, ...), custom_call_target="tpu_custom_call" | custom-call | flops 100663296 | bytes 3000000 | tf_op jit(solution)/shard_map/pallas_call | solution.py:270
  3.0 4.9 %collective-permute-start = (bf16[48,256]{1,0:T(8,128)(2,1)}, bf16[48,256]{1,0:T(8,128)(2,1)S(1)}, u32[]{:S(2)}, u32[]{:S(2)}) collective-permute-start(bf16[48,256]{1,0:T(8,128)(2,1)} %get-tuple-element.13), channel_id=1, source_target_pairs={{0,12},{1,13},{2,14},{3,15},{4,8},{5,9},{6,10},{7,11},{8,4},{9,5},... | collective-permute-start | bytes 73736 | tf_op jit(solution)/shard_map/ppermute | solution.py:295
  7.9 0.0 copy-start.5
  7.9 7.4 %all-to-all-start = ((bf16[16,8,2048]{2,1,0:T(8,128)(2,1)}), bf16[16,8,2048]{2,1,0:T(8,128)(2,1)S(1)}, u32[]{:S(2)}, u32[]{:S(2)}) async-start(bf16[16,8,2048]{2,1,0:T(8,128)(2,1)} %get-tuple-element.11), calls=%async_computation | async-start | bytes 1048576 | tf_op jit(solution)/shard_map/all_to_all | solution.py:293
  15.4 0.0 collective-permute-done
  15.4 0.0 copy-start.3
  15.4 32.7 %all_gather.3.kv = bf16[1536,256]{1,0:T(8,128)(2,1)S(1)} all-gather(bf16[96,256]{1,0:T(8,128)(2,1)S(1)} %pad_maximum_fusion), channel_id=1, replica_groups={{0,48,64,112,128,176,192,240,256,304,320,368,384,432,448,496},{16,32,80..., dimensions={0}, use_global_device_ids=true | all-gather | bytes 835584 | tf_op jit(solution)/shard_map/all_gather | solution.py:306
  48.1 3.1 %collective-permute-start.1 = (bf16[1536,256]{1,0:T(8,128)(2,1)S(1)}, bf16[1536,256]{1,0:T(8,128)(2,1)S(1)}, u32[]{:S(2)}, u32[]{:S(2)}) collective-permute-start(bf16[1536,256]{1,0:T(8,128)(2,1)S(1)} %all_gather.3.kv), channel_id=1, source_target_pairs={{0,16},{16,0},{32,48},{48,32},{64,80},{80,64},{96,112},{112,96},{1... | collective-permute-start | bytes 2359304 | tf_op jit(solution)/shard_map/ppermute | solution.py:313
  51.2 0.0 all-to-all-done
  51.2 0.0 copy-start.4
  51.2 0.6 copy-done.4
  51.9 1.2 %shard_map.101 = bf16[8,128,128]{2,1,0:T(8,128)(2,1)} custom-call(bf16[128,2048]{1,0:T(8,128)(2,1)S(1)} %bitcast.3, f32[1,2048]{1,0:T(1,128)S(1)} %bitcast.4, bf16[2048,128]{1,0:T(8,128)(2,1)S(1)} %copy-done, f32[1,128]{1,0:T(1,128)S(1)} %copy-done.4), custom_call_target="tpu_custom_call" | custom-call | flops 67108864 | bytes 1400000 | tf_op jit(solution)/shard_map/pallas_call | solution.py:297
  53.1 5.8 %all-to-all-start.1 = ((bf16[8,128,128]{2,1,0:T(8,128)(2,1)}), bf16[8,128,128]{2,1,0:T(8,128)(2,1)S(1)}, u32[]{:S(2)}, u32[]{:S(2)}) async-start(bf16[8,128,128]{2,1,0:T(8,128)(2,1)} %shard_map.101), calls=%async_computation.1 | async-start | bytes 524288 | tf_op jit(solution)/shard_map/all_to_all | solution.py:303
  58.9 1.9 %collective-permute-start.2 = (bf16[128,2048]{1,0:T(8,128)(2,1)S(1)}, bf16[128,2048]{1,0:T(8,128)(2,1)S(1)}, u32[]{:S(2)}, u32[]{:S(2)}) collective-permute-start(bf16[128,2048]{1,0:T(8,128)(2,1)S(1)} %copy-done.1), channel_id=1, source_target_pairs={{0,1},{1,0},{2,3},{3,2},{4,5},{5,4},{6,7},{7,6},{8,9},{9,8},{10,11... | collective-permute-start | bytes 1572872 | tf_op jit(solution)/shard_map/ppermute | solution.py:296
  60.9 4.9 %all-to-all-done.1.queries = bf16[8,128,128]{2,1,0:T(8,128)(2,1)S(1)} async-done(((bf16[8,128,128]{2,1,0:T(8,128)(2,1)}), bf16[8,128,128]{2,1,0:T(8,128)(2,1)S(1)}, u32[]{:S(2)}, u32[]{:S(2)}) %all-to-all-start.1) | async-done | bytes 262176 | tf_op jit(solution)/shard_map/all_to_all | solution.py:303
  65.8 2.7 %shard_map.102 = (f32[4,256,128]{2,1,0:T(8,128)S(1)}, f32[4,256,128]{2,1,0:T(8,128)S(1)}, f32[4,256,128]{2,1,0:T(8,128)S(1)}) custom-call(bf16[8,128,128]{2,1,0:T(8,128)(2,1)S(1)} %all-to-all-done.1.queries, bf16[1536,256]{1,0:T(8,128)(2,1)S(1)} %all_gather.3.kv), custom_call_target="tpu_custom_call" | custom-call | flops 805306368 | bytes 2500000 | tf_op jit(solution)/shard_map/pallas_call | solution.py:319
  68.5 0.0 collective-permute-done.1.kv
  68.5 4.0 %shard_map.103 = bf16[8,144,128]{2,1,0:T(8,128)(2,1)} custom-call(bf16[8,128,128]{2,1,0:T(8,128)(2,1)S(1)} %all-to-all-done.1.queries, bf16[1536,256]{1,0:T(8,128)(2,1)S(1)} %collective-permute-done.1.kv, f32[4,256,128]{2,1,0:T(8,128)S(1)} %get-tuple-element.14.peaks, f32[4,256,128]{2,1,0:T(8,128)S(1)} %get-tuple-element.15.totals, ...), custom_call_target="tpu_custom_call" | custom-call | flops 805306368 | bytes 2500000 | tf_op jit(solution)/shard_map/pallas_call | solution.py:320
  72.4 4.2 %all-to-all-start.2 = ((bf16[8,144,128]{2,1,0:T(8,128)(2,1)}), bf16[8,144,128]{2,1,0:T(8,128)(2,1)S(1)}, u32[]{:S(2)}, u32[]{:S(2)}) async-start(bf16[8,144,128]{2,1,0:T(8,128)(2,1)} %shard_map.103), calls=%async_computation.2 | async-start | bytes 589824 | tf_op jit(solution)/shard_map/all_to_all | solution.py:323
  76.6 6.3 %all-to-all-done.2.partials = bf16[8,144,128]{2,1,0:T(8,128)(2,1)S(1)} async-done(((bf16[8,144,128]{2,1,0:T(8,128)(2,1)}), bf16[8,144,128]{2,1,0:T(8,128)(2,1)S(1)}, u32[]{:S(2)}, u32[]{:S(2)}) %all-to-all-start.2) | async-done | bytes 294944 | tf_op jit(solution)/shard_map/all_to_all | solution.py:323
  82.9 0.5 shard_map.104
  83.4 0.0 copy-start.2
  83.4 13.0 %all_to_all.20.parts = bf16[8,8,2048]{2,1,0:T(8,128)(2,1)S(1)} all-to-all(bf16[8,8,2048]{2,1,0:T(8,128)(2,1)S(1)} %shard_map.104), channel_id=1, replica_groups={{0,2,4,6,8,10,12,14},{1,3,5,7,9,11,13,15},{16,18,20,22,24,26,28,30},{17..., dimensions={0} | all-to-all | bytes 524288 | tf_op jit(solution)/shard_map/all_to_all | solution.py:330
  96.5 0.7 shard_map.105
  (9 shorter events, 0.0 us)
Async XLA Ops:
  3.0 12.4 %collective-permute-start = (bf16[48,256]{1,0:T(8,128)(2,1)}, bf16[48,256]{1,0:T(8,128)(2,1)S(1)}, u32[]{:S(2)}, u32[]{:S(2)}) collective-permute-start(bf16[48,256]{1,0:T(8,128)(2,1)} %get-tuple-element.13), channel_id=1, source_target_pairs={{0,12},{1,13},{2,14},{3,15},{4,8},{5,9},{6,10},{7,11},{8,4},{9,5},... | collective-permute-start | bytes 73736 | tf_op jit(solution)/shard_map/ppermute | solution.py:295
  7.9 7.4 %copy-start.5 = (bf16[48,256]{1,0:T(8,128)(2,1)S(1)}, bf16[48,256]{1,0:T(8,128)(2,1)}, u32[]{:S(2)}) copy-start(bf16[48,256]{1,0:T(8,128)(2,1)} %get-tuple-element.12) | copy-start | bytes 73732
  7.9 43.3 %all-to-all-start = ((bf16[16,8,2048]{2,1,0:T(8,128)(2,1)}), bf16[16,8,2048]{2,1,0:T(8,128)(2,1)S(1)}, u32[]{:S(2)}, u32[]{:S(2)}) async-start(bf16[16,8,2048]{2,1,0:T(8,128)(2,1)} %get-tuple-element.11), calls=%async_computation | async-start | bytes 1048576 | tf_op jit(solution)/shard_map/all_to_all | solution.py:293
  15.3 35.9 %copy-start = (bf16[2048,128]{1,0:T(8,128)(2,1)S(1)}, bf16[2048,128]{1,0:T(8,128)(2,1)}, u32[]{:S(2)}) copy-start(bf16[2048,128]{1,0:T(8,128)(2,1)} %weight.1) | copy-start | bytes 1572868
  15.4 35.8 %copy-start.3 = (f32[2048]{0:T(1024)S(1)}, f32[2048]{0:T(1024)}, u32[]{:S(2)}) copy-start(f32[2048]{0:T(1024)} %param.12) | copy-start | bytes 24580
  48.1 20.4 %collective-permute-start.1 = (bf16[1536,256]{1,0:T(8,128)(2,1)S(1)}, bf16[1536,256]{1,0:T(8,128)(2,1)S(1)}, u32[]{:S(2)}, u32[]{:S(2)}) collective-permute-start(bf16[1536,256]{1,0:T(8,128)(2,1)S(1)} %all_gather.3.kv), channel_id=1, source_target_pairs={{0,16},{16,0},{32,48},{48,32},{64,80},{80,64},{96,112},{112,96},{1... | collective-permute-start | bytes 2359304 | tf_op jit(solution)/shard_map/ppermute | solution.py:313
  51.2 0.7 copy-start.4
  53.1 5.8 %copy-start.1 = (bf16[128,2048]{1,0:T(8,128)(2,1)S(1)}, bf16[128,2048]{1,0:T(8,128)(2,1)}, u32[]{:S(2)}) copy-start(bf16[128,2048]{1,0:T(8,128)(2,1)} %own_weight.1) | copy-start | bytes 1572868
  53.1 12.7 %all-to-all-start.1 = ((bf16[8,128,128]{2,1,0:T(8,128)(2,1)}), bf16[8,128,128]{2,1,0:T(8,128)(2,1)S(1)}, u32[]{:S(2)}, u32[]{:S(2)}) async-start(bf16[8,128,128]{2,1,0:T(8,128)(2,1)} %shard_map.101), calls=%async_computation.1 | async-start | bytes 524288 | tf_op jit(solution)/shard_map/all_to_all | solution.py:303
  58.9 17.7 %collective-permute-start.2 = (bf16[128,2048]{1,0:T(8,128)(2,1)S(1)}, bf16[128,2048]{1,0:T(8,128)(2,1)S(1)}, u32[]{:S(2)}, u32[]{:S(2)}) collective-permute-start(bf16[128,2048]{1,0:T(8,128)(2,1)S(1)} %copy-done.1), channel_id=1, source_target_pairs={{0,1},{1,0},{2,3},{3,2},{4,5},{5,4},{6,7},{7,6},{8,9},{9,8},{10,11... | collective-permute-start | bytes 1572872 | tf_op jit(solution)/shard_map/ppermute | solution.py:296
  72.4 10.5 %all-to-all-start.2 = ((bf16[8,144,128]{2,1,0:T(8,128)(2,1)}), bf16[8,144,128]{2,1,0:T(8,128)(2,1)S(1)}, u32[]{:S(2)}, u32[]{:S(2)}) async-start(bf16[8,144,128]{2,1,0:T(8,128)(2,1)} %shard_map.103), calls=%async_computation.2 | async-start | bytes 589824 | tf_op jit(solution)/shard_map/all_to_all | solution.py:323
  83.4 13.1 %copy-start.2 = (bf16[8,2048]{1,0:T(8,128)(2,1)S(1)}, bf16[8,2048]{1,0:T(8,128)(2,1)}, u32[]{:S(2)}) copy-start(bf16[8,2048]{1,0:T(8,128)(2,1)} %target.3) | copy-start | bytes 98308

commit v4 on v2

--- a/solution.py
+++ b/solution.py
@@ -35,27 +35,71 @@
 
 
 def key_value_kernel(
-    source, gain, key_matrix, value_matrix, key_gain, own, other, key_part, value_part, arrived
+    target,
+    source,
+    gain,
+    key_matrix,
+    value_matrix,
+    key_gain,
+    target_gain,
+    query_gain,
+    own,
+    other,
+    target_copies,
+    target_gain_here,
+    query_gain_here,
+    target_here,
+    source_here,
+    gain_here,
+    key_gain_here,
+    key_part,
+    value_part,
+    arrived,
+    matrix_arrived,
+    left,
 ):
     depth = key_part.shape[1]
     parts = key_part.shape[0]
-    copies = [
+    inputs = [
+        pltpu.make_async_copy(a, b, arrived.at[i])
+        for i, (a, b) in enumerate(
+            (
+                (target, target_here),
+                (source, source_here),
+                (gain, gain_here),
+                (key_gain, key_gain_here),
+                (target_gain, target_gain_here),
+                (query_gain, query_gain_here),
+            )
+        )
+    ]
+    matrices = [
         pltpu.make_async_copy(
-            matrix.at[pl.ds(i * depth, depth), :], buffer.at[i], arrived.at[i, j]
+            matrix.at[pl.ds(i * depth, depth), :], buffer.at[i], matrix_arrived.at[i, j]
         )
         for i in range(parts)
         for j, (matrix, buffer) in enumerate(
             ((key_matrix, key_part), (value_matrix, value_part))
         )
     ]
-    for c in copies:
+    outputs = [
+        pltpu.make_async_copy(target_here, target_copies.at[i], left.at[i])
+        for i in range(target_copies.shape[0])
+    ]
+    for c in inputs + matrices:
+        c.start()
+    inputs[0].wait()
+    for c in outputs:
         c.start()
     second = lax.axis_index("tp") >= GROUP
-    rows = normed(source[...].astype(jnp.float32), gain[...]).astype(jnp.bfloat16)
+    for c in inputs[1:]:
+        c.wait()
+    rows = normed(source_here[...].astype(jnp.float32), gain_here[...])
+    rows = rows.astype(jnp.bfloat16)
     raw, values = 0.0, 0.0
     for i in range(parts):
-        copies[2 * i].wait()
-        copies[2 * i + 1].wait()
+        matrices[2 * i].wait()
+        matrices[2 * i + 1].wait()
         part = rows[:, i * depth : (i + 1) * depth]
         raw += jnp.dot(part, key_part[i], preferred_element_type=jnp.float32)
         values += jnp.dot(part, value_part[i], preferred_element_type=jnp.float32)
@@ -63,10 +107,12 @@
     heads = []
     for h in range(KEY_VALUE_HEADS):
         at = slice(h * HEAD_SIZE, (h + 1) * HEAD_SIZE)
-        keys = normed(raw[:, at], key_gain[h : h + 1, :]).astype(jnp.bfloat16)
+        keys = normed(raw[:, at], key_gain_here[h : h + 1, :]).astype(jnp.bfloat16)
         heads.append(jnp.concatenate([keys, values[:, at]], axis=1))
     own[...] = jnp.where(second, heads[1], heads[0])
     other[...] = jnp.where(second, heads[0], heads[1])
+    for c in outputs:
+        c.wait()
 
 
 def query_kernel(target, gain, weight, head_gain, copies):
@@ -170,13 +216,13 @@
     out[...] = (target[...].astype(jnp.float32) + update).astype(jnp.bfloat16)
 
 
-def call(kernel, outs, estimate, specs, scratch=(), vmem=48 * 1024 * 1024):
+def call(kernel, outs, estimate, specs, out_specs=None, scratch=(), vmem=48 * 1024 * 1024):
     return pl.pallas_call(
         kernel,
         out_shape=outs,
         in_specs=specs,
         scratch_shapes=list(scratch),
-        out_specs=jax.tree.map(lambda _: VMEM, outs),
+        out_specs=out_specs or jax.tree.map(lambda _: VMEM, outs),
         cost_estimate=estimate,
         compiler_params=pltpu.CompilerParams(vmem_limit_bytes=vmem),
     )
@@ -211,22 +257,49 @@
     opposite = [(i, (side - 1 - i // side) * side + i % side) for i in range(tp)]
     depth = width // 4
 
-    own, other = call(
+    pieces = (source_rows, 2 * HEAD_SIZE)
+    own, other, target_copies, target_gain_here, query_gain_here = call(
         key_value_kernel,
-        (bf16(source_rows, 2 * HEAD_SIZE), bf16(source_rows, 2 * HEAD_SIZE)),
-        cost(2 * source_rows * width * 512, 2400000),
-        [VMEM, VMEM, HBM, HBM, VMEM],
         (
+            pltpu.VMEM(pieces, jnp.bfloat16),
+            pltpu.VMEM(pieces, jnp.bfloat16),
+            pltpu.HBM((tp, own_rows, width), jnp.bfloat16),
+            pltpu.VMEM((1, width), jnp.float32),
+            pltpu.VMEM((1, HEAD_SIZE), jnp.float32),
+        ),
+        cost(2 * source_rows * width * 512, 3000000),
+        [HBM] * 8,
+        (VMEM, VMEM, HBM, VMEM, VMEM),
+        (
+            pltpu.VMEM((own_rows, width), jnp.bfloat16),
+            pltpu.VMEM((source_rows, width), jnp.bfloat16),
+            pltpu.VMEM((1, width), jnp.float32),
+            pltpu.VMEM((KEY_VALUE_HEADS, HEAD_SIZE), jnp.float32),
             pltpu.VMEM((4, depth, 2 * HEAD_SIZE), jnp.bfloat16),
             pltpu.VMEM((4, depth, 2 * HEAD_SIZE), jnp.bfloat16),
+            pltpu.SemaphoreType.DMA((6,)),
             pltpu.SemaphoreType.DMA((4, 2)),
+            pltpu.SemaphoreType.DMA((tp,)),
         ),
-        vmem=67043328,
-    )(source, source_gain.reshape(1, width), key_matrix, value_matrix, key_gain)
+        vmem=16 * 1024 * 1024,
+    )(
+        *(
+            pltpu.with_memory_space_constraint(x, pltpu.HBM)
+            for x in (
+                target,
+                source,
+                source_gain.reshape(1, width),
+                key_matrix,
+                value_matrix,
+                key_gain,
+                target_gain.reshape(1, width),
+                query_gain,
+            )
+        )
+    )
     received = lax.ppermute(other, "tp", opposite)
-    everyone = lax.all_to_all(
-        jnp.broadcast_to(target, (tp, own_rows, width)), "tp", 0, 0, tiled=True
-    ).reshape(block, width)
+    everyone = lax.all_to_all(target_copies, "tp", 0, 0, tiled=True)
+    everyone = everyone.reshape(block, width)
     near = lax.all_gather(
         jnp.concatenate([own, received], axis=0),
         "sp",
@@ -239,7 +312,7 @@
         bf16(GROUP, block, HEAD_SIZE),
         cost(2 * block * width * HEAD_SIZE, 1400000),
         [VMEM] * 4,
-    )(everyone, target_gain.reshape(1, width), query_weight, query_gain)
+    )(everyone, target_gain_here, query_weight, query_gain_here)
     all_queries = lax.all_to_all(
         copies, "tp", 0, 0, tiled=True, axis_index_groups=halves
     )

time: 111 us -> 108 us (0.973)
  no operation moved by 1% of the time
where the time goes in v4:
time: 108 us; the launch traced here: 107 us
  blocking collectives  63.9 us (59%)
  starting transfers between devices  19 us (18%)
  waiting for transfers between devices  13.8 us (13%)
  Pallas kernels  10.4 us (10%)
    all_gather x1, blocking collectives, body(): lax.all_gather(jnp.concatenate([own, received], axis=0), 'sp', axis=0, ti...  35 us
    all_to_all x1, blocking collectives, body(): everyone = lax.all_to_all(target_copies, 'tp', 0, 0, tiled=True)  17.6 us
    all_to_all x1, blocking collectives, body(): lax.all_to_all(update, 'tp', 0, 0, tiled=True, axis_index_groups=parities)  11.3 us
    all_to_all x1, waiting for transfers between devices, body(): lax.all_to_all(partials, 'tp', 0, 0, tiled=True, axis_index_groups=halves)  6.29 us
    pallas_call x1, Pallas kernels, body(): call(attention_kernel, bf16(GROUP, block + STAT_ROWS, HEAD_SIZE), cost(4...  5.61 us
    all_to_all x1, waiting for transfers between devices, body(): lax.all_to_all(copies, 'tp', 0, 0, tiled=True, axis_index_groups=halves)  5.52 us
    ppermute x1, starting transfers between devices, body(): received = lax.ppermute(other, 'tp', opposite)  5.05 us
    all_to_all x1, starting transfers between devices, body(): lax.all_to_all(copies, 'tp', 0, 0, tiled=True, axis_index_groups=halves)  4.91 us
  transfers between devices with their start and end apart: 5, of which 3 were waited for; matrix products, arithmetic and copies ran while one was open for 0% of the time, Pallas kernels for 6%

profile of v4, /device:TPU:2, one launch (start us, length us, event | category | flops | bytes accessed | tf_op | source)
XLA Modules:
  0.0 107.2 jit_solution(1058870475622431177)
XLA Ops:
  0.0 2.4 %shard_map.100 = (bf16[48,256]{1,0:T(8,128)(2,1)S(1)}, bf16[48,256]{1,0:T(8,128)(2,1)S(1)}, bf16[16,8,2048]{2,1,0:T(8,128)(2,1)}, f32[1,2048]{1,0:T(1,128)S(1)}, f32[1,128]{1,0:T(1,128)S(1)}) custom-call(bf16[8,2048]{1,0:T(8,128)(2,1)} %target.3, bf16[48,2048]{1,0:T(8,128)(2,1)} %source.1, f32[1,2048]{1,0:T(1,128)} %bitcast.4, bf16[2048,256]{1,0:T(8,128)(2,1)} %key_matrix.1, ...), custom_call_target="tpu_custom_call" | custom-call | flops 100663296 | bytes 3000000 | tf_op jit(solution)/shard_map/pallas_call | solution.py:261
  2.4 0.0 copy-start.3
  2.4 5.1 %collective-permute-start = (bf16[48,256]{1,0:T(8,128)(2,1)S(1)}, bf16[48,256]{1,0:T(8,128)(2,1)S(1)}, u32[]{:S(2)}, u32[]{:S(2)}) collective-permute-start(bf16[48,256]{1,0:T(8,128)(2,1)S(1)} %get-tuple-element.14), channel_id=1, source_target_pairs={{0,12},{1,13},{2,14},{3,15},{4,8},{5,9},{6,10},{7,11},{8,4},{9,5},... | collective-permute-start | bytes 73736 | tf_op jit(solution)/shard_map/ppermute | solution.py:300
  7.4 2.0 %collective-permute-done = bf16[48,256]{1,0:T(8,128)(2,1)S(1)} collective-permute-done((bf16[48,256]{1,0:T(8,128)(2,1)S(1)}, bf16[48,256]{1,0:T(8,128)(2,1)S(1)}, u32[]{:S(2)}, u32[]{:S(2)}) %collective-permute-start) | collective-permute-done | bytes 24608 | tf_op jit(solution)/shard_map/ppermute | solution.py:300
  9.5 35.0 %all_gather.3.near = bf16[1536,256]{1,0:T(8,128)(2,1)S(1)} all-gather(bf16[96,256]{1,0:T(8,128)(2,1)S(1)} %pad_maximum_fusion), channel_id=1, replica_groups={{0,48,64,112,128,176,192,240,256,304,320,368,384,432,448,496},{16,32,80..., dimensions={0}, use_global_device_ids=true | all-gather | bytes 835584 | tf_op jit(solution)/shard_map/all_gather | solution.py:303
  44.4 3.2 %collective-permute-start.1 = (bf16[1536,256]{1,0:T(8,128)(2,1)S(1)}, bf16[1536,256]{1,0:T(8,128)(2,1)S(1)}, u32[]{:S(2)}, u32[]{:S(2)}) collective-permute-start(bf16[1536,256]{1,0:T(8,128)(2,1)S(1)} %all_gather.3.near), channel_id=1, source_target_pairs={{0,16},{16,0},{32,48},{48,32},{64,80},{80,64},{96,112},{112,96},{1... | collective-permute-start | bytes 2359304 | tf_op jit(solution)/shard_map/ppermute | solution.py:319
  47.6 0.0 copy-done.3
  47.6 0.0 copy-start
  47.6 17.6 %all_to_all.20 = bf16[16,8,2048]{2,1,0:T(8,128)(2,1)S(1)} all-to-all(bf16[16,8,2048]{2,1,0:T(8,128)(2,1)S(1)} %copy-done.3), channel_id=1, replica_groups=mesh['sp'=32,'tp'=16] {'tp'}, dimensions={0} | all-to-all | bytes 1048576 | tf_op jit(solution)/shard_map/all_to_all | solution.py:301
  65.2 0.0 copy-done
  65.2 1.2 %shard_map.101 = bf16[8,128,128]{2,1,0:T(8,128)(2,1)} custom-call(bf16[128,2048]{1,0:T(8,128)(2,1)S(1)} %bitcast.3, f32[1,2048]{1,0:T(1,128)S(1)} %get-tuple-element.11.gain, bf16[2048,128]{1,0:T(8,128)(2,1)S(1)} %copy-done, f32[1,128]{1,0:T(1,128)S(1)} %get-tuple-element.12.head_gain), custom_call_target="tpu_custom_call" | custom-call | flops 67108864 | bytes 1400000 | tf_op jit(solution)/shard_map/pallas_call | solution.py:310
  66.4 4.9 %all-to-all-start.1 = ((bf16[8,128,128]{2,1,0:T(8,128)(2,1)}), bf16[8,128,128]{2,1,0:T(8,128)(2,1)S(1)}, u32[]{:S(2)}, u32[]{:S(2)}) async-start(bf16[8,128,128]{2,1,0:T(8,128)(2,1)} %shard_map.101), calls=%async_computation.1 | async-start | bytes 524288 | tf_op jit(solution)/shard_map/all_to_all | solution.py:316
  71.3 0.0 copy-done.1
  71.3 2.0 %collective-permute-start.2 = (bf16[128,2048]{1,0:T(8,128)(2,1)S(1)}, bf16[128,2048]{1,0:T(8,128)(2,1)S(1)}, u32[]{:S(2)}, u32[]{:S(2)}) collective-permute-start(bf16[128,2048]{1,0:T(8,128)(2,1)S(1)} %copy-done.1), channel_id=1, source_target_pairs={{0,1},{1,0},{2,3},{3,2},{4,5},{5,4},{6,7},{7,6},{8,9},{9,8},{10,11... | collective-permute-start | bytes 1572872 | tf_op jit(solution)/shard_map/ppermute | solution.py:320
  73.4 5.5 %all-to-all-done.1.queries = bf16[8,128,128]{2,1,0:T(8,128)(2,1)S(1)} async-done(((bf16[8,128,128]{2,1,0:T(8,128)(2,1)}), bf16[8,128,128]{2,1,0:T(8,128)(2,1)S(1)}, u32[]{:S(2)}, u32[]{:S(2)}) %all-to-all-start.1) | async-done | bytes 262176 | tf_op jit(solution)/shard_map/all_to_all | solution.py:316
  78.9 0.0 collective-permute-done.1.far
  78.9 5.6 %shard_map.102 = bf16[8,144,128]{2,1,0:T(8,128)(2,1)} custom-call(bf16[8,128,128]{2,1,0:T(8,128)(2,1)S(1)} %all-to-all-done.1.queries, bf16[1536,256]{1,0:T(8,128)(2,1)S(1)} %all_gather.3.near, bf16[1536,256]{1,0:T(8,128)(2,1)S(1)} %collective-permute-done.1.far), custom_call_target="tpu_custom_call" | custom-call | flops 1610612736 | bytes 2500000 | tf_op jit(solution)/shard_map/pallas_call | solution.py:322
  84.5 3.9 %all-to-all-start.2 = ((bf16[8,144,128]{2,1,0:T(8,128)(2,1)}), bf16[8,144,128]{2,1,0:T(8,128)(2,1)S(1)}, u32[]{:S(2)}, u32[]{:S(2)}) async-start(bf16[8,144,128]{2,1,0:T(8,128)(2,1)} %shard_map.102), calls=%async_computation.2 | async-start | bytes 589824 | tf_op jit(solution)/shard_map/all_to_all | solution.py:328
  88.4 0.0 collective-permute-done.2.pair_weight
  88.4 6.3 %all-to-all-done.2.partials = bf16[8,144,128]{2,1,0:T(8,128)(2,1)S(1)} async-done(((bf16[8,144,128]{2,1,0:T(8,128)(2,1)}), bf16[8,144,128]{2,1,0:T(8,128)(2,1)S(1)}, u32[]{:S(2)}, u32[]{:S(2)}) %all-to-all-start.2) | async-done | bytes 294944 | tf_op jit(solution)/shard_map/all_to_all | solution.py:328
  94.7 0.5 shard_map.103
  95.2 0.0 copy-start.2
  95.2 11.3 %all_to_all.21.parts = bf16[8,8,2048]{2,1,0:T(8,128)(2,1)S(1)} all-to-all(bf16[8,8,2048]{2,1,0:T(8,128)(2,1)S(1)} %shard_map.103), channel_id=1, replica_groups={{0,2,4,6,8,10,12,14},{1,3,5,7,9,11,13,15},{16,18,20,22,24,26,28,30},{17..., dimensions={0} | all-to-all | bytes 524288 | tf_op jit(solution)/shard_map/all_to_all | solution.py:335
  106.5 0.7 shard_map.104
  (3 shorter events, 0.0 us)
Async XLA Ops:
  2.4 45.2 %copy-start.3 = (bf16[16,8,2048]{2,1,0:T(8,128)(2,1)S(1)}, bf16[16,8,2048]{2,1,0:T(8,128)(2,1)}, u32[]{:S(2)}) copy-start(bf16[16,8,2048]{2,1,0:T(8,128)(2,1)} %get-tuple-element.10) | copy-start | bytes 1572868
  2.4 7.1 %collective-permute-start = (bf16[48,256]{1,0:T(8,128)(2,1)S(1)}, bf16[48,256]{1,0:T(8,128)(2,1)S(1)}, u32[]{:S(2)}, u32[]{:S(2)}) collective-permute-start(bf16[48,256]{1,0:T(8,128)(2,1)S(1)} %get-tuple-element.14), channel_id=1, source_target_pairs={{0,12},{1,13},{2,14},{3,15},{4,8},{5,9},{6,10},{7,11},{8,4},{9,5},... | collective-permute-start | bytes 73736 | tf_op jit(solution)/shard_map/ppermute | solution.py:300
  44.4 34.5 %collective-permute-start.1 = (bf16[1536,256]{1,0:T(8,128)(2,1)S(1)}, bf16[1536,256]{1,0:T(8,128)(2,1)S(1)}, u32[]{:S(2)}, u32[]{:S(2)}) collective-permute-start(bf16[1536,256]{1,0:T(8,128)(2,1)S(1)} %all_gather.3.near), channel_id=1, source_target_pairs={{0,16},{16,0},{32,48},{48,32},{64,80},{80,64},{96,112},{112,96},{1... | collective-permute-start | bytes 2359304 | tf_op jit(solution)/shard_map/ppermute | solution.py:319
  47.6 17.6 %copy-start = (bf16[2048,128]{1,0:T(8,128)(2,1)S(1)}, bf16[2048,128]{1,0:T(8,128)(2,1)}, u32[]{:S(2)}) copy-start(bf16[2048,128]{1,0:T(8,128)(2,1)} %weight.1) | copy-start | bytes 1572868
  66.4 4.9 %copy-start.1 = (bf16[128,2048]{1,0:T(8,128)(2,1)S(1)}, bf16[128,2048]{1,0:T(8,128)(2,1)}, u32[]{:S(2)}) copy-start(bf16[128,2048]{1,0:T(8,128)(2,1)} %own_weight.1) | copy-start | bytes 1572868
  66.4 12.5 %all-to-all-start.1 = ((bf16[8,128,128]{2,1,0:T(8,128)(2,1)}), bf16[8,128,128]{2,1,0:T(8,128)(2,1)S(1)}, u32[]{:S(2)}, u32[]{:S(2)}) async-start(bf16[8,128,128]{2,1,0:T(8,128)(2,1)} %shard_map.101), calls=%async_computation.1 | async-start | bytes 524288 | tf_op jit(solution)/shard_map/all_to_all | solution.py:316
  71.3 17.1 %collective-permute-start.2 = (bf16[128,2048]{1,0:T(8,128)(2,1)S(1)}, bf16[128,2048]{1,0:T(8,128)(2,1)S(1)}, u32[]{:S(2)}, u32[]{:S(2)}) collective-permute-start(bf16[128,2048]{1,0:T(8,128)(2,1)S(1)} %copy-done.1), channel_id=1, source_target_pairs={{0,1},{1,0},{2,3},{3,2},{4,5},{5,4},{6,7},{7,6},{8,9},{9,8},{10,11... | collective-permute-start | bytes 1572872 | tf_op jit(solution)/shard_map/ppermute | solution.py:320
  84.5 10.2 %all-to-all-start.2 = ((bf16[8,144,128]{2,1,0:T(8,128)(2,1)}), bf16[8,144,128]{2,1,0:T(8,128)(2,1)S(1)}, u32[]{:S(2)}, u32[]{:S(2)}) async-start(bf16[8,144,128]{2,1,0:T(8,128)(2,1)} %shard_map.102), calls=%async_computation.2 | async-start | bytes 589824 | tf_op jit(solution)/shard_map/all_to_all | solution.py:328
  95.2 11.3 %copy-start.2 = (bf16[8,2048]{1,0:T(8,128)(2,1)S(1)}, bf16[8,2048]{1,0:T(8,128)(2,1)}, u32[]{:S(2)}) copy-start(bf16[8,2048]{1,0:T(8,128)(2,1)} %target.3) | copy-start | bytes 98308

commit v5 on v4

--- a/solution.py
+++ b/solution.py
@@ -115,12 +115,17 @@
         c.wait()
 
 
-def query_kernel(target, gain, weight, head_gain, copies):
+def query_kernel(target, gain, weight, head_gain, copies, here, left):
     rows = normed(target[...].astype(jnp.float32), gain[...]).astype(jnp.bfloat16)
     raw = jnp.dot(rows, weight[...], preferred_element_type=jnp.float32)
-    queries = normed(raw, head_gain[...]).astype(jnp.bfloat16)
-    for i in range(GROUP):
-        copies[i] = queries
+    here[...] = normed(raw, head_gain[...]).astype(jnp.bfloat16)
+    outputs = [
+        pltpu.make_async_copy(here, copies.at[i], left.at[i]) for i in range(GROUP)
+    ]
+    for c in outputs:
+        c.start()
+    for c in outputs:
+        c.wait()
 
 
 def in_three(x):
@@ -131,9 +136,8 @@
     return [first, second, third]
 
 
-def attention_kernel(queries, near, far, out):
-    per_tile = 2
-    rows = per_tile * HEAD_SIZE
+def attention_kernel(queries, near, far, out, here, left):
+    rows = 2 * HEAD_SIZE
     at_row = lax.broadcasted_iota(jnp.int32, (HEAD_SIZE, HEAD_SIZE), 0)
     at_lane = lax.broadcasted_iota(jnp.int32, (HEAD_SIZE, HEAD_SIZE), 1)
     eye = (at_row == at_lane).astype(jnp.float32)
@@ -141,8 +145,11 @@
     def as_row(column):
         return jnp.sum(eye * column, axis=0, keepdims=True)
 
-    for tile in range(GROUP // per_tile):
-        q = queries[tile * per_tile : (tile + 1) * per_tile].reshape(rows, HEAD_SIZE)
+    outputs = []
+    for head in range(GROUP):
+        if head % 4 >= 2:
+            continue
+        q = jnp.concatenate([queries[head], queries[head + 2]], axis=0)
         scores = [
             lax.dot_general(
                 q,
@@ -165,17 +172,21 @@
                 kv[:, HEAD_SIZE:],
                 preferred_element_type=jnp.float32,
             )
-        for odd in range(2):
+        for side in range(2):
             def picked(column):
                 return jnp.concatenate(
-                    [column[i : i + 8] for i in range(8 * odd, rows, 16)], axis=0
+                    [column[i : i + 16] for i in range(16 * side, rows, 32)], axis=0
                 )
 
-            to = tile * 2 + odd
-            out[to, :HEAD_SIZE, :] = picked(weighted).astype(jnp.bfloat16)
+            to = head + 2 * side
+            here[to, :HEAD_SIZE, :] = picked(weighted).astype(jnp.bfloat16)
             stats = in_three(as_row(picked(peak))) + in_three(as_row(picked(total)))
             empty = jnp.zeros((STAT_ROWS - len(stats), HEAD_SIZE), jnp.bfloat16)
-            out[to, HEAD_SIZE:, :] = jnp.concatenate(stats + [empty], axis=0)
+            here[to, HEAD_SIZE:, :] = jnp.concatenate(stats + [empty], axis=0)
+            outputs.append(pltpu.make_async_copy(here.at[to], out.at[to], left.at[to]))
+            outputs[-1].start()
+    for c in outputs:
+        c.wait()
 
 
 def output_kernel(partials, own_weight, pair_weight, out):
@@ -199,12 +210,12 @@
         column = jnp.sum(eye * (fades[j] / total), axis=1, keepdims=True)
         attended += column * partials[j, :HEAD_SIZE, :].astype(jnp.float32)
     attended = attended.astype(jnp.bfloat16)
-    even, odd = attended[: HEAD_SIZE // 2], attended[HEAD_SIZE // 2 :]
-    is_odd = lax.rem(lax.axis_index("tp"), 2) == 1
+    low, high = attended[: HEAD_SIZE // 2], attended[HEAD_SIZE // 2 :]
+    is_high = lax.rem(lax.axis_index("tp"), 4) >= 2
     update = jnp.dot(
-        jnp.where(is_odd, odd, even), own_weight[...], preferred_element_type=jnp.float32
+        jnp.where(is_high, high, low), own_weight[...], preferred_element_type=jnp.float32
     ) + jnp.dot(
-        jnp.where(is_odd, even, odd), pair_weight[...], preferred_element_type=jnp.float32
+        jnp.where(is_high, low, high), pair_weight[...], preferred_element_type=jnp.float32
     )
     out[...] = update.astype(jnp.bfloat16).reshape(out.shape)
 
@@ -251,7 +262,7 @@
     block = own_rows * tp
     source_rows = source.shape[0]
     halves = [[i + h * GROUP for i in range(GROUP)] for h in range(KEY_VALUE_HEADS)]
-    parities = [[e + 2 * i for i in range(tp // 2)] for e in range(2)]
+    sides = [[i for i in range(tp) if i // 2 % 2 == e] for e in range(2)]
     along_z = [[2 * z + (z + core) % 2 for z in range(sp // 2)] for core in range(2)]
     side = math.isqrt(tp)
     opposite = [(i, (side - 1 - i // side) * side + i % side) for i in range(tp)]
@@ -309,21 +320,31 @@
     )
     copies = call(
         query_kernel,
-        bf16(GROUP, block, HEAD_SIZE),
+        pltpu.HBM((GROUP, block, HEAD_SIZE), jnp.bfloat16),
         cost(2 * block * width * HEAD_SIZE, 1400000),
         [VMEM] * 4,
+        HBM,
+        (
+            pltpu.VMEM((block, HEAD_SIZE), jnp.bfloat16),
+            pltpu.SemaphoreType.DMA((GROUP,)),
+        ),
     )(everyone, target_gain_here, query_weight, query_gain_here)
     all_queries = lax.all_to_all(
         copies, "tp", 0, 0, tiled=True, axis_index_groups=halves
     )
     far = lax.ppermute(near, "sp", [(i, i ^ 1) for i in range(sp)])
-    pair_weight = lax.ppermute(out_weight, "tp", [(i, i ^ 1) for i in range(tp)])
+    pair_weight = lax.ppermute(out_weight, "tp", [(i, i ^ 2) for i in range(tp)])
     keys = 2 * near.shape[0]
     partials = call(
         attention_kernel,
-        bf16(GROUP, block + STAT_ROWS, HEAD_SIZE),
+        pltpu.HBM((GROUP, block + STAT_ROWS, HEAD_SIZE), jnp.bfloat16),
         cost(4 * GROUP * block * keys * HEAD_SIZE, 2500000, GROUP * block * keys),
         [VMEM] * 3,
+        HBM,
+        (
+            pltpu.VMEM((GROUP, block + STAT_ROWS, HEAD_SIZE), jnp.bfloat16),
+            pltpu.SemaphoreType.DMA((GROUP,)),
+        ),
     )(all_queries, near, far)
     mine = lax.all_to_all(partials, "tp", 0, 0, tiled=True, axis_index_groups=halves)
     update = call(
@@ -332,7 +353,7 @@
         cost(2 * block * width * HEAD_SIZE, 1900000),
         [VMEM] * 3,
     )(mine, out_weight, pair_weight)
-    parts = lax.all_to_all(update, "tp", 0, 0, tiled=True, axis_index_groups=parities)
+    parts = lax.all_to_all(update, "tp", 0, 0, tiled=True, axis_index_groups=sides)
     return call(
         final_kernel,
         bf16(own_rows, width),

time: 108 us -> 107 us (level)
  starting transfers between devices: 19 us -> 22.4 us
  waiting for transfers between devices: 13.8 us -> 11.4 us
  blocking collectives: 63.9 us -> 62.2 us
    all_to_all x1, waiting for transfers between devices: 5.52 us -> 3.07 us  [body(): lax.all_to_all(copies, 'tp', 0, 0, tiled=True, axis_index_groups=halves)]
    ppermute x1, starting transfers between devices: 2.02 us -> 3.98 us  [body(): lax.ppermute(out_weight, 'tp', [(i, i ^ 2) for i in range(tp)])]
    all_to_all x1, blocking collectives: 11.3 us -> 9.69 us  [body(): lax.all_to_all(update, 'tp', 0, 0, tiled=True, axis_index_groups=sides)]
    all_to_all x1, starting transfers between devices: 3.89 us -> 5.27 us  [body(): lax.all_to_all(partials, 'tp', 0, 0, tiled=True, axis_index_groups=halves)]
  transfers between devices with their start and end apart: 5 -> 5, of which waited for: 3 -> 3; matrix products, arithmetic and copies ran while one was open for 0% -> 0% of each run, Pallas kernels for 6% -> 7%
where the time goes in v5:
time: 107 us
  blocking collectives  62.2 us (58%)
  starting transfers between devices  22.4 us (21%)
  waiting for transfers between devices  11.4 us (11%)
  Pallas kernels  10.5 us (10%)
    all_gather x1, blocking collectives, body(): lax.all_gather(jnp.concatenate([own, received], axis=0), 'sp', axis=0, ti...  35 us
    all_to_all x1, blocking collectives, body(): everyone = lax.all_to_all(target_copies, 'tp', 0, 0, tiled=True)  17.6 us
    all_to_all x1, blocking collectives, body(): lax.all_to_all(update, 'tp', 0, 0, tiled=True, axis_index_groups=sides)  9.69 us
    all_to_all x1, waiting for transfers between devices, body(): lax.all_to_all(partials, 'tp', 0, 0, tiled=True, axis_index_groups=halves)  6.33 us
    pallas_call x1, Pallas kernels, body(): call(attention_kernel, pltpu.HBM((GROUP, block + STAT_ROWS, HEAD_SIZE), j...  5.64 us
    all_to_all x1, starting transfers between devices, body(): lax.all_to_all(partials, 'tp', 0, 0, tiled=True, axis_index_groups=halves)  5.27 us
    ppermute x1, starting transfers between devices, body(): received = lax.ppermute(other, 'tp', opposite)  5.05 us
    all_to_all x1, starting transfers between devices, body(): lax.all_to_all(copies, 'tp', 0, 0, tiled=True, axis_index_groups=halves)  4.92 us
  transfers between devices with their start and end apart: 5, of which 3 were waited for; matrix products, arithmetic and copies ran while one was open for 0% of the time, Pallas kernels for 7%

profile of v5, /device:TPU:2, one launch (start us, length us, event | category | flops | bytes accessed | tf_op | source)
XLA Modules:
  0.0 106.6 jit_solution(1733948499528603719)
XLA Ops:
  0.0 2.4 %shard_map.100 = (bf16[48,256]{1,0:T(8,128)(2,1)S(1)}, bf16[48,256]{1,0:T(8,128)(2,1)S(1)}, bf16[16,8,2048]{2,1,0:T(8,128)(2,1)}, f32[1,2048]{1,0:T(1,128)S(1)}, f32[1,128]{1,0:T(1,128)S(1)}) custom-call(bf16[8,2048]{1,0:T(8,128)(2,1)} %target.3, bf16[48,2048]{1,0:T(8,128)(2,1)} %source.1, f32[1,2048]{1,0:T(1,128)} %bitcast.4, bf16[2048,256]{1,0:T(8,128)(2,1)} %key_matrix.1, ...), custom_call_target="tpu_custom_call" | custom-call | flops 100663296 | bytes 3000000 | tf_op jit(solution)/shard_map/pallas_call | solution.py:272
  2.4 0.0 copy-start.3
  2.4 5.1 %collective-permute-start = (bf16[48,256]{1,0:T(8,128)(2,1)S(1)}, bf16[48,256]{1,0:T(8,128)(2,1)S(1)}, u32[]{:S(2)}, u32[]{:S(2)}) collective-permute-start(bf16[48,256]{1,0:T(8,128)(2,1)S(1)} %get-tuple-element.14), channel_id=1, source_target_pairs={{0,12},{1,13},{2,14},{3,15},{4,8},{5,9},{6,10},{7,11},{8,4},{9,5},... | collective-permute-start | bytes 73736 | tf_op jit(solution)/shard_map/ppermute | solution.py:311
  7.4 2.0 %collective-permute-done = bf16[48,256]{1,0:T(8,128)(2,1)S(1)} collective-permute-done((bf16[48,256]{1,0:T(8,128)(2,1)S(1)}, bf16[48,256]{1,0:T(8,128)(2,1)S(1)}, u32[]{:S(2)}, u32[]{:S(2)}) %collective-permute-start) | collective-permute-done | bytes 24608 | tf_op jit(solution)/shard_map/ppermute | solution.py:311
  9.5 35.0 %all_gather.3.near = bf16[1536,256]{1,0:T(8,128)(2,1)S(1)} all-gather(bf16[96,256]{1,0:T(8,128)(2,1)S(1)} %pad_maximum_fusion), channel_id=1, replica_groups={{0,48,64,112,128,176,192,240,256,304,320,368,384,432,448,496},{16,32,80..., dimensions={0}, use_global_device_ids=true | all-gather | bytes 835584 | tf_op jit(solution)/shard_map/all_gather | solution.py:314
  44.4 3.2 %collective-permute-start.1 = (bf16[1536,256]{1,0:T(8,128)(2,1)S(1)}, bf16[1536,256]{1,0:T(8,128)(2,1)S(1)}, u32[]{:S(2)}, u32[]{:S(2)}) collective-permute-start(bf16[1536,256]{1,0:T(8,128)(2,1)S(1)} %all_gather.3.near), channel_id=1, source_target_pairs={{0,16},{16,0},{32,48},{48,32},{64,80},{80,64},{96,112},{112,96},{1... | collective-permute-start | bytes 2359304 | tf_op jit(solution)/shard_map/ppermute | solution.py:335
  47.6 0.0 copy-start
  47.6 17.6 %all_to_all.20 = bf16[16,8,2048]{2,1,0:T(8,128)(2,1)S(1)} all-to-all(bf16[16,8,2048]{2,1,0:T(8,128)(2,1)S(1)} %copy-done.3), channel_id=1, replica_groups=mesh['sp'=32,'tp'=16] {'tp'}, dimensions={0} | all-to-all | bytes 1048576 | tf_op jit(solution)/shard_map/all_to_all | solution.py:312
  65.2 0.0 copy-done
  65.2 1.3 %shard_map.101 = bf16[8,128,128]{2,1,0:T(8,128)(2,1)} custom-call(bf16[128,2048]{1,0:T(8,128)(2,1)S(1)} %bitcast.3, f32[1,2048]{1,0:T(1,128)S(1)} %get-tuple-element.11.gain, bf16[2048,128]{1,0:T(8,128)(2,1)S(1)} %copy-done, f32[1,128]{1,0:T(1,128)S(1)} %get-tuple-element.12.head_gain), custom_call_target="tpu_custom_call" | custom-call | flops 67108864 | bytes 1400000 | tf_op jit(solution)/shard_map/pallas_call | solution.py:321
  66.5 0.0 copy-start.1
  66.5 4.9 %all-to-all-start.1 = ((bf16[8,128,128]{2,1,0:T(8,128)(2,1)}), bf16[8,128,128]{2,1,0:T(8,128)(2,1)S(1)}, u32[]{:S(2)}, u32[]{:S(2)}) async-start(bf16[8,128,128]{2,1,0:T(8,128)(2,1)} %shard_map.101), calls=%async_computation.1 | async-start | bytes 524288 | tf_op jit(solution)/shard_map/all_to_all | solution.py:332
  71.4 0.0 copy-done.1
  71.4 4.0 %collective-permute-start.2 = (bf16[128,2048]{1,0:T(8,128)(2,1)S(1)}, bf16[128,2048]{1,0:T(8,128)(2,1)S(1)}, u32[]{:S(2)}, u32[]{:S(2)}) collective-permute-start(bf16[128,2048]{1,0:T(8,128)(2,1)S(1)} %copy-done.1), channel_id=1, source_target_pairs={{0,2},{1,3},{2,0},{3,1},{4,6},{5,7},{6,4},{7,5},{8,10},{9,11},{10,... | collective-permute-start | bytes 1572872 | tf_op jit(solution)/shard_map/ppermute | solution.py:336
  75.4 3.1 %all-to-all-done.1.queries = bf16[8,128,128]{2,1,0:T(8,128)(2,1)S(1)} async-done(((bf16[8,128,128]{2,1,0:T(8,128)(2,1)}), bf16[8,128,128]{2,1,0:T(8,128)(2,1)S(1)}, u32[]{:S(2)}, u32[]{:S(2)}) %all-to-all-start.1) | async-done | bytes 262176 | tf_op jit(solution)/shard_map/all_to_all | solution.py:332
  78.5 0.0 collective-permute-done.1.far
  78.5 5.6 %shard_map.102 = bf16[8,144,128]{2,1,0:T(8,128)(2,1)} custom-call(bf16[8,128,128]{2,1,0:T(8,128)(2,1)S(1)} %all-to-all-done.1.queries, bf16[1536,256]{1,0:T(8,128)(2,1)S(1)} %all_gather.3.near, bf16[1536,256]{1,0:T(8,128)(2,1)S(1)} %collective-permute-done.1.far), custom_call_target="tpu_custom_call" | custom-call | flops 1610612736 | bytes 2500000 | tf_op jit(solution)/shard_map/pallas_call | solution.py:338
  84.1 5.3 %all-to-all-start.2 = ((bf16[8,144,128]{2,1,0:T(8,128)(2,1)}), bf16[8,144,128]{2,1,0:T(8,128)(2,1)S(1)}, u32[]{:S(2)}, u32[]{:S(2)}) async-start(bf16[8,144,128]{2,1,0:T(8,128)(2,1)} %shard_map.102), calls=%async_computation.2 | async-start | bytes 589824 | tf_op jit(solution)/shard_map/all_to_all | solution.py:349
  89.4 0.0 collective-permute-done.2.pair_weight
  89.4 6.3 %all-to-all-done.2.partials = bf16[8,144,128]{2,1,0:T(8,128)(2,1)S(1)} async-done(((bf16[8,144,128]{2,1,0:T(8,128)(2,1)}), bf16[8,144,128]{2,1,0:T(8,128)(2,1)S(1)}, u32[]{:S(2)}, u32[]{:S(2)}) %all-to-all-start.2) | async-done | bytes 294944 | tf_op jit(solution)/shard_map/all_to_all | solution.py:349
  95.7 0.5 shard_map.103
  96.3 0.0 copy-start.2
  96.3 9.7 %all_to_all.21.parts = bf16[8,8,2048]{2,1,0:T(8,128)(2,1)S(1)} all-to-all(bf16[8,8,2048]{2,1,0:T(8,128)(2,1)S(1)} %shard_map.103), channel_id=1, replica_groups={{0,1,4,5,8,9,12,13},{2,3,6,7,10,11,14,15},{16,17,20,21,24,25,28,29},{18..., dimensions={0} | all-to-all | bytes 524288 | tf_op jit(solution)/shard_map/all_to_all | solution.py:356
  106.0 0.7 shard_map.104
  (3 shorter events, 0.0 us)
Async XLA Ops:
  2.4 45.2 %copy-start.3 = (bf16[16,8,2048]{2,1,0:T(8,128)(2,1)S(1)}, bf16[16,8,2048]{2,1,0:T(8,128)(2,1)}, u32[]{:S(2)}) copy-start(bf16[16,8,2048]{2,1,0:T(8,128)(2,1)} %get-tuple-element.10) | copy-start | bytes 1572868
  2.4 7.1 %collective-permute-start = (bf16[48,256]{1,0:T(8,128)(2,1)S(1)}, bf16[48,256]{1,0:T(8,128)(2,1)S(1)}, u32[]{:S(2)}, u32[]{:S(2)}) collective-permute-start(bf16[48,256]{1,0:T(8,128)(2,1)S(1)} %get-tuple-element.14), channel_id=1, source_target_pairs={{0,12},{1,13},{2,14},{3,15},{4,8},{5,9},{6,10},{7,11},{8,4},{9,5},... | collective-permute-start | bytes 73736 | tf_op jit(solution)/shard_map/ppermute | solution.py:311
  44.4 34.1 %collective-permute-start.1 = (bf16[1536,256]{1,0:T(8,128)(2,1)S(1)}, bf16[1536,256]{1,0:T(8,128)(2,1)S(1)}, u32[]{:S(2)}, u32[]{:S(2)}) collective-permute-start(bf16[1536,256]{1,0:T(8,128)(2,1)S(1)} %all_gather.3.near), channel_id=1, source_target_pairs={{0,16},{16,0},{32,48},{48,32},{64,80},{80,64},{96,112},{112,96},{1... | collective-permute-start | bytes 2359304 | tf_op jit(solution)/shard_map/ppermute | solution.py:335
  47.6 17.6 %copy-start = (bf16[2048,128]{1,0:T(8,128)(2,1)S(1)}, bf16[2048,128]{1,0:T(8,128)(2,1)}, u32[]{:S(2)}) copy-start(bf16[2048,128]{1,0:T(8,128)(2,1)} %weight.1) | copy-start | bytes 1572868
  66.5 4.9 %copy-start.1 = (bf16[128,2048]{1,0:T(8,128)(2,1)S(1)}, bf16[128,2048]{1,0:T(8,128)(2,1)}, u32[]{:S(2)}) copy-start(bf16[128,2048]{1,0:T(8,128)(2,1)} %own_weight.1) | copy-start | bytes 1572868
  66.5 12.0 %all-to-all-start.1 = ((bf16[8,128,128]{2,1,0:T(8,128)(2,1)}), bf16[8,128,128]{2,1,0:T(8,128)(2,1)S(1)}, u32[]{:S(2)}, u32[]{:S(2)}) async-start(bf16[8,128,128]{2,1,0:T(8,128)(2,1)} %shard_map.101), calls=%async_computation.1 | async-start | bytes 524288 | tf_op jit(solution)/shard_map/all_to_all | solution.py:332
  71.4 18.0 %collective-permute-start.2 = (bf16[128,2048]{1,0:T(8,128)(2,1)S(1)}, bf16[128,2048]{1,0:T(8,128)(2,1)S(1)}, u32[]{:S(2)}, u32[]{:S(2)}) collective-permute-start(bf16[128,2048]{1,0:T(8,128)(2,1)S(1)} %copy-done.1), channel_id=1, source_target_pairs={{0,2},{1,3},{2,0},{3,1},{4,6},{5,7},{6,4},{7,5},{8,10},{9,11},{10,... | collective-permute-start | bytes 1572872 | tf_op jit(solution)/shard_map/ppermute | solution.py:336
  84.1 11.6 %all-to-all-start.2 = ((bf16[8,144,128]{2,1,0:T(8,128)(2,1)}), bf16[8,144,128]{2,1,0:T(8,128)(2,1)S(1)}, u32[]{:S(2)}, u32[]{:S(2)}) async-start(bf16[8,144,128]{2,1,0:T(8,128)(2,1)} %shard_map.102), calls=%async_computation.2 | async-start | bytes 589824 | tf_op jit(solution)/shard_map/all_to_all | solution.py:349
  96.3 9.7 %copy-start.2 = (bf16[8,2048]{1,0:T(8,128)(2,1)S(1)}, bf16[8,2048]{1,0:T(8,128)(2,1)}, u32[]{:S(2)}) copy-start(bf16[8,2048]{1,0:T(8,128)(2,1)} %target.3) | copy-start | bytes 98308

commit v6 on v5

--- a/solution.py
+++ b/solution.py
@@ -136,87 +136,92 @@
     return [first, second, third]
 
 
-def attention_kernel(queries, near, far, out, here, left):
-    rows = 2 * HEAD_SIZE
+def attention_kernel(queries, near, far, out):
+    rows = GROUP * HEAD_SIZE
     at_row = lax.broadcasted_iota(jnp.int32, (HEAD_SIZE, HEAD_SIZE), 0)
     at_lane = lax.broadcasted_iota(jnp.int32, (HEAD_SIZE, HEAD_SIZE), 1)
     eye = (at_row == at_lane).astype(jnp.float32)
-
-    def as_row(column):
-        return jnp.sum(eye * column, axis=0, keepdims=True)
-
-    outputs = []
+    q = queries[...].reshape(rows, HEAD_SIZE)
+    peak = None
+    for kv in (near, far):
+        scores = lax.dot_general(
+            q,
+            kv[:, :HEAD_SIZE],
+            (((1,), (1,)), ((), ())),
+            preferred_element_type=jnp.float32,
+        )
+        highest = jnp.max(scores, axis=-1, keepdims=True)
+        before, peak = peak, highest if peak is None else jnp.maximum(peak, highest)
+        weights = jnp.exp2((scores - peak) * EXP2_SCALE)
+        share = jnp.sum(weights, axis=-1, keepdims=True)
+        part = jnp.dot(
+            weights.astype(jnp.bfloat16),
+            kv[:, HEAD_SIZE:],
+            preferred_element_type=jnp.float32,
+        )
+        if before is None:
+            total, weighted = share, part
+        else:
+            fade = jnp.exp2((before - peak) * EXP2_SCALE)
+            total, weighted = total * fade + share, weighted * fade + part
+
+    def as_rows(column, head):
+        at = slice(head * HEAD_SIZE, (head + 1) * HEAD_SIZE)
+        return in_three(jnp.sum(eye * column[at], axis=0, keepdims=True))
+
     for head in range(GROUP):
         if head % 4 >= 2:
             continue
-        q = jnp.concatenate([queries[head], queries[head + 2]], axis=0)
-        scores = [
-            lax.dot_general(
-                q,
-                kv[:, :HEAD_SIZE],
-                (((1,), (1,)), ((), ())),
-                preferred_element_type=jnp.float32,
-            )
-            for kv in (near, far)
-        ]
-        peak = jnp.maximum(
-            jnp.max(scores[0], axis=-1, keepdims=True),
-            jnp.max(scores[1], axis=-1, keepdims=True),
-        )
-        total, weighted = 0.0, 0.0
-        for kv, s in zip((near, far), scores):
-            weights = jnp.exp2((s - peak) * EXP2_SCALE)
-            total += jnp.sum(weights, axis=-1, keepdims=True)
-            weighted += jnp.dot(
-                weights.astype(jnp.bfloat16),
-                kv[:, HEAD_SIZE:],
-                preferred_element_type=jnp.float32,
-            )
+        stats = []
+        for h in (head, head + 2):
+            stats += as_rows(peak, h) + as_rows(total, h)
+        empty = jnp.zeros((STAT_ROWS - len(stats), HEAD_SIZE), jnp.bfloat16)
+        stats = jnp.concatenate(stats + [empty], axis=0)
         for side in range(2):
-            def picked(column):
-                return jnp.concatenate(
-                    [column[i : i + 16] for i in range(16 * side, rows, 32)], axis=0
-                )
-
             to = head + 2 * side
-            here[to, :HEAD_SIZE, :] = picked(weighted).astype(jnp.bfloat16)
-            stats = in_three(as_row(picked(peak))) + in_three(as_row(picked(total)))
-            empty = jnp.zeros((STAT_ROWS - len(stats), HEAD_SIZE), jnp.bfloat16)
-            here[to, HEAD_SIZE:, :] = jnp.concatenate(stats + [empty], axis=0)
-            outputs.append(pltpu.make_async_copy(here.at[to], out.at[to], left.at[to]))
-            outputs[-1].start()
-    for c in outputs:
-        c.wait()
-
-
-def output_kernel(partials, own_weight, pair_weight, out):
-    at_row = lax.broadcasted_iota(jnp.int32, (HEAD_SIZE, HEAD_SIZE), 0)
-    at_lane = lax.broadcasted_iota(jnp.int32, (HEAD_SIZE, HEAD_SIZE), 1)
-    eye = (at_row == at_lane).astype(jnp.float32)
-    peaks, totals = [], []
-    for j in range(GROUP):
-        stats = partials[j, HEAD_SIZE:, :].astype(jnp.float32)
-        peaks.append(stats[0:1] + stats[1:2] + stats[2:3])
-        totals.append(stats[3:4] + stats[4:5] + stats[5:6])
-    peak = peaks[0]
-    for p in peaks[1:]:
-        peak = jnp.maximum(peak, p)
-    fades = [jnp.exp2((p - peak) * EXP2_SCALE) for p in peaks]
-    total = fades[0] * totals[0]
-    for f, t in zip(fades[1:], totals[1:]):
-        total += f * t
-    attended = 0.0
-    for j in range(GROUP):
-        column = jnp.sum(eye * (fades[j] / total), axis=1, keepdims=True)
-        attended += column * partials[j, :HEAD_SIZE, :].astype(jnp.float32)
-    attended = attended.astype(jnp.bfloat16)
-    low, high = attended[: HEAD_SIZE // 2], attended[HEAD_SIZE // 2 :]
+            out[to, :HEAD_SIZE, :] = jnp.concatenate(
+                [
+                    weighted[h * HEAD_SIZE + i : h * HEAD_SIZE + i + 16]
+                    for h in (head, head + 2)
+                    for i in range(16 * side, HEAD_SIZE, 32)
+                ],
+                axis=0,
+            ).astype(jnp.bfloat16)
+            out[to, HEAD_SIZE:, :] = stats
+
+
+def combine_kernel(partials, own, pair):
     is_high = lax.rem(lax.axis_index("tp"), 4) >= 2
-    update = jnp.dot(
-        jnp.where(is_high, high, low), own_weight[...], preferred_element_type=jnp.float32
-    ) + jnp.dot(
-        jnp.where(is_high, low, high), pair_weight[...], preferred_element_type=jnp.float32
-    )
+    half = HEAD_SIZE // 2
+    row = lax.broadcasted_iota(jnp.int32, (half, HEAD_SIZE), 0)
+    lane = lax.broadcasted_iota(jnp.int32, (half, HEAD_SIZE), 1)
+    place = row + (row // 16) * 16 + jnp.where(is_high, 16, 0)
+    selection = (lane == place).astype(jnp.float32)
+    stats = [partials[j, HEAD_SIZE:, :].astype(jnp.float32) for j in range(GROUP)]
+    results = []
+    for k in range(2):
+        peaks = [s[6 * k : 6 * k + 1] + s[6 * k + 1 : 6 * k + 2] + s[6 * k + 2 : 6 * k + 3] for s in stats]
+        totals = [s[6 * k + 3 : 6 * k + 4] + s[6 * k + 4 : 6 * k + 5] + s[6 * k + 5 : 6 * k + 6] for s in stats]
+        peak = peaks[0]
+        for p in peaks[1:]:
+            peak = jnp.maximum(peak, p)
+        fades = [jnp.exp2((p - peak) * EXP2_SCALE) for p in peaks]
+        total = fades[0] * totals[0]
+        for f, t in zip(fades[1:], totals[1:]):
+            total += f * t
+        attended = 0.0
+        for j in range(GROUP):
+            column = jnp.sum(selection * (fades[j] / total), axis=1, keepdims=True)
+            attended += column * partials[j, half * k : half * (k + 1), :].astype(jnp.float32)
+        results.append(attended.astype(jnp.bfloat16))
+    low, high = results
+    own[...] = jnp.where(is_high, high, low)
+    pair[...] = jnp.where(is_high, low, high)
+
+
+def output_kernel(own, pair, own_weight, pair_weight, out):
+    update = jnp.dot(own[...], own_weight[...], preferred_element_type=jnp.float32)
+    update += jnp.dot(pair[...], pair_weight[...], preferred_element_type=jnp.float32)
     out[...] = update.astype(jnp.bfloat16).reshape(out.shape)
 
 
@@ -227,7 +232,7 @@
     out[...] = (target[...].astype(jnp.float32) + update).astype(jnp.bfloat16)
 
 
-def call(kernel, outs, estimate, specs, out_specs=None, scratch=(), vmem=48 * 1024 * 1024):
+def call(kernel, outs, estimate, specs, out_specs=None, scratch=(), vmem=32 * 1024 * 1024):
     return pl.pallas_call(
         kernel,
         out_shape=outs,
@@ -337,22 +342,21 @@
     keys = 2 * near.shape[0]
     partials = call(
         attention_kernel,
-        pltpu.HBM((GROUP, block + STAT_ROWS, HEAD_SIZE), jnp.bfloat16),
+        bf16(GROUP, block + STAT_ROWS, HEAD_SIZE),
         cost(4 * GROUP * block * keys * HEAD_SIZE, 2500000, GROUP * block * keys),
         [VMEM] * 3,
-        HBM,
-        (
-            pltpu.VMEM((GROUP, block + STAT_ROWS, HEAD_SIZE), jnp.bfloat16),
-            pltpu.SemaphoreType.DMA((GROUP,)),
-        ),
-    )(all_queries, near, far)
+    )(all_queries, near, pltpu.with_memory_space_constraint(far, pltpu.VMEM))
     mine = lax.all_to_all(partials, "tp", 0, 0, tiled=True, axis_index_groups=halves)
+    half = bf16(block // 2, HEAD_SIZE)
+    own_part, pair_part = call(
+        combine_kernel, (half, half), cost(4 * GROUP * block * HEAD_SIZE, 400000), [VMEM]
+    )(mine)
     update = call(
         output_kernel,
         bf16(tp // 2, own_rows, width),
         cost(2 * block * width * HEAD_SIZE, 1900000),
-        [VMEM] * 3,
-    )(mine, out_weight, pair_weight)
+        [VMEM] * 4,
+    )(own_part, pair_part, out_weight, pair_weight)
     parts = lax.all_to_all(update, "tp", 0, 0, tiled=True, axis_index_groups=sides)
     return call(
         final_kernel,

time: 107 us -> 105 us (0.981)
  blocking collectives: 62.2 us -> 73 us
  waiting for transfers between devices: 11.4 us -> 5.07 us
  starting transfers between devices: 22.4 us -> 17.1 us
  Pallas kernels: 10.5 us -> 9.21 us
    all_to_all x0 -> x1, blocking collectives: none -> 10.6 us  [body(): lax.all_to_all(partials, 'tp', 0, 0, tiled=True, axis_index_groups=halves)]
    all_to_all x1 -> x0, waiting for transfers between devices: 6.33 us -> none  [body(): lax.all_to_all(partials, 'tp', 0, 0, tiled=True, axis_index_groups=halves)]
    all_to_all x1 -> x0, starting transfers between devices: 5.27 us -> none  [body(): lax.all_to_all(partials, 'tp', 0, 0, tiled=True, axis_index_groups=halves)]
    pallas_call x1 -> x2, Pallas kernels: 5.64 us -> 4.57 us  [the longest x1 4.32 us: body(): call(attention_kernel, bf16(GROUP, block + STAT_ROWS, HEAD_SIZE), cost(4...]
  transfers between devices with their start and end apart: 5 -> 4, of which waited for: 3 -> 2; matrix products, arithmetic and copies ran while one was open for 0% -> 0% of each run, Pallas kernels for 7% -> 6%
where the time goes in v6:
time: 105 us
  blocking collectives  73 us (70%)
  starting transfers between devices  17.1 us (16%)
  Pallas kernels  9.21 us (9%)
  waiting for transfers between devices  5.07 us (5%)
    all_gather x1, blocking collectives, body(): lax.all_gather(jnp.concatenate([own, received], axis=0), 'sp', axis=0, ti...  35 us
    all_to_all x1, blocking collectives, body(): everyone = lax.all_to_all(target_copies, 'tp', 0, 0, tiled=True)  17.6 us
    all_to_all x1, blocking collectives, body(): lax.all_to_all(partials, 'tp', 0, 0, tiled=True, axis_index_groups=halves)  10.6 us
    all_to_all x1, blocking collectives, body(): lax.all_to_all(update, 'tp', 0, 0, tiled=True, axis_index_groups=sides)  9.9 us
    ppermute x1, starting transfers between devices, body(): received = lax.ppermute(other, 'tp', opposite)  5.05 us
    all_to_all x1, starting transfers between devices, body(): lax.all_to_all(copies, 'tp', 0, 0, tiled=True, axis_index_groups=halves)  4.92 us
    pallas_call x1, Pallas kernels, body(): call(attention_kernel, bf16(GROUP, block + STAT_ROWS, HEAD_SIZE), cost(4...  4.32 us
    ppermute x1, starting transfers between devices, body(): lax.ppermute(out_weight, 'tp', [(i, i ^ 2) for i in range(tp)])  3.98 us
  transfers between devices with their start and end apart: 4, of which 2 were waited for; matrix products, arithmetic and copies ran while one was open for 0% of the time, Pallas kernels for 6%

profile of v6, /device:TPU:2, one launch (start us, length us, event | category | flops | bytes accessed | tf_op | source)
XLA Modules:
  0.0 104.6 jit_solution(17733469214587011410)
XLA Ops:
  0.0 2.4 %shard_map.100 = (bf16[48,256]{1,0:T(8,128)(2,1)S(1)}, bf16[48,256]{1,0:T(8,128)(2,1)S(1)}, bf16[16,8,2048]{2,1,0:T(8,128)(2,1)}, f32[1,2048]{1,0:T(1,128)S(1)}, f32[1,128]{1,0:T(1,128)S(1)}) custom-call(bf16[8,2048]{1,0:T(8,128)(2,1)} %target.3, bf16[48,2048]{1,0:T(8,128)(2,1)} %source.1, f32[1,2048]{1,0:T(1,128)} %bitcast.4, bf16[2048,256]{1,0:T(8,128)(2,1)} %key_matrix.1, ...), custom_call_target="tpu_custom_call" | custom-call | flops 100663296 | bytes 3000000 | tf_op jit(solution)/shard_map/pallas_call | solution.py:277
  2.4 0.0 copy-start.3
  2.4 5.1 %collective-permute-start = (bf16[48,256]{1,0:T(8,128)(2,1)S(1)}, bf16[48,256]{1,0:T(8,128)(2,1)S(1)}, u32[]{:S(2)}, u32[]{:S(2)}) collective-permute-start(bf16[48,256]{1,0:T(8,128)(2,1)S(1)} %get-tuple-element.16), channel_id=1, source_target_pairs={{0,12},{1,13},{2,14},{3,15},{4,8},{5,9},{6,10},{7,11},{8,4},{9,5},... | collective-permute-start | bytes 73736 | tf_op jit(solution)/shard_map/ppermute | solution.py:316
  7.4 2.0 %collective-permute-done = bf16[48,256]{1,0:T(8,128)(2,1)S(1)} collective-permute-done((bf16[48,256]{1,0:T(8,128)(2,1)S(1)}, bf16[48,256]{1,0:T(8,128)(2,1)S(1)}, u32[]{:S(2)}, u32[]{:S(2)}) %collective-permute-start) | collective-permute-done | bytes 24608 | tf_op jit(solution)/shard_map/ppermute | solution.py:316
  9.5 35.0 %all_gather.3.near = bf16[1536,256]{1,0:T(8,128)(2,1)S(1)} all-gather(bf16[96,256]{1,0:T(8,128)(2,1)S(1)} %pad_maximum_fusion), channel_id=1, replica_groups={{0,48,64,112,128,176,192,240,256,304,320,368,384,432,448,496},{16,32,80..., dimensions={0}, use_global_device_ids=true | all-gather | bytes 835584 | tf_op jit(solution)/shard_map/all_gather | solution.py:319
  44.4 3.2 %collective-permute-start.1 = (bf16[1536,256]{1,0:T(8,128)(2,1)S(1)}, bf16[1536,256]{1,0:T(8,128)(2,1)S(1)}, u32[]{:S(2)}, u32[]{:S(2)}) collective-permute-start(bf16[1536,256]{1,0:T(8,128)(2,1)S(1)} %all_gather.3.near), channel_id=1, source_target_pairs={{0,16},{16,0},{32,48},{48,32},{64,80},{80,64},{96,112},{112,96},{1... | collective-permute-start | bytes 2359304 | tf_op jit(solution)/shard_map/ppermute | solution.py:340
  47.6 0.0 copy-done.3
  47.6 0.0 copy-start
  47.6 17.6 %all_to_all.20 = bf16[16,8,2048]{2,1,0:T(8,128)(2,1)S(1)} all-to-all(bf16[16,8,2048]{2,1,0:T(8,128)(2,1)S(1)} %copy-done.3), channel_id=1, replica_groups=mesh['sp'=32,'tp'=16] {'tp'}, dimensions={0} | all-to-all | bytes 1048576 | tf_op jit(solution)/shard_map/all_to_all | solution.py:317
  65.2 0.0 copy-done
  65.2 1.3 %shard_map.101 = bf16[8,128,128]{2,1,0:T(8,128)(2,1)} custom-call(bf16[128,2048]{1,0:T(8,128)(2,1)S(1)} %bitcast.3, f32[1,2048]{1,0:T(1,128)S(1)} %get-tuple-element.13.gain, bf16[2048,128]{1,0:T(8,128)(2,1)S(1)} %copy-done, f32[1,128]{1,0:T(1,128)S(1)} %get-tuple-element.14.head_gain), custom_call_target="tpu_custom_call" | custom-call | flops 67108864 | bytes 1400000 | tf_op jit(solution)/shard_map/pallas_call | solution.py:326
  66.5 0.0 copy-start.1
  66.5 4.9 %all-to-all-start.1 = ((bf16[8,128,128]{2,1,0:T(8,128)(2,1)}), bf16[8,128,128]{2,1,0:T(8,128)(2,1)S(1)}, u32[]{:S(2)}, u32[]{:S(2)}) async-start(bf16[8,128,128]{2,1,0:T(8,128)(2,1)} %shard_map.101), calls=%async_computation.1 | async-start | bytes 524288 | tf_op jit(solution)/shard_map/all_to_all | solution.py:337
  71.4 4.0 %collective-permute-start.2 = (bf16[128,2048]{1,0:T(8,128)(2,1)S(1)}, bf16[128,2048]{1,0:T(8,128)(2,1)S(1)}, u32[]{:S(2)}, u32[]{:S(2)}) collective-permute-start(bf16[128,2048]{1,0:T(8,128)(2,1)S(1)} %copy-done.1), channel_id=1, source_target_pairs={{0,2},{1,3},{2,0},{3,1},{4,6},{5,7},{6,4},{7,5},{8,10},{9,11},{10,... | collective-permute-start | bytes 1572872 | tf_op jit(solution)/shard_map/ppermute | solution.py:341
  75.4 3.1 %all-to-all-done.1.queries = bf16[8,128,128]{2,1,0:T(8,128)(2,1)S(1)} async-done(((bf16[8,128,128]{2,1,0:T(8,128)(2,1)}), bf16[8,128,128]{2,1,0:T(8,128)(2,1)S(1)}, u32[]{:S(2)}, u32[]{:S(2)}) %all-to-all-start.1) | async-done | bytes 262176 | tf_op jit(solution)/shard_map/all_to_all | solution.py:337
  78.5 0.0 collective-permute-done.1.far
  78.5 4.3 %shard_map.102 = bf16[8,144,128]{2,1,0:T(8,128)(2,1)S(1)} custom-call(bf16[8,128,128]{2,1,0:T(8,128)(2,1)S(1)} %all-to-all-done.1.queries, bf16[1536,256]{1,0:T(8,128)(2,1)S(1)} %all_gather.3.near, bf16[1536,256]{1,0:T(8,128)(2,1)S(1)} %collective-permute-done.1.far), custom_call_target="tpu_custom_call" | custom-call | flops 1610612736 | bytes 2500000 | tf_op jit(solution)/shard_map/pallas_call | solution.py:343
  82.8 10.6 %all_to_all.21.partials = bf16[8,144,128]{2,1,0:T(8,128)(2,1)S(1)} all-to-all(bf16[8,144,128]{2,1,0:T(8,128)(2,1)S(1)} %shard_map.102), channel_id=1, replica_groups={{0,1,2,3,4,5,6,7},{8,9,10,11,12,13,14,15},{16,17,18,19,20,21,22,23},{24..., dimensions={0} | all-to-all | bytes 589824 | tf_op jit(solution)/shard_map/all_to_all | solution.py:349
  93.4 0.3 shard_map.103
  93.7 0.0 collective-permute-done.2.pair_weight
  93.7 0.3 shard_map.104
  94.0 0.0 copy-start.2
  94.0 9.9 %all_to_all.22.parts = bf16[8,8,2048]{2,1,0:T(8,128)(2,1)S(1)} all-to-all(bf16[8,8,2048]{2,1,0:T(8,128)(2,1)S(1)} %shard_map.104), channel_id=1, replica_groups={{0,1,4,5,8,9,12,13},{2,3,6,7,10,11,14,15},{16,17,20,21,24,25,28,29},{18..., dimensions={0} | all-to-all | bytes 524288 | tf_op jit(solution)/shard_map/all_to_all | solution.py:360
  103.9 0.7 shard_map.105
  (3 shorter events, 0.0 us)
Async XLA Ops:
  2.4 45.2 %copy-start.3 = (bf16[16,8,2048]{2,1,0:T(8,128)(2,1)S(1)}, bf16[16,8,2048]{2,1,0:T(8,128)(2,1)}, u32[]{:S(2)}) copy-start(bf16[16,8,2048]{2,1,0:T(8,128)(2,1)} %get-tuple-element.12) | copy-start | bytes 1572868
  2.4 7.1 %collective-permute-start = (bf16[48,256]{1,0:T(8,128)(2,1)S(1)}, bf16[48,256]{1,0:T(8,128)(2,1)S(1)}, u32[]{:S(2)}, u32[]{:S(2)}) collective-permute-start(bf16[48,256]{1,0:T(8,128)(2,1)S(1)} %get-tuple-element.16), channel_id=1, source_target_pairs={{0,12},{1,13},{2,14},{3,15},{4,8},{5,9},{6,10},{7,11},{8,4},{9,5},... | collective-permute-start | bytes 73736 | tf_op jit(solution)/shard_map/ppermute | solution.py:316
  44.4 34.1 %collective-permute-start.1 = (bf16[1536,256]{1,0:T(8,128)(2,1)S(1)}, bf16[1536,256]{1,0:T(8,128)(2,1)S(1)}, u32[]{:S(2)}, u32[]{:S(2)}) collective-permute-start(bf16[1536,256]{1,0:T(8,128)(2,1)S(1)} %all_gather.3.near), channel_id=1, source_target_pairs={{0,16},{16,0},{32,48},{48,32},{64,80},{80,64},{96,112},{112,96},{1... | collective-permute-start | bytes 2359304 | tf_op jit(solution)/shard_map/ppermute | solution.py:340
  47.6 17.6 %copy-start = (bf16[2048,128]{1,0:T(8,128)(2,1)S(1)}, bf16[2048,128]{1,0:T(8,128)(2,1)}, u32[]{:S(2)}) copy-start(bf16[2048,128]{1,0:T(8,128)(2,1)} %weight.1) | copy-start | bytes 1572868
  66.5 4.9 %copy-start.1 = (bf16[128,2048]{1,0:T(8,128)(2,1)S(1)}, bf16[128,2048]{1,0:T(8,128)(2,1)}, u32[]{:S(2)}) copy-start(bf16[128,2048]{1,0:T(8,128)(2,1)} %own_weight.1) | copy-start | bytes 1572868
  66.5 12.0 %all-to-all-start.1 = ((bf16[8,128,128]{2,1,0:T(8,128)(2,1)}), bf16[8,128,128]{2,1,0:T(8,128)(2,1)S(1)}, u32[]{:S(2)}, u32[]{:S(2)}) async-start(bf16[8,128,128]{2,1,0:T(8,128)(2,1)} %shard_map.101), calls=%async_computation.1 | async-start | bytes 524288 | tf_op jit(solution)/shard_map/all_to_all | solution.py:337
  71.4 22.3 %collective-permute-start.2 = (bf16[128,2048]{1,0:T(8,128)(2,1)S(1)}, bf16[128,2048]{1,0:T(8,128)(2,1)S(1)}, u32[]{:S(2)}, u32[]{:S(2)}) collective-permute-start(bf16[128,2048]{1,0:T(8,128)(2,1)S(1)} %copy-done.1), channel_id=1, source_target_pairs={{0,2},{1,3},{2,0},{3,1},{4,6},{5,7},{6,4},{7,5},{8,10},{9,11},{10,... | collective-permute-start | bytes 1572872 | tf_op jit(solution)/shard_map/ppermute | solution.py:341
  94.0 9.9 %copy-start.2 = (bf16[8,2048]{1,0:T(8,128)(2,1)S(1)}, bf16[8,2048]{1,0:T(8,128)(2,1)}, u32[]{:S(2)}) copy-start(bf16[8,2048]{1,0:T(8,128)(2,1)} %target.3) | copy-start | bytes 98308

commit v7 on v6

--- a/solution.py
+++ b/solution.py
@@ -136,6 +136,10 @@
     return [first, second, third]
 
 
+def is_inner(device):
+    return device % 4 in (1, 2)
+
+
 def attention_kernel(queries, near, far, out):
     rows = GROUP * HEAD_SIZE
     at_row = lax.broadcasted_iota(jnp.int32, (HEAD_SIZE, HEAD_SIZE), 0)
@@ -169,33 +173,34 @@
         at = slice(head * HEAD_SIZE, (head + 1) * HEAD_SIZE)
         return in_three(jnp.sum(eye * column[at], axis=0, keepdims=True))
 
-    for head in range(GROUP):
-        if head % 4 >= 2:
-            continue
+    for head in range(0, GROUP, 2):
         stats = []
-        for h in (head, head + 2):
+        for h in (head, head + 1):
             stats += as_rows(peak, h) + as_rows(total, h)
         empty = jnp.zeros((STAT_ROWS - len(stats), HEAD_SIZE), jnp.bfloat16)
         stats = jnp.concatenate(stats + [empty], axis=0)
-        for side in range(2):
-            to = head + 2 * side
-            out[to, :HEAD_SIZE, :] = jnp.concatenate(
+        for h in (head, head + 1):
+            starts = (8, 16) if is_inner(h) else (0, 24)
+            out[h, :HEAD_SIZE, :] = jnp.concatenate(
                 [
-                    weighted[h * HEAD_SIZE + i : h * HEAD_SIZE + i + 16]
-                    for h in (head, head + 2)
-                    for i in range(16 * side, HEAD_SIZE, 32)
+                    weighted[i + start : i + start + 8]
+                    for i in range(head * HEAD_SIZE, (head + 2) * HEAD_SIZE, 32)
+                    for start in starts
                 ],
                 axis=0,
             ).astype(jnp.bfloat16)
-            out[to, HEAD_SIZE:, :] = stats
+            out[h, HEAD_SIZE:, :] = stats
 
 
 def combine_kernel(partials, own, pair):
-    is_high = lax.rem(lax.axis_index("tp"), 4) >= 2
+    x = lax.rem(lax.axis_index("tp"), 4)
+    is_high = lax.rem(x, 2) == 1
+    inner = (x == 1) | (x == 2)
     half = HEAD_SIZE // 2
     row = lax.broadcasted_iota(jnp.int32, (half, HEAD_SIZE), 0)
     lane = lax.broadcasted_iota(jnp.int32, (half, HEAD_SIZE), 1)
-    place = row + (row // 16) * 16 + jnp.where(is_high, 16, 0)
+    outer_place = jnp.where(row % 16 >= 8, 16, 0)
+    place = row + (row // 16) * 16 + jnp.where(inner, 8, outer_place)
     selection = (lane == place).astype(jnp.float32)
     stats = [partials[j, HEAD_SIZE:, :].astype(jnp.float32) for j in range(GROUP)]
     results = []
@@ -232,7 +237,7 @@
     out[...] = (target[...].astype(jnp.float32) + update).astype(jnp.bfloat16)
 
 
-def call(kernel, outs, estimate, specs, out_specs=None, scratch=(), vmem=32 * 1024 * 1024):
+def call(kernel, outs, estimate, specs, out_specs=None, scratch=(), vmem=48 * 1024 * 1024):
     return pl.pallas_call(
         kernel,
         out_shape=outs,
@@ -267,7 +272,7 @@
     block = own_rows * tp
     source_rows = source.shape[0]
     halves = [[i + h * GROUP for i in range(GROUP)] for h in range(KEY_VALUE_HEADS)]
-    sides = [[i for i in range(tp) if i // 2 % 2 == e] for e in range(2)]
+    sides = [[i for i in range(tp) if is_inner(i) == e] for e in (False, True)]
     along_z = [[2 * z + (z + core) % 2 for z in range(sp // 2)] for core in range(2)]
     side = math.isqrt(tp)
     opposite = [(i, (side - 1 - i // side) * side + i % side) for i in range(tp)]
@@ -338,14 +343,14 @@
         copies, "tp", 0, 0, tiled=True, axis_index_groups=halves
     )
     far = lax.ppermute(near, "sp", [(i, i ^ 1) for i in range(sp)])
-    pair_weight = lax.ppermute(out_weight, "tp", [(i, i ^ 2) for i in range(tp)])
+    pair_weight = lax.ppermute(out_weight, "tp", [(i, i ^ 1) for i in range(tp)])
     keys = 2 * near.shape[0]
     partials = call(
         attention_kernel,
         bf16(GROUP, block + STAT_ROWS, HEAD_SIZE),
         cost(4 * GROUP * block * keys * HEAD_SIZE, 2500000, GROUP * block * keys),
         [VMEM] * 3,
-    )(all_queries, near, pltpu.with_memory_space_constraint(far, pltpu.VMEM))
+    )(all_queries, near, far)
     mine = lax.all_to_all(partials, "tp", 0, 0, tiled=True, axis_index_groups=halves)
     half = bf16(block // 2, HEAD_SIZE)
     own_part, pair_part = call(

time: 105 us -> 106 us (level)
  the two profiles are of different devices: /device:TPU:2 before, /device:TPU:32 now
where the time goes in v7:
time: 106 us
  blocking collectives  76 us (72%)
  starting transfers between devices  14.7 us (14%)
  Pallas kernels  9.22 us (9%)
  waiting for transfers between devices  5.4 us (5%)
    all_gather x1, blocking collectives, body(): lax.all_gather(jnp.concatenate([own, received], axis=0), 'sp', axis=0, ti...  34.8 us
    all_to_all x1, blocking collectives, body(): everyone = lax.all_to_all(target_copies, 'tp', 0, 0, tiled=True)  18.6 us
    all_to_all x1, blocking collectives, body(): lax.all_to_all(partials, 'tp', 0, 0, tiled=True, axis_index_groups=halves)  11.6 us
    all_to_all x1, blocking collectives, body(): lax.all_to_all(update, 'tp', 0, 0, tiled=True, axis_index_groups=sides)  11 us
    ppermute x1, starting transfers between devices, body(): received = lax.ppermute(other, 'tp', opposite)  5.05 us
    pallas_call x1, Pallas kernels, body(): call(attention_kernel, bf16(GROUP, block + STAT_ROWS, HEAD_SIZE), cost(4...  4.33 us
    ppermute x1, starting transfers between devices, body(): lax.ppermute(out_weight, 'tp', [(i, i ^ 1) for i in range(tp)])  3.81 us
    all_to_all x1, starting transfers between devices, body(): lax.all_to_all(copies, 'tp', 0, 0, tiled=True, axis_index_groups=halves)  3.55 us
  transfers between devices with their start and end apart: 4, of which 2 were waited for; matrix products, arithmetic and copies ran while one was open for 0% of the time, Pallas kernels for 6%

profile of v7, /device:TPU:32, one launch (start us, length us, event | category | flops | bytes accessed | tf_op | source)
XLA Modules:
  0.0 105.5 jit_solution(9421116438834150297)
XLA Ops:
  0.0 2.4 %shard_map.100 = (bf16[48,256]{1,0:T(8,128)(2,1)S(1)}, bf16[48,256]{1,0:T(8,128)(2,1)S(1)}, bf16[16,8,2048]{2,1,0:T(8,128)(2,1)}, f32[1,2048]{1,0:T(1,128)S(1)}, f32[1,128]{1,0:T(1,128)S(1)}) custom-call(bf16[8,2048]{1,0:T(8,128)(2,1)} %target.3, bf16[48,2048]{1,0:T(8,128)(2,1)} %source.1, f32[1,2048]{1,0:T(1,128)} %bitcast.4, bf16[2048,256]{1,0:T(8,128)(2,1)} %key_matrix.1, ...), custom_call_target="tpu_custom_call" | custom-call | flops 100663296 | bytes 3000000 | tf_op jit(solution)/shard_map/pallas_call | solution.py:282
  2.4 0.0 copy-start.3
  2.4 5.1 %collective-permute-start = (bf16[48,256]{1,0:T(8,128)(2,1)S(1)}, bf16[48,256]{1,0:T(8,128)(2,1)S(1)}, u32[]{:S(2)}, u32[]{:S(2)}) collective-permute-start(bf16[48,256]{1,0:T(8,128)(2,1)S(1)} %get-tuple-element.16), channel_id=1, source_target_pairs={{0,12},{1,13},{2,14},{3,15},{4,8},{5,9},{6,10},{7,11},{8,4},{9,5},... | collective-permute-start | bytes 73736 | tf_op jit(solution)/shard_map/ppermute | solution.py:321
  7.4 2.0 %collective-permute-done = bf16[48,256]{1,0:T(8,128)(2,1)S(1)} collective-permute-done((bf16[48,256]{1,0:T(8,128)(2,1)S(1)}, bf16[48,256]{1,0:T(8,128)(2,1)S(1)}, u32[]{:S(2)}, u32[]{:S(2)}) %collective-permute-start) | collective-permute-done | bytes 24608 | tf_op jit(solution)/shard_map/ppermute | solution.py:321
  9.5 34.8 %all_gather.3.near = bf16[1536,256]{1,0:T(8,128)(2,1)S(1)} all-gather(bf16[96,256]{1,0:T(8,128)(2,1)S(1)} %pad_maximum_fusion), channel_id=1, replica_groups={{0,48,64,112,128,176,192,240,256,304,320,368,384,432,448,496},{16,32,80..., dimensions={0}, use_global_device_ids=true | all-gather | bytes 835584 | tf_op jit(solution)/shard_map/all_gather | solution.py:324
  44.3 2.3 %collective-permute-start.1 = (bf16[1536,256]{1,0:T(8,128)(2,1)S(1)}, bf16[1536,256]{1,0:T(8,128)(2,1)S(1)}, u32[]{:S(2)}, u32[]{:S(2)}) collective-permute-start(bf16[1536,256]{1,0:T(8,128)(2,1)S(1)} %all_gather.3.near), channel_id=1, source_target_pairs={{0,16},{16,0},{32,48},{48,32},{64,80},{80,64},{96,112},{112,96},{1... | collective-permute-start | bytes 2359304 | tf_op jit(solution)/shard_map/ppermute | solution.py:345
  46.6 0.0 copy-done.3
  46.6 0.0 copy-start
  46.6 18.6 %all_to_all.20 = bf16[16,8,2048]{2,1,0:T(8,128)(2,1)S(1)} all-to-all(bf16[16,8,2048]{2,1,0:T(8,128)(2,1)S(1)} %copy-done.3), channel_id=1, replica_groups=mesh['sp'=32,'tp'=16] {'tp'}, dimensions={0} | all-to-all | bytes 1048576 | tf_op jit(solution)/shard_map/all_to_all | solution.py:322
  65.2 1.3 %shard_map.101 = bf16[8,128,128]{2,1,0:T(8,128)(2,1)} custom-call(bf16[128,2048]{1,0:T(8,128)(2,1)S(1)} %bitcast.3, f32[1,2048]{1,0:T(1,128)S(1)} %get-tuple-element.13.gain, bf16[2048,128]{1,0:T(8,128)(2,1)S(1)} %copy-done, f32[1,128]{1,0:T(1,128)S(1)} %get-tuple-element.14.head_gain), custom_call_target="tpu_custom_call" | custom-call | flops 67108864 | bytes 1400000 | tf_op jit(solution)/shard_map/pallas_call | solution.py:331
  66.5 0.0 copy-start.1
  66.5 3.6 %all-to-all-start.1 = ((bf16[8,128,128]{2,1,0:T(8,128)(2,1)}), bf16[8,128,128]{2,1,0:T(8,128)(2,1)S(1)}, u32[]{:S(2)}, u32[]{:S(2)}) async-start(bf16[8,128,128]{2,1,0:T(8,128)(2,1)} %shard_map.101), calls=%async_computation.1 | async-start | bytes 524288 | tf_op jit(solution)/shard_map/all_to_all | solution.py:342
  70.1 0.0 copy-done.1
  70.1 3.8 %collective-permute-start.2 = (bf16[128,2048]{1,0:T(8,128)(2,1)S(1)}, bf16[128,2048]{1,0:T(8,128)(2,1)S(1)}, u32[]{:S(2)}, u32[]{:S(2)}) collective-permute-start(bf16[128,2048]{1,0:T(8,128)(2,1)S(1)} %copy-done.1), channel_id=1, source_target_pairs={{0,1},{1,0},{2,3},{3,2},{4,5},{5,4},{6,7},{7,6},{8,9},{9,8},{10,11... | collective-permute-start | bytes 1572872 | tf_op jit(solution)/shard_map/ppermute | solution.py:346
  73.9 3.4 %all-to-all-done.1.queries = bf16[8,128,128]{2,1,0:T(8,128)(2,1)S(1)} async-done(((bf16[8,128,128]{2,1,0:T(8,128)(2,1)}), bf16[8,128,128]{2,1,0:T(8,128)(2,1)S(1)}, u32[]{:S(2)}, u32[]{:S(2)}) %all-to-all-start.1) | async-done | bytes 262176 | tf_op jit(solution)/shard_map/all_to_all | solution.py:342
  77.3 0.0 collective-permute-done.1.far
  77.3 4.3 %shard_map.102 = bf16[8,144,128]{2,1,0:T(8,128)(2,1)S(1)} custom-call(bf16[8,128,128]{2,1,0:T(8,128)(2,1)S(1)} %all-to-all-done.1.queries, bf16[1536,256]{1,0:T(8,128)(2,1)S(1)} %all_gather.3.near, bf16[1536,256]{1,0:T(8,128)(2,1)S(1)} %collective-permute-done.1.far), custom_call_target="tpu_custom_call" | custom-call | flops 1610612736 | bytes 2500000 | tf_op jit(solution)/shard_map/pallas_call | solution.py:348
  81.6 11.6 %all_to_all.21.partials = bf16[8,144,128]{2,1,0:T(8,128)(2,1)S(1)} all-to-all(bf16[8,144,128]{2,1,0:T(8,128)(2,1)S(1)} %shard_map.102), channel_id=1, replica_groups={{0,1,2,3,4,5,6,7},{8,9,10,11,12,13,14,15},{16,17,18,19,20,21,22,23},{24..., dimensions={0} | all-to-all | bytes 589824 | tf_op jit(solution)/shard_map/all_to_all | solution.py:354
  93.2 0.3 shard_map.103
  93.5 0.0 collective-permute-done.2.pair_weight
  93.5 0.3 shard_map.104
  93.8 0.0 copy-start.2
  93.8 11.0 %all_to_all.22.parts = bf16[8,8,2048]{2,1,0:T(8,128)(2,1)S(1)} all-to-all(bf16[8,8,2048]{2,1,0:T(8,128)(2,1)S(1)} %shard_map.104), channel_id=1, replica_groups={{0,3,4,7,8,11,12,15},{1,2,5,6,9,10,13,14},{16,19,20,23,24,27,28,31},{17..., dimensions={0} | all-to-all | bytes 524288 | tf_op jit(solution)/shard_map/all_to_all | solution.py:365
  104.9 0.7 shard_map.105
  (3 shorter events, 0.0 us)
Async XLA Ops:
  2.4 44.2 %copy-start.3 = (bf16[16,8,2048]{2,1,0:T(8,128)(2,1)S(1)}, bf16[16,8,2048]{2,1,0:T(8,128)(2,1)}, u32[]{:S(2)}) copy-start(bf16[16,8,2048]{2,1,0:T(8,128)(2,1)} %get-tuple-element.12) | copy-start | bytes 1572868
  2.4 7.1 %collective-permute-start = (bf16[48,256]{1,0:T(8,128)(2,1)S(1)}, bf16[48,256]{1,0:T(8,128)(2,1)S(1)}, u32[]{:S(2)}, u32[]{:S(2)}) collective-permute-start(bf16[48,256]{1,0:T(8,128)(2,1)S(1)} %get-tuple-element.16), channel_id=1, source_target_pairs={{0,12},{1,13},{2,14},{3,15},{4,8},{5,9},{6,10},{7,11},{8,4},{9,5},... | collective-permute-start | bytes 73736 | tf_op jit(solution)/shard_map/ppermute | solution.py:321
  44.3 33.1 %collective-permute-start.1 = (bf16[1536,256]{1,0:T(8,128)(2,1)S(1)}, bf16[1536,256]{1,0:T(8,128)(2,1)S(1)}, u32[]{:S(2)}, u32[]{:S(2)}) collective-permute-start(bf16[1536,256]{1,0:T(8,128)(2,1)S(1)} %all_gather.3.near), channel_id=1, source_target_pairs={{0,16},{16,0},{32,48},{48,32},{64,80},{80,64},{96,112},{112,96},{1... | collective-permute-start | bytes 2359304 | tf_op jit(solution)/shard_map/ppermute | solution.py:345
  46.6 18.6 %copy-start = (bf16[2048,128]{1,0:T(8,128)(2,1)S(1)}, bf16[2048,128]{1,0:T(8,128)(2,1)}, u32[]{:S(2)}) copy-start(bf16[2048,128]{1,0:T(8,128)(2,1)} %weight.1) | copy-start | bytes 1572868
  66.5 3.6 %copy-start.1 = (bf16[128,2048]{1,0:T(8,128)(2,1)S(1)}, bf16[128,2048]{1,0:T(8,128)(2,1)}, u32[]{:S(2)}) copy-start(bf16[128,2048]{1,0:T(8,128)(2,1)} %own_weight.1) | copy-start | bytes 1572868
  66.5 10.8 %all-to-all-start.1 = ((bf16[8,128,128]{2,1,0:T(8,128)(2,1)}), bf16[8,128,128]{2,1,0:T(8,128)(2,1)S(1)}, u32[]{:S(2)}, u32[]{:S(2)}) async-start(bf16[8,128,128]{2,1,0:T(8,128)(2,1)} %shard_map.101), calls=%async_computation.1 | async-start | bytes 524288 | tf_op jit(solution)/shard_map/all_to_all | solution.py:342
  70.1 23.4 %collective-permute-start.2 = (bf16[128,2048]{1,0:T(8,128)(2,1)S(1)}, bf16[128,2048]{1,0:T(8,128)(2,1)S(1)}, u32[]{:S(2)}, u32[]{:S(2)}) collective-permute-start(bf16[128,2048]{1,0:T(8,128)(2,1)S(1)} %copy-done.1), channel_id=1, source_target_pairs={{0,1},{1,0},{2,3},{3,2},{4,5},{5,4},{6,7},{7,6},{8,9},{9,8},{10,11... | collective-permute-start | bytes 1572872 | tf_op jit(solution)/shard_map/ppermute | solution.py:346
  93.8 11.0 %copy-start.2 = (bf16[8,2048]{1,0:T(8,128)(2,1)S(1)}, bf16[8,2048]{1,0:T(8,128)(2,1)}, u32[]{:S(2)}) copy-start(bf16[8,2048]{1,0:T(8,128)(2,1)} %target.3) | copy-start | bytes 98308

commit v8 on v6

--- a/solution.py
+++ b/solution.py
@@ -136,34 +136,40 @@
     return [first, second, third]
 
 
-def attention_kernel(queries, near, far, out):
-    rows = GROUP * HEAD_SIZE
+def attended_part(queries, kv, before=None):
+    scores = lax.dot_general(
+        queries[...].reshape(GROUP * HEAD_SIZE, HEAD_SIZE),
+        kv[:, :HEAD_SIZE],
+        (((1,), (1,)), ((), ())),
+        preferred_element_type=jnp.float32,
+    )
+    peak = jnp.max(scores, axis=-1, keepdims=True)
+    if before is not None:
+        peak = jnp.maximum(before, peak)
+    weights = jnp.exp2((scores - peak) * EXP2_SCALE)
+    total = jnp.sum(weights, axis=-1, keepdims=True)
+    weighted = jnp.dot(
+        weights.astype(jnp.bfloat16), kv[:, HEAD_SIZE:], preferred_element_type=jnp.float32
+    )
+    return peak, total, weighted
+
+
+def near_kernel(queries, kv, peaks, totals, sums):
+    peak, total, weighted = attended_part(queries, kv)
+    peaks[...] = jnp.broadcast_to(peak, peaks.shape)
+    totals[...] = jnp.broadcast_to(total, totals.shape)
+    sums[...] = weighted
+
+
+def far_kernel(queries, kv, peaks, totals, sums, out):
     at_row = lax.broadcasted_iota(jnp.int32, (HEAD_SIZE, HEAD_SIZE), 0)
     at_lane = lax.broadcasted_iota(jnp.int32, (HEAD_SIZE, HEAD_SIZE), 1)
     eye = (at_row == at_lane).astype(jnp.float32)
-    q = queries[...].reshape(rows, HEAD_SIZE)
-    peak = None
-    for kv in (near, far):
-        scores = lax.dot_general(
-            q,
-            kv[:, :HEAD_SIZE],
-            (((1,), (1,)), ((), ())),
-            preferred_element_type=jnp.float32,
-        )
-        highest = jnp.max(scores, axis=-1, keepdims=True)
-        before, peak = peak, highest if peak is None else jnp.maximum(peak, highest)
-        weights = jnp.exp2((scores - peak) * EXP2_SCALE)
-        share = jnp.sum(weights, axis=-1, keepdims=True)
-        part = jnp.dot(
-            weights.astype(jnp.bfloat16),
-            kv[:, HEAD_SIZE:],
-            preferred_element_type=jnp.float32,
-        )
-        if before is None:
-            total, weighted = share, part
-        else:
-            fade = jnp.exp2((before - peak) * EXP2_SCALE)
-            total, weighted = total * fade + share, weighted * fade + part
+    before = peaks[:, :1]
+    peak, share, part = attended_part(queries, kv, before)
+    fade = jnp.exp2((before - peak) * EXP2_SCALE)
+    total = totals[:, :1] * fade + share
+    weighted = sums[...] * fade + part
 
     def as_rows(column, head):
         at = slice(head * HEAD_SIZE, (head + 1) * HEAD_SIZE)
@@ -339,13 +345,17 @@
     )
     far = lax.ppermute(near, "sp", [(i, i ^ 1) for i in range(sp)])
     pair_weight = lax.ppermute(out_weight, "tp", [(i, i ^ 2) for i in range(tp)])
-    keys = 2 * near.shape[0]
+    keys = near.shape[0]
+    work = cost(
+        4 * GROUP * block * keys * HEAD_SIZE, 2500000, GROUP * block * keys
+    )
+    carried = pltpu.VMEM((GROUP * block, HEAD_SIZE), jnp.float32)
+    state = call(near_kernel, (carried,) * 3, work, [VMEM] * 2, (VMEM,) * 3)(
+        all_queries, near
+    )
     partials = call(
-        attention_kernel,
-        bf16(GROUP, block + STAT_ROWS, HEAD_SIZE),
-        cost(4 * GROUP * block * keys * HEAD_SIZE, 2500000, GROUP * block * keys),
-        [VMEM] * 3,
-    )(all_queries, near, pltpu.with_memory_space_constraint(far, pltpu.VMEM))
+        far_kernel, bf16(GROUP, block + STAT_ROWS, HEAD_SIZE), work, [VMEM] * 5
+    )(all_queries, far, *state)
     mine = lax.all_to_all(partials, "tp", 0, 0, tiled=True, axis_index_groups=halves)
     half = bf16(block // 2, HEAD_SIZE)
     own_part, pair_part = call(

time: 105 us -> 95.1 us (0.906)
  blocking collectives: 73 us -> 54.4 us
  starting transfers between devices: 17.1 us -> 25.3 us
  Pallas kernels: 9.21 us -> 12.5 us
  waiting for transfers between devices: 5.07 us -> 2.32 us
    all_to_all x1 -> x0, blocking collectives: 17.6 us -> none  [body(): everyone = lax.all_to_all(target_copies, 'tp', 0, 0, tiled=True)]
    all_to_all x0 -> x1, starting transfers between devices: none -> 7.4 us  [body(): everyone = lax.all_to_all(target_copies, 'tp', 0, 0, tiled=True)]
    pallas_call x1 -> x2, Pallas kernels: 4.32 us -> 7.59 us  [the longest x1 3.96 us: body(): call(near_kernel, (carried,) * 3, work, [VMEM] * 2, (VMEM,) * 3)]
    all_gather x1, blocking collectives: 35 us -> 32.7 us  [body(): lax.all_gather(jnp.concatenate([own, received], axis=0), 'sp', axis=0, ti...]
    ppermute x1, waiting for transfers between devices: 2 us -> 0.01 us  [body(): received = lax.ppermute(other, 'tp', opposite)]
    all_to_all x1, blocking collectives: 9.9 us -> 11.3 us  [body(): lax.all_to_all(update, 'tp', 0, 0, tiled=True, axis_index_groups=sides)]
  transfers between devices with their start and end apart: 4 -> 5, of which waited for: 2 -> 1; matrix products, arithmetic and copies ran while one was open for 0% -> 0% of each run, Pallas kernels for 6% -> 10%
where the time goes in v8:
time: 95.1 us; the launch traced here: 94.6 us
  blocking collectives  54.4 us (57%)
  starting transfers between devices  25.3 us (27%)
  Pallas kernels  12.5 us (13%)
  waiting for transfers between devices  2.32 us (2%)
    all_gather x1, blocking collectives, body(): lax.all_gather(jnp.concatenate([own, received], axis=0), 'sp', axis=0, ti...  32.7 us
    all_to_all x1, blocking collectives, body(): lax.all_to_all(update, 'tp', 0, 0, tiled=True, axis_index_groups=sides)  11.3 us
    all_to_all x1, blocking collectives, body(): lax.all_to_all(partials, 'tp', 0, 0, tiled=True, axis_index_groups=halves)  10.4 us
    all_to_all x1, starting transfers between devices, body(): everyone = lax.all_to_all(target_copies, 'tp', 0, 0, tiled=True)  7.4 us
    all_to_all x1, starting transfers between devices, body(): lax.all_to_all(copies, 'tp', 0, 0, tiled=True, axis_index_groups=halves)  5.85 us
    ppermute x1, starting transfers between devices, body(): received = lax.ppermute(other, 'tp', opposite)  4.92 us
    ppermute x1, starting transfers between devices, body(): lax.ppermute(out_weight, 'tp', [(i, i ^ 2) for i in range(tp)])  3.97 us
    pallas_call x1, Pallas kernels, body(): call(near_kernel, (carried,) * 3, work, [VMEM] * 2, (VMEM,) * 3)  3.96 us
  transfers between devices with their start and end apart: 5, of which 1 were waited for; matrix products, arithmetic and copies ran while one was open for 0% of the time, Pallas kernels for 10%

profile of v8, /device:TPU:2, one launch (start us, length us, event | category | flops | bytes accessed | tf_op | source)
XLA Modules:
  0.0 94.6 jit_solution(5492123688076040797)
XLA Ops:
  0.0 2.4 %shard_map.100 = (bf16[48,256]{1,0:T(8,128)(2,1)S(1)}, bf16[48,256]{1,0:T(8,128)(2,1)S(1)}, bf16[16,8,2048]{2,1,0:T(8,128)(2,1)}, f32[1,2048]{1,0:T(1,128)S(1)}, f32[1,128]{1,0:T(1,128)S(1)}) custom-call(bf16[8,2048]{1,0:T(8,128)(2,1)} %target.3, bf16[48,2048]{1,0:T(8,128)(2,1)} %source.1, f32[1,2048]{1,0:T(1,128)} %bitcast.4, bf16[2048,256]{1,0:T(8,128)(2,1)} %key_matrix.1, ...), custom_call_target="tpu_custom_call" | custom-call | flops 100663296 | bytes 3000000 | tf_op jit(solution)/shard_map/pallas_call | solution.py:283
  2.4 4.9 %collective-permute-start = (bf16[48,256]{1,0:T(8,128)(2,1)S(1)}, bf16[48,256]{1,0:T(8,128)(2,1)S(1)}, u32[]{:S(2)}, u32[]{:S(2)}) collective-permute-start(bf16[48,256]{1,0:T(8,128)(2,1)S(1)} %get-tuple-element.19), channel_id=1, source_target_pairs={{0,12},{1,13},{2,14},{3,15},{4,8},{5,9},{6,10},{7,11},{8,4},{9,5},... | collective-permute-start | bytes 73736 | tf_op jit(solution)/shard_map/ppermute | solution.py:322
  7.3 7.4 %all-to-all-start = ((bf16[16,8,2048]{2,1,0:T(8,128)(2,1)}), bf16[16,8,2048]{2,1,0:T(8,128)(2,1)S(1)}, u32[]{:S(2)}, u32[]{:S(2)}) async-start(bf16[16,8,2048]{2,1,0:T(8,128)(2,1)} %get-tuple-element.15), calls=%async_computation | async-start | bytes 1048576 | tf_op jit(solution)/shard_map/all_to_all | solution.py:323
  14.7 0.0 collective-permute-done
  14.7 32.7 %all_gather.3.kv = bf16[1536,256]{1,0:T(8,128)(2,1)S(1)} all-gather(bf16[96,256]{1,0:T(8,128)(2,1)S(1)} %pad_maximum_fusion), channel_id=1, replica_groups={{0,48,64,112,128,176,192,240,256,304,320,368,384,432,448,496},{16,32,80..., dimensions={0}, use_global_device_ids=true | all-gather | bytes 835584 | tf_op jit(solution)/shard_map/all_gather | solution.py:325
  47.4 3.1 %collective-permute-start.1 = (bf16[1536,256]{1,0:T(8,128)(2,1)S(1)}, bf16[1536,256]{1,0:T(8,128)(2,1)S(1)}, u32[]{:S(2)}, u32[]{:S(2)}) collective-permute-start(bf16[1536,256]{1,0:T(8,128)(2,1)S(1)} %all_gather.3.kv), channel_id=1, source_target_pairs={{0,16},{16,0},{32,48},{48,32},{64,80},{80,64},{96,112},{112,96},{1... | collective-permute-start | bytes 2359304 | tf_op jit(solution)/shard_map/ppermute | solution.py:346
  50.5 0.0 all-to-all-done
  50.5 0.0 copy-done
  50.6 1.3 %shard_map.101 = bf16[8,128,128]{2,1,0:T(8,128)(2,1)} custom-call(bf16[128,2048]{1,0:T(8,128)(2,1)S(1)} %bitcast.3, f32[1,2048]{1,0:T(1,128)S(1)} %get-tuple-element.16.gain, bf16[2048,128]{1,0:T(8,128)(2,1)S(1)} %copy-done, f32[1,128]{1,0:T(1,128)S(1)} %get-tuple-element.17.head_gain), custom_call_target="tpu_custom_call" | custom-call | flops 67108864 | bytes 1400000 | tf_op jit(solution)/shard_map/pallas_call | solution.py:332
  51.9 0.0 copy-start.1
  51.9 5.8 %all-to-all-start.1 = ((bf16[8,128,128]{2,1,0:T(8,128)(2,1)}), bf16[8,128,128]{2,1,0:T(8,128)(2,1)S(1)}, u32[]{:S(2)}, u32[]{:S(2)}) async-start(bf16[8,128,128]{2,1,0:T(8,128)(2,1)} %shard_map.101), calls=%async_computation.1 | async-start | bytes 524288 | tf_op jit(solution)/shard_map/all_to_all | solution.py:343
  57.7 0.0 copy-done.1
  57.7 4.0 %collective-permute-start.2 = (bf16[128,2048]{1,0:T(8,128)(2,1)S(1)}, bf16[128,2048]{1,0:T(8,128)(2,1)S(1)}, u32[]{:S(2)}, u32[]{:S(2)}) collective-permute-start(bf16[128,2048]{1,0:T(8,128)(2,1)S(1)} %copy-done.1), channel_id=1, source_target_pairs={{0,2},{1,3},{2,0},{3,1},{4,6},{5,7},{6,4},{7,5},{8,10},{9,11},{10,... | collective-permute-start | bytes 1572872 | tf_op jit(solution)/shard_map/ppermute | solution.py:347
  61.7 2.3 %all-to-all-done.1.queries = bf16[8,128,128]{2,1,0:T(8,128)(2,1)S(1)} async-done(((bf16[8,128,128]{2,1,0:T(8,128)(2,1)}), bf16[8,128,128]{2,1,0:T(8,128)(2,1)S(1)}, u32[]{:S(2)}, u32[]{:S(2)}) %all-to-all-start.1) | async-done | bytes 262176 | tf_op jit(solution)/shard_map/all_to_all | solution.py:343
  64.0 4.0 %shard_map.102 = (f32[1024,128]{1,0:T(8,128)S(1)}, f32[1024,128]{1,0:T(8,128)S(1)}, f32[1024,128]{1,0:T(8,128)S(1)}) custom-call(bf16[8,128,128]{2,1,0:T(8,128)(2,1)S(1)} %all-to-all-done.1.queries, bf16[1536,256]{1,0:T(8,128)(2,1)S(1)} %all_gather.3.kv), custom_call_target="tpu_custom_call" | custom-call | flops 805306368 | bytes 2500000 | tf_op jit(solution)/shard_map/pallas_call | solution.py:353
  68.0 0.0 collective-permute-done.1.kv
  68.0 3.6 %shard_map.103 = bf16[8,144,128]{2,1,0:T(8,128)(2,1)S(1)} custom-call(bf16[8,128,128]{2,1,0:T(8,128)(2,1)S(1)} %all-to-all-done.1.queries, bf16[1536,256]{1,0:T(8,128)(2,1)S(1)} %collective-permute-done.1.kv, f32[1024,128]{1,0:T(8,128)S(1)} %get-tuple-element.20.peaks, f32[1024,128]{1,0:T(8,128)S(1)} %get-tuple-element.21.totals, ...), custom_call_target="tpu_custom_call" | custom-call | flops 805306368 | bytes 2500000 | tf_op jit(solution)/shard_map/pallas_call | solution.py:356
  71.6 10.4 %all_to_all.20.partials = bf16[8,144,128]{2,1,0:T(8,128)(2,1)S(1)} all-to-all(bf16[8,144,128]{2,1,0:T(8,128)(2,1)S(1)} %shard_map.103), channel_id=1, replica_groups={{0,1,2,3,4,5,6,7},{8,9,10,11,12,13,14,15},{16,17,18,19,20,21,22,23},{24..., dimensions={0} | all-to-all | bytes 589824 | tf_op jit(solution)/shard_map/all_to_all | solution.py:359
  82.0 0.3 shard_map.104
  82.3 0.0 collective-permute-done.2.pair_weight
  82.3 0.3 shard_map.105
  82.6 0.0 copy-start.2
  82.6 11.3 %all_to_all.21.parts = bf16[8,8,2048]{2,1,0:T(8,128)(2,1)S(1)} all-to-all(bf16[8,8,2048]{2,1,0:T(8,128)(2,1)S(1)} %shard_map.105), channel_id=1, replica_groups={{0,1,4,5,8,9,12,13},{2,3,6,7,10,11,14,15},{16,17,20,21,24,25,28,29},{18..., dimensions={0} | all-to-all | bytes 524288 | tf_op jit(solution)/shard_map/all_to_all | solution.py:370
  93.9 0.7 shard_map.106
  (3 shorter events, 0.0 us)
Async XLA Ops:
  2.4 12.3 %collective-permute-start = (bf16[48,256]{1,0:T(8,128)(2,1)S(1)}, bf16[48,256]{1,0:T(8,128)(2,1)S(1)}, u32[]{:S(2)}, u32[]{:S(2)}) collective-permute-start(bf16[48,256]{1,0:T(8,128)(2,1)S(1)} %get-tuple-element.19), channel_id=1, source_target_pairs={{0,12},{1,13},{2,14},{3,15},{4,8},{5,9},{6,10},{7,11},{8,4},{9,5},... | collective-permute-start | bytes 73736 | tf_op jit(solution)/shard_map/ppermute | solution.py:322
  7.3 43.2 %all-to-all-start = ((bf16[16,8,2048]{2,1,0:T(8,128)(2,1)}), bf16[16,8,2048]{2,1,0:T(8,128)(2,1)S(1)}, u32[]{:S(2)}, u32[]{:S(2)}) async-start(bf16[16,8,2048]{2,1,0:T(8,128)(2,1)} %get-tuple-element.15), calls=%async_computation | async-start | bytes 1048576 | tf_op jit(solution)/shard_map/all_to_all | solution.py:323
  14.7 35.8 %copy-start = (bf16[2048,128]{1,0:T(8,128)(2,1)S(1)}, bf16[2048,128]{1,0:T(8,128)(2,1)}, u32[]{:S(2)}) copy-start(bf16[2048,128]{1,0:T(8,128)(2,1)} %weight.1) | copy-start | bytes 1572868
  47.4 20.6 %collective-permute-start.1 = (bf16[1536,256]{1,0:T(8,128)(2,1)S(1)}, bf16[1536,256]{1,0:T(8,128)(2,1)S(1)}, u32[]{:S(2)}, u32[]{:S(2)}) collective-permute-start(bf16[1536,256]{1,0:T(8,128)(2,1)S(1)} %all_gather.3.kv), channel_id=1, source_target_pairs={{0,16},{16,0},{32,48},{48,32},{64,80},{80,64},{96,112},{112,96},{1... | collective-permute-start | bytes 2359304 | tf_op jit(solution)/shard_map/ppermute | solution.py:346
  51.9 5.9 %copy-start.1 = (bf16[128,2048]{1,0:T(8,128)(2,1)S(1)}, bf16[128,2048]{1,0:T(8,128)(2,1)}, u32[]{:S(2)}) copy-start(bf16[128,2048]{1,0:T(8,128)(2,1)} %own_weight.1) | copy-start | bytes 1572868
  51.9 12.1 %all-to-all-start.1 = ((bf16[8,128,128]{2,1,0:T(8,128)(2,1)}), bf16[8,128,128]{2,1,0:T(8,128)(2,1)S(1)}, u32[]{:S(2)}, u32[]{:S(2)}) async-start(bf16[8,128,128]{2,1,0:T(8,128)(2,1)} %shard_map.101), calls=%async_computation.1 | async-start | bytes 524288 | tf_op jit(solution)/shard_map/all_to_all | solution.py:343
  57.7 24.5 %collective-permute-start.2 = (bf16[128,2048]{1,0:T(8,128)(2,1)S(1)}, bf16[128,2048]{1,0:T(8,128)(2,1)S(1)}, u32[]{:S(2)}, u32[]{:S(2)}) collective-permute-start(bf16[128,2048]{1,0:T(8,128)(2,1)S(1)} %copy-done.1), channel_id=1, source_target_pairs={{0,2},{1,3},{2,0},{3,1},{4,6},{5,7},{6,4},{7,5},{8,10},{9,11},{10,... | collective-permute-start | bytes 1572872 | tf_op jit(solution)/shard_map/ppermute | solution.py:347
  82.6 11.3 %copy-start.2 = (bf16[8,2048]{1,0:T(8,128)(2,1)S(1)}, bf16[8,2048]{1,0:T(8,128)(2,1)}, u32[]{:S(2)}) copy-start(bf16[8,2048]{1,0:T(8,128)(2,1)} %target.3) | copy-start | bytes 98308

commit v9 on v6

--- a/solution.py
+++ b/solution.py
@@ -172,17 +172,18 @@
     for head in range(GROUP):
         if head % 4 >= 2:
             continue
+        opposite = head + 3 - 2 * (head % 4)
         stats = []
-        for h in (head, head + 2):
+        for h in (head, opposite):
             stats += as_rows(peak, h) + as_rows(total, h)
         empty = jnp.zeros((STAT_ROWS - len(stats), HEAD_SIZE), jnp.bfloat16)
         stats = jnp.concatenate(stats + [empty], axis=0)
         for side in range(2):
-            to = head + 2 * side
+            to = opposite if side else head
             out[to, :HEAD_SIZE, :] = jnp.concatenate(
                 [
                     weighted[h * HEAD_SIZE + i : h * HEAD_SIZE + i + 16]
-                    for h in (head, head + 2)
+                    for h in (head, opposite)
                     for i in range(16 * side, HEAD_SIZE, 32)
                 ],
                 axis=0,
@@ -232,7 +233,7 @@
     out[...] = (target[...].astype(jnp.float32) + update).astype(jnp.bfloat16)
 
 
-def call(kernel, outs, estimate, specs, out_specs=None, scratch=(), vmem=32 * 1024 * 1024):
+def call(kernel, outs, estimate, specs, out_specs=None, scratch=(), vmem=48 * 1024 * 1024):
     return pl.pallas_call(
         kernel,
         out_shape=outs,
@@ -338,14 +339,14 @@
         copies, "tp", 0, 0, tiled=True, axis_index_groups=halves
     )
     far = lax.ppermute(near, "sp", [(i, i ^ 1) for i in range(sp)])
-    pair_weight = lax.ppermute(out_weight, "tp", [(i, i ^ 2) for i in range(tp)])
+    pair_weight = lax.ppermute(out_weight, "tp", [(i, i ^ 3) for i in range(tp)])
     keys = 2 * near.shape[0]
     partials = call(
         attention_kernel,
         bf16(GROUP, block + STAT_ROWS, HEAD_SIZE),
         cost(4 * GROUP * block * keys * HEAD_SIZE, 2500000, GROUP * block * keys),
         [VMEM] * 3,
-    )(all_queries, near, pltpu.with_memory_space_constraint(far, pltpu.VMEM))
+    )(all_queries, near, far)
     mine = lax.all_to_all(partials, "tp", 0, 0, tiled=True, axis_index_groups=halves)
     half = bf16(block // 2, HEAD_SIZE)
     own_part, pair_part = call(

time: 105 us -> 104 us (level)
  no operation moved by 1% of the time
where the time goes in v9:
time: 104 us
  blocking collectives  72.9 us (70%)
  starting transfers between devices  16.5 us (16%)
  Pallas kernels  9.22 us (9%)
  waiting for transfers between devices  4.89 us (5%)
    all_gather x1, blocking collectives, body(): lax.all_gather(jnp.concatenate([own, received], axis=0), 'sp', axis=0, ti...  35 us
    all_to_all x1, blocking collectives, body(): everyone = lax.all_to_all(target_copies, 'tp', 0, 0, tiled=True)  17.6 us
    all_to_all x1, blocking collectives, body(): lax.all_to_all(partials, 'tp', 0, 0, tiled=True, axis_index_groups=halves)  10.4 us
    all_to_all x1, blocking collectives, body(): lax.all_to_all(update, 'tp', 0, 0, tiled=True, axis_index_groups=sides)  9.9 us
    ppermute x1, starting transfers between devices, body(): received = lax.ppermute(other, 'tp', opposite)  5.05 us
    all_to_all x1, starting transfers between devices, body(): lax.all_to_all(copies, 'tp', 0, 0, tiled=True, axis_index_groups=halves)  4.92 us
    pallas_call x1, Pallas kernels, body(): call(attention_kernel, bf16(GROUP, block + STAT_ROWS, HEAD_SIZE), cost(4...  4.34 us
    ppermute x1, starting transfers between devices, body(): lax.ppermute(out_weight, 'tp', [(i, i ^ 3) for i in range(tp)])  3.37 us
  transfers between devices with their start and end apart: 4, of which 2 were waited for; matrix products, arithmetic and copies ran while one was open for 0% of the time, Pallas kernels for 6%

profile of v9, /device:TPU:2, one launch (start us, length us, event | category | flops | bytes accessed | tf_op | source)
XLA Modules:
  0.0 103.6 jit_solution(10319197871782108552)
XLA Ops:
  0.0 2.4 %shard_map.100 = (bf16[48,256]{1,0:T(8,128)(2,1)S(1)}, bf16[48,256]{1,0:T(8,128)(2,1)S(1)}, bf16[16,8,2048]{2,1,0:T(8,128)(2,1)}, f32[1,2048]{1,0:T(1,128)S(1)}, f32[1,128]{1,0:T(1,128)S(1)}) custom-call(bf16[8,2048]{1,0:T(8,128)(2,1)} %target.3, bf16[48,2048]{1,0:T(8,128)(2,1)} %source.1, f32[1,2048]{1,0:T(1,128)} %bitcast.4, bf16[2048,256]{1,0:T(8,128)(2,1)} %key_matrix.1, ...), custom_call_target="tpu_custom_call" | custom-call | flops 100663296 | bytes 3000000 | tf_op jit(solution)/shard_map/pallas_call | solution.py:278
  2.4 0.0 copy-start.3
  2.4 5.1 %collective-permute-start = (bf16[48,256]{1,0:T(8,128)(2,1)S(1)}, bf16[48,256]{1,0:T(8,128)(2,1)S(1)}, u32[]{:S(2)}, u32[]{:S(2)}) collective-permute-start(bf16[48,256]{1,0:T(8,128)(2,1)S(1)} %get-tuple-element.16), channel_id=1, source_target_pairs={{0,12},{1,13},{2,14},{3,15},{4,8},{5,9},{6,10},{7,11},{8,4},{9,5},... | collective-permute-start | bytes 73736 | tf_op jit(solution)/shard_map/ppermute | solution.py:317
  7.4 2.0 %collective-permute-done = bf16[48,256]{1,0:T(8,128)(2,1)S(1)} collective-permute-done((bf16[48,256]{1,0:T(8,128)(2,1)S(1)}, bf16[48,256]{1,0:T(8,128)(2,1)S(1)}, u32[]{:S(2)}, u32[]{:S(2)}) %collective-permute-start) | collective-permute-done | bytes 24608 | tf_op jit(solution)/shard_map/ppermute | solution.py:317
  9.5 35.0 %all_gather.3.near = bf16[1536,256]{1,0:T(8,128)(2,1)S(1)} all-gather(bf16[96,256]{1,0:T(8,128)(2,1)S(1)} %pad_maximum_fusion), channel_id=1, replica_groups={{0,48,64,112,128,176,192,240,256,304,320,368,384,432,448,496},{16,32,80..., dimensions={0}, use_global_device_ids=true | all-gather | bytes 835584 | tf_op jit(solution)/shard_map/all_gather | solution.py:320
  44.4 3.2 %collective-permute-start.1 = (bf16[1536,256]{1,0:T(8,128)(2,1)S(1)}, bf16[1536,256]{1,0:T(8,128)(2,1)S(1)}, u32[]{:S(2)}, u32[]{:S(2)}) collective-permute-start(bf16[1536,256]{1,0:T(8,128)(2,1)S(1)} %all_gather.3.near), channel_id=1, source_target_pairs={{0,16},{16,0},{32,48},{48,32},{64,80},{80,64},{96,112},{112,96},{1... | collective-permute-start | bytes 2359304 | tf_op jit(solution)/shard_map/ppermute | solution.py:341
  47.6 0.0 copy-start
  47.6 17.6 %all_to_all.20 = bf16[16,8,2048]{2,1,0:T(8,128)(2,1)S(1)} all-to-all(bf16[16,8,2048]{2,1,0:T(8,128)(2,1)S(1)} %copy-done.3), channel_id=1, replica_groups=mesh['sp'=32,'tp'=16] {'tp'}, dimensions={0} | all-to-all | bytes 1048576 | tf_op jit(solution)/shard_map/all_to_all | solution.py:318
  65.2 0.0 copy-done
  65.2 1.3 %shard_map.101 = bf16[8,128,128]{2,1,0:T(8,128)(2,1)} custom-call(bf16[128,2048]{1,0:T(8,128)(2,1)S(1)} %bitcast.3, f32[1,2048]{1,0:T(1,128)S(1)} %get-tuple-element.13.gain, bf16[2048,128]{1,0:T(8,128)(2,1)S(1)} %copy-done, f32[1,128]{1,0:T(1,128)S(1)} %get-tuple-element.14.head_gain), custom_call_target="tpu_custom_call" | custom-call | flops 67108864 | bytes 1400000 | tf_op jit(solution)/shard_map/pallas_call | solution.py:327
  66.5 0.0 copy-start.1
  66.5 4.9 %all-to-all-start.1 = ((bf16[8,128,128]{2,1,0:T(8,128)(2,1)}), bf16[8,128,128]{2,1,0:T(8,128)(2,1)S(1)}, u32[]{:S(2)}, u32[]{:S(2)}) async-start(bf16[8,128,128]{2,1,0:T(8,128)(2,1)} %shard_map.101), calls=%async_computation.1 | async-start | bytes 524288 | tf_op jit(solution)/shard_map/all_to_all | solution.py:338
  71.4 3.4 %collective-permute-start.2 = (bf16[128,2048]{1,0:T(8,128)(2,1)S(1)}, bf16[128,2048]{1,0:T(8,128)(2,1)S(1)}, u32[]{:S(2)}, u32[]{:S(2)}) collective-permute-start(bf16[128,2048]{1,0:T(8,128)(2,1)S(1)} %copy-done.1), channel_id=1, source_target_pairs={{0,3},{1,2},{2,1},{3,0},{4,7},{5,6},{6,5},{7,4},{8,11},{9,10},{10,... | collective-permute-start | bytes 1572872 | tf_op jit(solution)/shard_map/ppermute | solution.py:342
  74.8 2.9 %all-to-all-done.1.queries = bf16[8,128,128]{2,1,0:T(8,128)(2,1)S(1)} async-done(((bf16[8,128,128]{2,1,0:T(8,128)(2,1)}), bf16[8,128,128]{2,1,0:T(8,128)(2,1)S(1)}, u32[]{:S(2)}, u32[]{:S(2)}) %all-to-all-start.1) | async-done | bytes 262176 | tf_op jit(solution)/shard_map/all_to_all | solution.py:338
  77.7 0.0 collective-permute-done.1.far
  77.7 4.3 %shard_map.102 = bf16[8,144,128]{2,1,0:T(8,128)(2,1)S(1)} custom-call(bf16[8,128,128]{2,1,0:T(8,128)(2,1)S(1)} %all-to-all-done.1.queries, bf16[1536,256]{1,0:T(8,128)(2,1)S(1)} %all_gather.3.near, bf16[1536,256]{1,0:T(8,128)(2,1)S(1)} %collective-permute-done.1.far), custom_call_target="tpu_custom_call" | custom-call | flops 1610612736 | bytes 2500000 | tf_op jit(solution)/shard_map/pallas_call | solution.py:344
  82.0 10.4 %all_to_all.21.partials = bf16[8,144,128]{2,1,0:T(8,128)(2,1)S(1)} all-to-all(bf16[8,144,128]{2,1,0:T(8,128)(2,1)S(1)} %shard_map.102), channel_id=1, replica_groups={{0,1,2,3,4,5,6,7},{8,9,10,11,12,13,14,15},{16,17,18,19,20,21,22,23},{24..., dimensions={0} | all-to-all | bytes 589824 | tf_op jit(solution)/shard_map/all_to_all | solution.py:350
  92.5 0.3 shard_map.103
  92.7 0.0 collective-permute-done.2.pair_weight
  92.7 0.3 shard_map.104
  93.0 0.0 copy-start.2
  93.1 9.9 %all_to_all.22.parts = bf16[8,8,2048]{2,1,0:T(8,128)(2,1)S(1)} all-to-all(bf16[8,8,2048]{2,1,0:T(8,128)(2,1)S(1)} %shard_map.104), channel_id=1, replica_groups={{0,1,4,5,8,9,12,13},{2,3,6,7,10,11,14,15},{16,17,20,21,24,25,28,29},{18..., dimensions={0} | all-to-all | bytes 524288 | tf_op jit(solution)/shard_map/all_to_all | solution.py:361
  103.0 0.0 copy-done.2
  103.0 0.7 shard_map.105
  (3 shorter events, 0.0 us)
Async XLA Ops:
  2.4 45.2 %copy-start.3 = (bf16[16,8,2048]{2,1,0:T(8,128)(2,1)S(1)}, bf16[16,8,2048]{2,1,0:T(8,128)(2,1)}, u32[]{:S(2)}) copy-start(bf16[16,8,2048]{2,1,0:T(8,128)(2,1)} %get-tuple-element.12) | copy-start | bytes 1572868
  2.4 7.1 %collective-permute-start = (bf16[48,256]{1,0:T(8,128)(2,1)S(1)}, bf16[48,256]{1,0:T(8,128)(2,1)S(1)}, u32[]{:S(2)}, u32[]{:S(2)}) collective-permute-start(bf16[48,256]{1,0:T(8,128)(2,1)S(1)} %get-tuple-element.16), channel_id=1, source_target_pairs={{0,12},{1,13},{2,14},{3,15},{4,8},{5,9},{6,10},{7,11},{8,4},{9,5},... | collective-permute-start | bytes 73736 | tf_op jit(solution)/shard_map/ppermute | solution.py:317
  44.4 33.3 %collective-permute-start.1 = (bf16[1536,256]{1,0:T(8,128)(2,1)S(1)}, bf16[1536,256]{1,0:T(8,128)(2,1)S(1)}, u32[]{:S(2)}, u32[]{:S(2)}) collective-permute-start(bf16[1536,256]{1,0:T(8,128)(2,1)S(1)} %all_gather.3.near), channel_id=1, source_target_pairs={{0,16},{16,0},{32,48},{48,32},{64,80},{80,64},{96,112},{112,96},{1... | collective-permute-start | bytes 2359304 | tf_op jit(solution)/shard_map/ppermute | solution.py:341
  47.6 17.6 %copy-start = (bf16[2048,128]{1,0:T(8,128)(2,1)S(1)}, bf16[2048,128]{1,0:T(8,128)(2,1)}, u32[]{:S(2)}) copy-start(bf16[2048,128]{1,0:T(8,128)(2,1)} %weight.1) | copy-start | bytes 1572868
  66.5 4.9 %copy-start.1 = (bf16[128,2048]{1,0:T(8,128)(2,1)S(1)}, bf16[128,2048]{1,0:T(8,128)(2,1)}, u32[]{:S(2)}) copy-start(bf16[128,2048]{1,0:T(8,128)(2,1)} %own_weight.1) | copy-start | bytes 1572868
  66.5 11.2 %all-to-all-start.1 = ((bf16[8,128,128]{2,1,0:T(8,128)(2,1)}), bf16[8,128,128]{2,1,0:T(8,128)(2,1)S(1)}, u32[]{:S(2)}, u32[]{:S(2)}) async-start(bf16[8,128,128]{2,1,0:T(8,128)(2,1)} %shard_map.101), calls=%async_computation.1 | async-start | bytes 524288 | tf_op jit(solution)/shard_map/all_to_all | solution.py:338
  71.4 21.3 %collective-permute-start.2 = (bf16[128,2048]{1,0:T(8,128)(2,1)S(1)}, bf16[128,2048]{1,0:T(8,128)(2,1)S(1)}, u32[]{:S(2)}, u32[]{:S(2)}) collective-permute-start(bf16[128,2048]{1,0:T(8,128)(2,1)S(1)} %copy-done.1), channel_id=1, source_target_pairs={{0,3},{1,2},{2,1},{3,0},{4,7},{5,6},{6,5},{7,4},{8,11},{9,10},{10,... | collective-permute-start | bytes 1572872 | tf_op jit(solution)/shard_map/ppermute | solution.py:342
  93.0 9.9 %copy-start.2 = (bf16[8,2048]{1,0:T(8,128)(2,1)S(1)}, bf16[8,2048]{1,0:T(8,128)(2,1)}, u32[]{:S(2)}) copy-start(bf16[8,2048]{1,0:T(8,128)(2,1)} %target.3) | copy-start | bytes 98308
